TPU v7x, 1024 devices: a whole 4x4x32 slice. The times are simulated.
1024 devices in a mesh: sp: 256 (over z, x, core), tp: 4 (over y).
Axes of the slice: x: 4, y: 4, z: 32, core: 2. Of those that a mesh axis runs over, the one named last changes fastest.
Arguments:
- proj_value: bfloat16 [98304, 1024], P('sp', 'tp'), may hold values from -6 to 6
- proj_gate: bfloat16 [98304, 1024], P('sp', 'tp'), may hold values from -8 to 8
- out_cotangent: bfloat16 [98304, 2048], P('sp'), may hold values from -24 to 24
- out_weight: bfloat16 [1024, 2048], P('tp'), may hold values from -0.1875 to 0.1875
- conv_taps: bfloat16 [31, 1024], P(None, 'tp'), may hold values from -1 to 1
- norm_gain: float32 [1024], P('tp'), may hold values from 0.1 to 1.9
- row_mean: float32 [98304], P('sp'), may hold values from -2 to 2
- row_scale: float32 [98304], P('sp'), may hold values from 0.7 to 3
Outputs:
- value_grad: bfloat16 [98304, 1024], P('sp', 'tp')
- gate_grad: bfloat16 [98304, 1024], P('sp', 'tp')
- out_weight_grad: float32 [2048, 1024], P('sp', 'tp')
- taps_grad: float32 [31, 1024], P(None, 'tp')
- gain_grad: float32 [1024], P('tp')
All inputs are finite; a program needn't handle non-finite values.
Results may differ from a plain program's by a relative error of at most 0.0047.
Values may be sent and summed in bfloat16 or wider, within the bound.
No kernel may reach another device: no remote copies, remote signals or barrier semaphores. Data moves between devices by JAX's collectives and lax.ppermute only.
A program may use at most 32 MiB of HBM per device.

v0:
```python
import jax
import jax.numpy as jnp
from jax import lax
from jax.experimental import pallas as pl
from jax.experimental.pallas import tpu as pltpu
from jax.sharding import Mesh
from jax.sharding import PartitionSpec as P


SP = ("zh", "zl", "x", "c")
NEAR = ("zl", "x")
FAR = 16
CLOSE = 8
AXES = (("zh", FAR), ("zl", 2), ("x", 4), ("c", 2))
TP = 4
SUMS_ORDER = [3, 0, 1, 2]
OFFSETS = ((0, -1, -2, -3, 3, 2, 1, -4), (6, 7, 8, 5, -7, -6, -5, 4))
BLOCK = CLOSE * 2 * 8
GATHER_ORDER = [(place + 1) % (2 * CLOSE) for place in range(2 * CLOSE)]
TAPS = 31
SMALL = TAPS + 1
ROWS = 384
EDGE = 32
LANES = 128
HALVES = 2
WIDTH = HALVES * LANES
MODEL = 2048
OWN = 8
PART_ENDS = (128, 256, 352)
CHUNK = 64
WIDE = jnp.float32
NARROW = jnp.bfloat16


def shifted(value, axis, steps):
    count = lax.axis_size(axis)
    first, last = (max(0, -steps), min(count, count - steps))
    return lax.ppermute(value, axis, [(source, source + steps) for source in range(first, last)])


def exchange(pieces, axes, order=None):
    groups = order and [order]
    return lax.all_to_all(pieces, axes, 0, 0, tiled=True, axis_index_groups=groups)


def lanes(half):
    return slice(half * LANES, (half + 1) * LANES)


def column(row):
    return jnp.transpose(jnp.broadcast_to(row, (LANES, LANES)))


def call(body, outs, *args, flops=0, limit=6):
    shapes = [jax.ShapeDtypeStruct(shape, dtype) for shape, dtype in outs]
    size = sum(a.size * a.dtype.itemsize for a in (*args, *shapes))
    return pl.pallas_call(
        body,
        out_shape=shapes,
        compiler_params=pltpu.CompilerParams(vmem_limit_bytes=limit << 20),
        cost_estimate=pl.CostEstimate(flops=flops, bytes_accessed=size, transcendentals=0),
    )(*args)


def norm_backward(normed, factor, gain_row, upstream):
    active = normed * gain_row
    sig = jax.nn.sigmoid(active)
    hidden = (active * sig).astype(NARROW)
    d_active = upstream * sig * (1.0 + active * (1.0 - sig))
    d_normed = d_active * gain_row
    gain_part = jnp.sum((d_active * normed).reshape(normed.shape[0] // 8, 8, LANES), 0)
    return hidden, factor * d_normed, factor * normed, d_normed, d_normed * normed, gain_part


def convolve(source, half, taps_wide, start, size):
    conv = jnp.zeros((size, LANES), WIDE)
    for tap in range(TAPS):
        begin = start + tap + EDGE - TAPS + 1
        conv = conv + taps_wide[tap : tap + 1, lanes(half)] * source[half, begin : begin + size]
    return conv


def column_sums(source):
    return jnp.sum(jnp.transpose(source), 0, keepdims=True)


def both_blocks(cotangent, place, near):
    far, core = place[0] // (2 * CLOSE), place[0] % 2
    low, high = OFFSETS[0][near], OFFSETS[1][near]
    own = lax.rem(far + jnp.where(core == 0, low, high) + FAR, FAR)
    theirs = lax.rem(far + jnp.where(core == 0, high, low) + FAR, FAR)
    columns = [pl.ds(pl.multiple_of(block * BLOCK, BLOCK), BLOCK) for block in (own, theirs)]
    return jnp.concatenate([cotangent[:, columns[0]], cotangent[:, columns[1]]], 1)


def forward(
    place, value, gate, cotangent, weight, far_taps, far_gain, far_mean, far_scale,
    gated, scaled, spread, sums, gain_part, first_upstream, first_cotangent, product,
    held_value, held_gate, held, held_weight, taps, gain, mean, scale, arrivals,
    taps_wide, mean_columns, scale_columns, sum_first, sum_second,
    hidden, normed, upstream,
):
    copies = [
        pltpu.make_async_copy(source, target, arrivals.at[i])
        for i, (source, target) in enumerate(
            (
                (value, held_value), (gate, held_gate), (far_taps, taps), (far_mean, mean),
                (far_scale, scale), (far_gain, gain), (weight, held_weight), (cotangent, held),
            )
        )
    ]
    for copy in copies:
        copy.start()
    sum_first[0:EDGE] = jnp.zeros((EDGE, LANES), WIDE)
    sum_second[0:EDGE] = jnp.zeros((EDGE, LANES), WIDE)
    hidden[0:EDGE] = jnp.zeros((EDGE, WIDTH), WIDE)
    for copy in copies[:6]:
        copy.wait()
    taps_wide[0:TAPS] = taps[...].astype(WIDE)
    for block in range(ROWS // LANES):
        rows = slice(block * LANES, (block + 1) * LANES)
        mean_columns[rows] = column(mean[rows].reshape(1, LANES))
        scale_columns[rows] = column(scale[rows].reshape(1, LANES))
    for half in range(HALVES):
        for start in range(0, ROWS, CHUNK):
            rows = slice(start, start + CHUNK)
            sig = jax.nn.sigmoid(held_gate[rows, lanes(half)].astype(WIDE))
            narrow = (held_value[rows, lanes(half)].astype(WIDE) * sig).astype(NARROW)
            gated[half, rows] = narrow.astype(WIDE)
        for start in range(EDGE, ROWS, EDGE):
            rows = slice(start, start + EDGE)
            conv = convolve(gated, half, taps_wide, start - EDGE, EDGE)
            normed[half, rows] = (conv - mean_columns[rows]) * scale_columns[rows]
    copies[6].wait()
    copies[7].wait()
    upstream[...] = lax.dot_general(
        held[...], held_weight[...], (((1,), (1,)), ((), ())), preferred_element_type=WIDE
    )
    first_upstream[...] = upstream[0:EDGE]
    first_cotangent[...] = held[0:EDGE]
    for half in range(HALVES):
        gain_row = gain[0:1, lanes(half)]
        gain_sum = jnp.zeros((8, LANES), WIDE)
        for start in range(EDGE, ROWS, EDGE):
            rows = slice(start, start + EDGE)
            narrow, own_scaled, own_spread, first, second, part = norm_backward(
                normed[half, rows], scale_columns[rows], gain_row, upstream[rows, lanes(half)]
            )
            hidden[rows, lanes(half)] = narrow.astype(WIDE)
            scaled[half, start - EDGE : start] = own_scaled
            spread[half, start - EDGE : start] = own_spread
            gain_sum = gain_sum + part
            if half == 0:
                sum_first[rows] = first
                sum_second[rows] = second
            else:
                sum_first[rows] = sum_first[rows] + first
                sum_second[rows] = sum_second[rows] + second
        gain_part[half] = gain_sum
    found = [
        column_sums(source[block * LANES : (block + 1) * LANES])
        for source in (sum_first, sum_second)
        for block in range(ROWS // LANES)
    ]
    sums[...] = jnp.concatenate([*found, jnp.zeros((2, LANES), WIDE)], 0)
    turned = jnp.transpose(hidden[...]).astype(NARROW)
    for near in range(CLOSE):
        product[near] = jnp.dot(
            turned, both_blocks(held, place, near), preferred_element_type=WIDE
        )


def head(
    halo, gated, upstream, taps, gain, mean, scale, sums, gain_part,
    scaled, spread, hidden, message, gain_total,
    padded, taps_wide, turned,
):
    taps_wide[0:TAPS] = taps[...].astype(WIDE)
    rows = slice(0, EDGE)
    mean_columns = column(mean[0:LANES].reshape(1, LANES))[rows]
    scale_columns = column(scale[0:LANES].reshape(1, LANES))[rows]
    turned[...] = jnp.zeros((2, LANES, LANES), WIDE)
    for half in range(HALVES):
        padded[half, rows] = halo[:, lanes(half)].astype(WIDE)
        padded[half, EDGE:] = gated[half, rows]
    for half in range(HALVES):
        conv = convolve(padded, half, taps_wide, 0, EDGE)
        normed = (conv - mean_columns) * scale_columns
        narrow, own_scaled, own_spread, first, second, part = norm_backward(
            normed, scale_columns, gain[0:1, lanes(half)], upstream[rows, lanes(half)]
        )
        hidden[:, lanes(half)] = narrow
        scaled[half] = own_scaled
        spread[half] = own_spread
        gain_total[half] = gain_part[half] + part
        turned[0, rows] = turned[0, rows] + first
        turned[1, rows] = turned[1, rows] + second
    blocks = ROWS // LANES
    total = sums[...]
    extra = [column_sums(turned[0]), column_sums(turned[1])]
    none = jnp.zeros((blocks - 1, LANES), WIDE)
    last = jnp.zeros((2, LANES), WIDE)
    total = total + jnp.concatenate([extra[0], none, extra[1], none, last], 0)
    for peer in range(TP):
        message[peer] = total


def head_product(cotangent, hidden, place, near, side):
    columns = both_blocks(cotangent, place, near)[:, side * BLOCK : (side + 1) * BLOCK]
    return lax.dot_general(
        hidden[...], columns, (((0,), (0,)), ((), ())), preferred_element_type=WIDE
    )


def backward(
    place, sums, scaled, spread, first_scaled, first_spread, halo, gated, scale, gain_part,
    first_cotangent, first_hidden, product,
    other, small, extended,
    joint,
):
    for half in range(HALVES):
        joint[half, 0:EDGE] = halo[:, lanes(half)].astype(WIDE)
        joint[half, EDGE:] = gated[half, 0:8]
    total = (sums[0] + sums[1]) + (sums[2] + sums[3])
    total = total * (1.0 / (TP * WIDTH))
    blocks = ROWS // LANES
    for half in range(HALVES):
        extended[half, 0:EDGE] = jnp.zeros((EDGE, LANES), WIDE)
        extended[half, EDGE + ROWS :] = jnp.zeros((EDGE, LANES), WIDE)
    for block in range(blocks):
        rows = slice(block * LANES, (block + 1) * LANES)
        first = column(total[block : block + 1] * scale[rows].reshape(1, LANES))
        second = column(total[blocks + block : blocks + block + 1])
        for half in range(HALVES):
            cut = 0
            if block == 0:
                cut = EDGE
                d_conv = first_scaled[half] - first[0:cut] - first_spread[half] * second[0:cut]
                extended[half, EDGE : EDGE + cut] = d_conv
            rows = slice(block * LANES + cut - EDGE, (block + 1) * LANES - EDGE)
            d_conv = scaled[half, rows] - first[cut:] - spread[half, rows] * second[cut:]
            extended[half, EDGE + block * LANES + cut : EDGE + (block + 1) * LANES] = d_conv
    lead = EDGE - TAPS + 1
    groups = ROWS // 8
    for offset in range(8):
        steps = [q for q in range(5) if 0 <= 8 * q + offset - lead < TAPS]
        found = {(half, q): jnp.zeros((8, LANES), WIDE) for half in range(HALVES) for q in steps}
        loaded = {}
        for m in range(groups + steps[-1]):
            for half in range(HALVES):
                if m < groups:
                    begin = EDGE + 8 * m
                    loaded[half, m] = extended[half, begin : begin + 8]
                begin = 8 * m + offset
                if begin < EDGE:
                    moved = joint[half, begin : begin + 8]
                else:
                    moved = gated[half, begin - EDGE : begin - EDGE + 8]
                for q in steps:
                    if 0 <= m - q < groups:
                        found[half, q] = found[half, q] + loaded[half, m - q] * moved
        for half in range(HALVES):
            for q in steps:
                tap = 8 * q + offset - lead
                small[tap : tap + 1, lanes(half)] = jnp.sum(found[half, q], 0, keepdims=True)
        near = offset
        whole = product[near, :, BLOCK:] + head_product(first_cotangent, first_hidden, place, near, 1)
        other[near * WIDTH : (near + 1) * WIDTH] = whole.astype(NARROW)
    for half in range(HALVES):
        small[TAPS:SMALL, lanes(half)] = jnp.sum(gain_part[half], 0, keepdims=True)
    for half in range(HALVES):
        value = small[:, lanes(half)]
        top = value.astype(NARROW)
        begin = CLOSE * WIDTH + half * 2 * SMALL
        other[begin : begin + SMALL] = top
        other[begin + SMALL : begin + 2 * SMALL] = (value - top.astype(WIDE)).astype(NARROW)


def pack(mine, small, other, pieces):
    for half in range(HALVES):
        begin = CLOSE * WIDTH + half * 2 * SMALL
        top = other[begin : begin + SMALL].astype(WIDE)
        rest = other[begin + SMALL : begin + 2 * SMALL].astype(WIDE)
        both = (small[:, lanes(half)] + (top + rest)).astype(NARROW)
        for near in range(CLOSE):
            pieces[near, WIDTH + half * SMALL : WIDTH + (half + 1) * SMALL] = both
    for near in range(CLOSE):
        for start in range(0, WIDTH, 64):
            rows = slice(start, start + 64)
            there = other[near * WIDTH + start : near * WIDTH + start + 64].astype(WIDE)
            pieces[near, rows] = (mine[near, rows] + there).astype(NARROW)


def gated_gradient(
    place, extended, taps, value, gate, first_cotangent, first_hidden, product,
    value_grad, gate_grad, margin, last, mine,
    taps_wide, held_value_grad, held_gate_grad, departures,
):
    taps_wide[0:TAPS] = taps[...].astype(WIDE)
    parts = []
    for start in range(0, EDGE + ROWS, EDGE):
        rows = slice(start - EDGE, start)
        for half in range(HALVES):
            found = jnp.zeros((EDGE, LANES), WIDE)
            for tap in range(TAPS):
                begin = start + TAPS - 1 - tap
                found = found + taps_wide[tap : tap + 1, lanes(half)] * extended[half, begin : begin + EDGE]
            if start == 0:
                margin[half] = found
                continue
            sig = jax.nn.sigmoid(gate[rows, lanes(half)].astype(WIDE))
            slope = value[rows, lanes(half)].astype(WIDE) * sig * (1.0 - sig)
            if start == ROWS:
                last[0, half], last[1, half], last[2, half] = found, sig, slope
            else:
                held_value_grad[rows, lanes(half)] = (found * sig).astype(NARROW)
                held_gate_grad[rows, lanes(half)] = (found * slope).astype(NARROW)
        if start in PART_ENDS:
            part = PART_ENDS.index(start)
            begin = PART_ENDS[part - 1] if part else 0
            sent = pl.ds(begin, start - begin)
            for i, (source, target) in enumerate(
                ((held_value_grad, value_grad), (held_gate_grad, gate_grad))
            ):
                parts.append(
                    pltpu.make_async_copy(
                        source.at[sent], target.at[sent], departures.at[2 * part + i]
                    )
                )
                parts[-1].start()
    for near in range(CLOSE):
        mine[near] = product[near, :, 0:BLOCK] + head_product(
            first_cotangent, first_hidden, place, near, 0
        )
    for part in parts:
        part.wait()


def fold_near(arrived, payload):
    for start in range(0, WIDTH + 2 * SMALL, 64):
        rows = slice(start, start + 64)
        total = arrived[0, rows].astype(WIDE)
        for near in range(1, CLOSE):
            total = total + arrived[near, rows].astype(WIDE)
        payload[rows] = total.astype(NARROW)


def hand_out(payload, message):
    weights = jnp.transpose(payload[0:WIDTH].astype(WIDE)).astype(NARROW)
    small = jnp.concatenate([payload[WIDTH : WIDTH + SMALL], payload[WIDTH + SMALL :]], 1)
    for position, member in enumerate(GATHER_ORDER):
        message[position, 0:OWN] = weights[member * OWN : (member + 1) * OWN]
        message[position, OWN:] = small


def totals(arrived, total):
    for start in range(0, OWN + SMALL, 8):
        rows = slice(start, start + 8)
        found = arrived[0, rows].astype(WIDE)
        for position in range(1, 2 * CLOSE):
            found = found + arrived[position, rows].astype(WIDE)
        total[rows] = found


def finish(
    value_part, gate_part, total, last, late,
    value_grad, gate_grad, weight_grad, taps_grad, gain_grad,
    held_value_grad, held_gate_grad, departures,
):
    del value_part, gate_part
    for half in range(HALVES):
        grad = last[0, half] + late[half]
        held_value_grad[:, lanes(half)] = (grad * last[1, half]).astype(NARROW)
        held_gate_grad[:, lanes(half)] = (grad * last[2, half]).astype(NARROW)
    rows = pl.ds(ROWS - EDGE, EDGE)
    copies = [
        pltpu.make_async_copy(held_value_grad, value_grad.at[rows], departures.at[0]),
        pltpu.make_async_copy(held_gate_grad, gate_grad.at[rows], departures.at[1]),
    ]
    for copy in copies:
        copy.start()
    weight_grad[...] = total[0:OWN]
    taps_grad[...] = total[OWN : OWN + TAPS]
    gain_grad[...] = total[OWN + TAPS :]
    for copy in copies:
        copy.wait()


def to_block(value):
    pairs = []
    for far in range(FAR):
        for near in range(CLOSE):
            for core in range(2):
                target = (far + OFFSETS[core][near]) % FAR
                pairs.append(((far * CLOSE + near) * 2 + core, (target * CLOSE + near) * 2 + core))
    return lax.ppermute(value, SP, pairs)


def shards(
    proj_value, proj_gate, out_cotangent, out_weight, conv_taps, norm_gain, row_mean, row_scale
):
    end_gate = jax.nn.sigmoid(proj_gate[ROWS - EDGE :].astype(WIDE))
    end = (proj_value[ROWS - EDGE :].astype(WIDE) * end_gate).astype(NARROW)
    halo = shifted(end, SP, 1)
    split = (HALVES, ROWS, LANES)
    rest = (HALVES, ROWS - EDGE, LANES)
    row_gain = norm_gain.reshape(1, WIDTH)
    sides = pltpu.VMEM((HALVES, EDGE + ROWS, LANES), WIDE)
    taps_scratch = pltpu.VMEM((TAPS + 1, WIDTH), WIDE)
    place = lax.axis_index(SP).reshape(1)
    narrow = ((ROWS, WIDTH), NARROW)
    gated, scaled, spread, sums, gain_part, first_upstream, first_cotangent, product = (
        scalar_call(
            forward,
            [
                (split, WIDE), (rest, WIDE), (rest, WIDE), ((8, LANES), WIDE),
                ((HALVES, 8, LANES), WIDE), ((EDGE, WIDTH), WIDE), ((EDGE, MODEL), NARROW),
                ((CLOSE, WIDTH, 2 * BLOCK), WIDE),
            ],
            place, proj_value, proj_gate, out_cotangent, out_weight,
            conv_taps, row_gain, row_mean, row_scale, in_hbm=8,
            scratch=[
                pltpu.VMEM(*narrow), pltpu.VMEM(*narrow), pltpu.VMEM((ROWS, MODEL), NARROW),
                pltpu.VMEM((WIDTH, MODEL), NARROW), pltpu.VMEM((TAPS, WIDTH), NARROW),
                pltpu.VMEM((1, WIDTH), WIDE), pltpu.VMEM((ROWS,), WIDE),
                pltpu.VMEM((ROWS,), WIDE), pltpu.SemaphoreType.DMA((8,)),
                taps_scratch, *([pltpu.VMEM((ROWS, LANES), WIDE)] * 4),
                pltpu.VMEM((ROWS, WIDTH), WIDE), pltpu.VMEM(split, WIDE),
                pltpu.VMEM((ROWS, WIDTH), WIDE),
            ],
            flops=4 * ROWS * WIDTH * MODEL, limit=12,
        )
    )
    edge = (HALVES, EDGE, LANES)
    first_scaled, first_spread, first_hidden, message, gain_part = call_with(
        head,
        [
            (edge, WIDE), (edge, WIDE), ((EDGE, WIDTH), NARROW),
            ((TP, 8, LANES), WIDE), ((HALVES, 8, LANES), WIDE),
        ],
        [
            pltpu.VMEM((HALVES, 2 * EDGE, LANES), WIDE),
            taps_scratch,
            pltpu.VMEM((2, LANES, LANES), WIDE),
        ],
        halo, gated, first_upstream, conv_taps, row_gain, row_mean, row_scale, sums,
        gain_part, flops=10 * ROWS * WIDTH,
    )
    sums = exchange(message, "tp", SUMS_ORDER)
    rows = CLOSE * WIDTH + 4 * SMALL
    other, small, extended = scalar_call(
        backward,
        [
            ((rows, BLOCK), NARROW), ((SMALL, WIDTH), WIDE),
            ((HALVES, ROWS + 2 * EDGE, LANES), WIDE),
        ],
        place, sums, scaled, spread, first_scaled, first_spread, halo, gated, row_scale,
        gain_part, first_cotangent, first_hidden, product,
        scratch=[pltpu.VMEM((HALVES, EDGE + 8, LANES), WIDE)], flops=100 * ROWS * WIDTH,
    )
    other = lax.ppermute(other, "c", [(0, 1), (1, 0)])
    value_grad, gate_grad, margin, last, mine = scalar_call(
        gated_gradient,
        [
            narrow, narrow, (edge, WIDE), ((3, *edge), WIDE),
            ((CLOSE, WIDTH, BLOCK), WIDE),
        ],
        place, extended, conv_taps, proj_value, proj_gate,
        first_cotangent, first_hidden, product, outs_in_hbm=2,
        scratch=[
            taps_scratch, pltpu.VMEM(*narrow), pltpu.VMEM(*narrow),
            pltpu.SemaphoreType.DMA((2 * len(PART_ENDS),)),
        ],
        flops=100 * ROWS * WIDTH,
    )
    (pieces,) = call(
        pack, [((CLOSE, WIDTH + 2 * SMALL, BLOCK), NARROW)], mine, small, other, flops=1 << 20
    )
    arrived = exchange(pieces, NEAR)
    (payload,) = call(
        fold_near, [((WIDTH + 2 * SMALL, BLOCK), NARROW)], arrived, flops=1 << 20
    )
    payload = to_block(payload)
    late = shifted(margin, SP, -1)
    (message,) = call(hand_out, [((2 * CLOSE, OWN + SMALL, WIDTH), NARROW)], payload, flops=1 << 16)
    arrived = exchange(message, (*NEAR, "c"), GATHER_ORDER)
    (total,) = call(totals, [((OWN + SMALL, WIDTH), WIDE)], arrived, flops=1 << 20)
    value_grad, gate_grad, weight_grad, taps_grad, gain_grad = last_call(
        [narrow, narrow, ((OWN, WIDTH), WIDE), ((TAPS, WIDTH), WIDE), ((1, WIDTH), WIDE)],
        value_grad, gate_grad, total, last, late,
    )
    return (value_grad, gate_grad, weight_grad, taps_grad, gain_grad.reshape(WIDTH))


def call_with(body, outs, scratch, *args, flops=0, limit=6):
    shapes = [jax.ShapeDtypeStruct(shape, dtype) for shape, dtype in outs]
    size = sum(a.size * a.dtype.itemsize for a in (*args, *shapes))
    return pl.pallas_call(
        body,
        out_shape=shapes,
        scratch_shapes=scratch,
        compiler_params=pltpu.CompilerParams(vmem_limit_bytes=limit << 20),
        cost_estimate=pl.CostEstimate(flops=flops, bytes_accessed=size, transcendentals=0),
    )(*args)


def scalar_call(
    body, outs, scalar, *args, scratch=(), flops=1 << 20, limit=6, in_hbm=0, outs_in_hbm=0
):
    shapes = [jax.ShapeDtypeStruct(shape, dtype) for shape, dtype in outs]
    placed = [pltpu.HBM(*out) for out in outs[:outs_in_hbm]] + shapes[outs_in_hbm:]
    size = sum(a.size * a.dtype.itemsize for a in (*args, *shapes))
    whole = pl.BlockSpec(memory_space=pltpu.VMEM)
    far = [pltpu.with_memory_space_constraint(a, pltpu.HBM) for a in args[:in_hbm]]
    return pl.pallas_call(
        body,
        out_shape=placed,
        in_specs=[
            pl.BlockSpec(memory_space=pltpu.SMEM),
            *([pl.BlockSpec(memory_space=pltpu.HBM)] * in_hbm),
            *([whole] * (len(args) - in_hbm)),
        ],
        out_specs=[
            *([pl.BlockSpec(memory_space=pltpu.HBM)] * outs_in_hbm),
            *([whole] * (len(shapes) - outs_in_hbm)),
        ],
        scratch_shapes=scratch,
        compiler_params=pltpu.CompilerParams(vmem_limit_bytes=limit << 20),
        cost_estimate=pl.CostEstimate(flops=flops, bytes_accessed=size, transcendentals=0),
    )(scalar, *far, *args[in_hbm:])


def last_call(outs, *args):
    shapes = [jax.ShapeDtypeStruct(shape, dtype) for shape, dtype in outs]
    far, whole = pl.BlockSpec(memory_space=pltpu.HBM), pl.BlockSpec(memory_space=pltpu.VMEM)
    edge = pltpu.VMEM((EDGE, WIDTH), NARROW)
    held = [pltpu.with_memory_space_constraint(a, pltpu.HBM) for a in args[:2]]
    return pl.pallas_call(
        finish,
        out_shape=[*(pltpu.HBM(*out) for out in outs[:2]), *shapes[2:]],
        in_specs=[far, far, whole, whole, whole],
        out_specs=[far, far, whole, whole, whole],
        scratch_shapes=[edge, edge, pltpu.SemaphoreType.DMA((2,))],
        input_output_aliases={0: 0, 1: 1},
        compiler_params=pltpu.CompilerParams(vmem_limit_bytes=6 << 20),
        cost_estimate=pl.CostEstimate(flops=1 << 16, bytes_accessed=1 << 18, transcendentals=0),
        name="finish",
    )(*held, *args[2:])


def solution(mesh):
    sizes = [size for _, size in AXES]
    split = Mesh(mesh.devices.reshape(*sizes, mesh.shape["tp"]), (*SP, "tp"))
    placed = (
        P(SP, "tp"),
        P(SP, "tp"),
        P(SP, None),
        P("tp", None),
        P(None, "tp"),
        P("tp"),
        P(SP),
        P(SP),
    )
    return jax.shard_map(
        shards,
        mesh=split,
        in_specs=placed,
        out_specs=(P(SP, "tp"), P(SP, "tp"), P(SP, "tp"), P(None, "tp"), P("tp")),
        check_vma=False,
    )
```

profile of v0, /device:TPU:7, one launch (start us, length us, event | category | flops | bytes accessed | tf_op | source)
XLA Modules:
  0.0 82.3 jit_solution(3264287964200932396)
XLA Ops:
  0.6 0.0 copy-start.3
  0.6 0.0 copy-start.2
  0.7 0.0 copy-start.4
  0.7 0.0 copy-start.5
  0.7 0.8 multiply_convert_fusion
  1.5 4.0 %collective-permute-start = (bf16[32,256]{1,0:T(8,128)(2,1)S(1)}, bf16[32,256]{1,0:T(8,128)(2,1)S(1)}, u32[]{:S(2)}, u32[]{:S(2)}) collective-permute-start(bf16[32,256]{1,0:T(8,128)(2,1)S(1)} %multiply_convert_fusion), channel_id=1, source_target_pairs={{0,4},{4,8},{8,12},{12,16},{16,20},{20,24},{24,28},{28,32},{32,36}... | collective-permute-start | bytes 49160 | tf_op jit(solution)/shard_map/ppermute | solution.py:38
  5.5 3.4 %shard_map.119 = (f32[2,384,128]{2,1,0:T(8,128)S(1)}, f32[2,352,128]{2,1,0:T(8,128)S(1)}, f32[2,352,128]{2,1,0:T(8,128)S(1)}, f32[8,128]{1,0:T(8,128)S(1)}, f32[...) custom-call(s32[1]{0:T(128)} %bitcast.place, ...), custom_call_target="tpu_custom_call" | custom-call | flops 805306368 | bytes 6422016 | tf_op jit(solution)/shard_map/pallas_call | solution.py:515
  8.9 0.0 copy-start
  8.9 0.0 copy-start.1
  8.9 0.0 collective-permute-done.halo
  8.9 0.0 copy-done.3
  8.9 0.0 copy-done.2
  8.9 0.0 copy-done.4
  9.0 0.0 copy-done.5
  9.0 0.2 shard_map.120
  9.2 7.5 %all_to_all.15.sums = f32[4,8,128]{2,1,0:T(8,128)S(1)} all-to-all(f32[4,8,128]{2,1,0:T(8,128)S(1)} %get-tuple-element.35), channel_id=1, replica_groups={{3,0,1,2},{7,4,5,6},{11,8,9,10},{15,12,13,14},{19,16,17,18},{23,20,21,2..., dimensions={0} | all-to-all | bytes 32768 | tf_op jit(solution)/shard_map/all_to_all | solution.py:43
  16.7 1.6 %shard_map.121 = (bf16[2176,128]{1,0:T(8,128)(2,1)S(1)}, f32[32,256]{1,0:T(8,128)S(1)}, f32[2,448,128]{2,1,0:T(8,128)S(1)}) custom-call(s32[1]{0:T(128)} %bitcast.place, f32[4,8,128]{2,1,0:T(8,128)S(1)} %all_to_all.15.sums, f32[2,352,128]{2,1,0:T(8,128)S(1)} %get-tuple-element.36.scaled, f32[2,352,128]{2,1,0:T(8,128)S(1)} %get-tuple-element.37.spread, ...), custom_call_target="tpu_custom_call" | custom-call | flops 9830400 | bytes 4515328 | tf_op jit(solution)/shard_map/pallas_call | solution.py:515
  18.3 1.9 %collective-permute-start.1 = (bf16[2176,128]{1,0:T(8,128)(2,1)S(1)}, bf16[2176,128]{1,0:T(8,128)(2,1)S(1)}, u32[]{:S(2)}, u32[]{:S(2)}) collective-permute-start(bf16[2176,128]{1,0:T(8,128)(2,1)S(1)} %get-tuple-element.49), channel_id=1, source_target_pairs={{0,4},{4,0},{1,5},{5,1},{2,6},{6,2},{3,7},{7,3},{8,12},{12,8},{9,1... | collective-permute-start | bytes 1671176 | tf_op jit(solution)/shard_map/ppermute | solution.py:461
  20.2 0.0 copy-done
  20.3 0.0 copy-done.1
  20.3 2.1 %shard_map.122 = (bf16[384,256]{1,0:T(8,128)(2,1)}, bf16[384,256]{1,0:T(8,128)(2,1)}, f32[2,32,128]{2,1,0:T(8,128)S(1)}, f32[3,2,32,128]{3,2,1,0:T(8,128)S(1)}, f32[8,256,128]{2,1,0:T(8,128)S(1)}) custom-call(s32[1]{0:T(128)} %bitcast.place, f32[2,448,128]{2,1,0:T(8,128)S(1)} %get-tuple-element.44.extended, bf16[31,256]{1,0:T(8,128)(2,1)S(1)} %copy-done.2, ...), custom_call_target="tpu_custom_call" | custom-call | flops 9830400 | bytes 4685312 | tf_op jit(solution)/shard_map/pallas_call | solution.py:515
  22.3 0.0 collective-permute-done.1.other
  22.3 0.1 shard_map.123
  22.4 22.4 %all_to_all.16.arrived = bf16[8,320,128]{2,1,0:T(8,128)(2,1)S(1)} all-to-all(bf16[8,320,128]{2,1,0:T(8,128)(2,1)S(1)} %shard_map.123), channel_id=1, replica_groups=mesh['zh'=16,'zl'=2,'x'=4,'c'=2,'tp'=4] {'zl','x'}, dimensions={0} | all-to-all | bytes 1310720 | tf_op jit(solution)/shard_map/all_to_all | solution.py:43
  44.8 0.1 shard_map.124
  44.9 10.7 %collective-permute-start.2 = (bf16[320,128]{1,0:T(8,128)(2,1)S(1)}, bf16[320,128]{1,0:T(8,128)(2,1)S(1)}, u32[]{:S(2)}, u32[]{:S(2)}) collective-permute-start(bf16[320,128]{1,0:T(8,128)(2,1)S(1)} %shard_map.124), channel_id=1, source_target_pairs={{0,0},{4,388},{8,968},{12,460},{16,912},{20,532},{24,856},{28,348}... | collective-permute-start | bytes 245768 | tf_op jit(solution)/shard_map/ppermute | solution.py:396
  55.6 6.7 %collective-permute-done.2.payload = bf16[320,128]{1,0:T(8,128)(2,1)S(1)} collective-permute-done((bf16[320,128]{1,0:T(8,128)(2,1)S(1)}, bf16[320,128]{1,0:T(8,128)(2,1)S(1)}, u32[]{:S(2)}, u32[]{:S(2)}) %collective-permute-start.2) | collective-permute-done | bytes 81952 | tf_op jit(solution)/shard_map/ppermute | solution.py:396
  62.3 0.8 %shard_map.125 = bf16[16,40,256]{2,1,0:T(8,128)(2,1)} custom-call(bf16[320,128]{1,0:T(8,128)(2,1)S(1)} %collective-permute-done.2.payload), custom_call_target="tpu_custom_call" | custom-call | flops 65536 | bytes 409600 | tf_op jit(solution)/shard_map/pallas_call | solution.py:57
  63.2 10.6 %all-to-all-start.2 = ((bf16[16,40,256]{2,1,0:T(8,128)(2,1)}), bf16[16,40,256]{2,1,0:T(8,128)(2,1)S(1)}, u32[]{:S(2)}, u32[]{:S(2)}) async-start(bf16[16,40,256]{2,1,0:T(8,128)(2,1)} %shard_map.125), calls=%async_computation.2 | async-start | bytes 655360 | tf_op jit(solution)/shard_map/all_to_all | solution.py:43
  73.7 2.3 %collective-permute-start.3 = (f32[2,32,128]{2,1,0:T(8,128)S(1)}, f32[2,32,128]{2,1,0:T(8,128)S(1)}, u32[]{:S(2)}, u32[]{:S(2)}) collective-permute-start(f32[2,32,128]{2,1,0:T(8,128)S(1)} %get-tuple-element.51), channel_id=1, source_target_pairs={{4,0},{8,4},{12,8},{16,12},{20,16},{24,20},{28,24},{32,28},{36,32}... | collective-permute-start | bytes 98312 | tf_op jit(solution)/shard_map/ppermute | solution.py:38
  76.0 4.4 %all-to-all-done.2.arrived = bf16[16,40,256]{2,1,0:T(8,128)(2,1)S(1)} async-done(((bf16[16,40,256]{2,1,0:T(8,128)(2,1)}), bf16[16,40,256]{2,1,0:T(8,128)(2,1)S(1)}, u32[]{:S(2)}, u32[]{:S(2)}) %all-to-all-start.2) | async-done | bytes 327712 | tf_op jit(solution)/shard_map/all_to_all | solution.py:43
  80.5 0.5 collective-permute-done.3.late
  81.1 1.3 %finish.1 = (bf16[384,256]{1,0:T(8,128)(2,1)}, bf16[384,256]{1,0:T(8,128)(2,1)}, f32[8,256]{1,0:T(8,128)}, f32[31,256]{1,0:T(8,128)}, f32[1,256]{1,0:T(1,128)}) custom-call(bf16[384,256]{1,0:T(8,128)(2,1)} %get-tuple-element.45.value_part, bf16[384,256]{1,0:T(8,128)(2,1)} %get-tuple-element.46.gate_part, ...), custom_call_target="tpu_custom_call", output_to_operand_aliasing={{0}: (0, {}), {1}: (1, {})} | custom-call | flops 65536 | bytes 262144 | tf_op jit(solution)/shard_map/finish/pallas_call | solution.py:538
  (1 shorter events, 0.0 us)
Async XLA Ops:
  0.6 8.3 %copy-start.3 = (f32[384]{0:T(512)S(1)}, f32[384]{0:T(512)}, u32[]{:S(2)}) copy-start(f32[384]{0:T(512)} %scale.3) | copy-start | bytes 4612
  0.6 8.3 %copy-start.2 = (bf16[31,256]{1,0:T(8,128)(2,1)S(1)}, bf16[31,256]{1,0:T(8,128)(2,1)}, u32[]{:S(2)}) copy-start(bf16[31,256]{1,0:T(8,128)(2,1)} %taps.3) | copy-start | bytes 47620
  0.7 8.3 %copy-start.4 = (f32[384]{0:T(512)S(1)}, f32[384]{0:T(512)}, u32[]{:S(2)}) copy-start(f32[384]{0:T(512)} %mean.1) | copy-start | bytes 4612
  0.7 8.3 %copy-start.5 = (f32[256]{0:T(256)S(1)}, f32[256]{0:T(256)}, u32[]{:S(2)}) copy-start(f32[256]{0:T(256)} %param.13) | copy-start | bytes 3076
  1.5 7.5 %collective-permute-start = (bf16[32,256]{1,0:T(8,128)(2,1)S(1)}, bf16[32,256]{1,0:T(8,128)(2,1)S(1)}, u32[]{:S(2)}, u32[]{:S(2)}) collective-permute-start(bf16[32,256]{1,0:T(8,128)(2,1)S(1)} %multiply_convert_fusion), channel_id=1, source_target_pairs={{0,4},{4,8},{8,12},{12,16},{16,20},{20,24},{24,28},{28,32},{32,36}... | collective-permute-start | bytes 49160 | tf_op jit(solution)/shard_map/ppermute | solution.py:38
  8.9 11.4 %copy-start = (bf16[384,256]{1,0:T(8,128)(2,1)S(1)}, bf16[384,256]{1,0:T(8,128)(2,1)}, u32[]{:S(2)}) copy-start(bf16[384,256]{1,0:T(8,128)(2,1)} %gate.3) | copy-start | bytes 589828
  8.9 11.4 %copy-start.1 = (bf16[384,256]{1,0:T(8,128)(2,1)S(1)}, bf16[384,256]{1,0:T(8,128)(2,1)}, u32[]{:S(2)}) copy-start(bf16[384,256]{1,0:T(8,128)(2,1)} %value.3) | copy-start | bytes 589828
  18.3 4.0 %collective-permute-start.1 = (bf16[2176,128]{1,0:T(8,128)(2,1)S(1)}, bf16[2176,128]{1,0:T(8,128)(2,1)S(1)}, u32[]{:S(2)}, u32[]{:S(2)}) collective-permute-start(bf16[2176,128]{1,0:T(8,128)(2,1)S(1)} %get-tuple-element.49), channel_id=1, source_target_pairs={{0,4},{4,0},{1,5},{5,1},{2,6},{6,2},{3,7},{7,3},{8,12},{12,8},{9,1... | collective-permute-start | bytes 1671176 | tf_op jit(solution)/shard_map/ppermute | solution.py:461
  44.9 17.4 %collective-permute-start.2 = (bf16[320,128]{1,0:T(8,128)(2,1)S(1)}, bf16[320,128]{1,0:T(8,128)(2,1)S(1)}, u32[]{:S(2)}, u32[]{:S(2)}) collective-permute-start(bf16[320,128]{1,0:T(8,128)(2,1)S(1)} %shard_map.124), channel_id=1, source_target_pairs={{0,0},{4,388},{8,968},{12,460},{16,912},{20,532},{24,856},{28,348}... | collective-permute-start | bytes 245768 | tf_op jit(solution)/shard_map/ppermute | solution.py:396
  63.2 17.3 %all-to-all-start.2 = ((bf16[16,40,256]{2,1,0:T(8,128)(2,1)}), bf16[16,40,256]{2,1,0:T(8,128)(2,1)S(1)}, u32[]{:S(2)}, u32[]{:S(2)}) async-start(bf16[16,40,256]{2,1,0:T(8,128)(2,1)} %shard_map.125), calls=%async_computation.2 | async-start | bytes 655360 | tf_op jit(solution)/shard_map/all_to_all | solution.py:43
  73.7 7.3 %collective-permute-start.3 = (f32[2,32,128]{2,1,0:T(8,128)S(1)}, f32[2,32,128]{2,1,0:T(8,128)S(1)}, u32[]{:S(2)}, u32[]{:S(2)}) collective-permute-start(f32[2,32,128]{2,1,0:T(8,128)S(1)} %get-tuple-element.51), channel_id=1, source_target_pairs={{4,0},{8,4},{12,8},{16,12},{20,16},{24,20},{28,24},{32,28},{36,32}... | collective-permute-start | bytes 98312 | tf_op jit(solution)/shard_map/ppermute | solution.py:38
where the time goes:
time: 83.9 us; the launch traced here: 82.3 us
  blocking collectives  29.9 us (36%)
  starting transfers between devices  29.5 us (35%)
  waiting for transfers between devices  11.7 us (14%)
  Pallas kernels  9.59 us (11%)
    all_to_all x2, blocking collectives, exchange(): lax.all_to_all(pieces, axes, 0, 0, tiled=True, axis_index_groups=groups)  29.9 us
    ppermute x1, starting transfers between devices, to_block(): return lax.ppermute(value, SP, pairs)  10.7 us
    all_to_all x1, starting transfers between devices, exchange(): lax.all_to_all(pieces, axes, 0, 0, tiled=True, axis_index_groups=groups)  10.6 us
    pallas_call x3, Pallas kernels, scalar_call(): pl.pallas_call(body, out_shape=placed, in_specs=[pl.BlockSpec(memory_spac...  7.07 us
    ppermute x1, waiting for transfers between devices, to_block(): return lax.ppermute(value, SP, pairs)  6.72 us
    ppermute x2, starting transfers between devices, shifted(): lax.ppermute(value, axis, [(source, source + steps) for source in range(f...  6.31 us
    all_to_all x1, waiting for transfers between devices, exchange(): lax.all_to_all(pieces, axes, 0, 0, tiled=True, axis_index_groups=groups)  4.45 us
    ppermute x1, starting transfers between devices, shards(): other = lax.ppermute(other, 'c', [(0, 1), (1, 0)])  1.92 us
  transfers between devices with their start and end apart: 5, of which 3 were waited for; matrix products, arithmetic and copies ran while one was open for 0% of the time, Pallas kernels for 7%

commit v1 on v0

--- a/solution.py
+++ b/solution.py
@@ -26,7 +26,6 @@
 WIDTH = HALVES * LANES
 MODEL = 2048
 OWN = 8
-PART_ENDS = (128, 256, 352)
 CHUNK = 64
 WIDE = jnp.float32
 NARROW = jnp.bfloat16
@@ -97,7 +96,7 @@
     place, value, gate, cotangent, weight, far_taps, far_gain, far_mean, far_scale,
     gated, scaled, spread, sums, gain_part, first_upstream, first_cotangent, product,
     held_value, held_gate, held, held_weight, taps, gain, mean, scale, arrivals,
-    taps_wide, mean_columns, scale_columns, sum_first, sum_second,
+    padded, taps_wide, mean_columns, scale_columns, sum_first, sum_second,
     hidden, normed, upstream,
 ):
     copies = [
@@ -126,10 +125,11 @@
             rows = slice(start, start + CHUNK)
             sig = jax.nn.sigmoid(held_gate[rows, lanes(half)].astype(WIDE))
             narrow = (held_value[rows, lanes(half)].astype(WIDE) * sig).astype(NARROW)
-            gated[half, rows] = narrow.astype(WIDE)
+            gated[rows, lanes(half)] = narrow
+            padded[half, EDGE + start : EDGE + start + CHUNK] = narrow.astype(WIDE)
         for start in range(EDGE, ROWS, EDGE):
             rows = slice(start, start + EDGE)
-            conv = convolve(gated, half, taps_wide, start - EDGE, EDGE)
+            conv = convolve(padded, half, taps_wide, start, EDGE)
             normed[half, rows] = (conv - mean_columns[rows]) * scale_columns[rows]
     copies[6].wait()
     copies[7].wait()
@@ -182,7 +182,7 @@
     turned[...] = jnp.zeros((2, LANES, LANES), WIDE)
     for half in range(HALVES):
         padded[half, rows] = halo[:, lanes(half)].astype(WIDE)
-        padded[half, EDGE:] = gated[half, rows]
+        padded[half, EDGE:] = gated[rows, lanes(half)].astype(WIDE)
     for half in range(HALVES):
         conv = convolve(padded, half, taps_wide, 0, EDGE)
         normed = (conv - mean_columns) * scale_columns
@@ -205,22 +205,15 @@
         message[peer] = total
 
 
-def head_product(cotangent, hidden, place, near, side):
-    columns = both_blocks(cotangent, place, near)[:, side * BLOCK : (side + 1) * BLOCK]
-    return lax.dot_general(
-        hidden[...], columns, (((0,), (0,)), ((), ())), preferred_element_type=WIDE
-    )
-
-
 def backward(
     place, sums, scaled, spread, first_scaled, first_spread, halo, gated, scale, gain_part,
     first_cotangent, first_hidden, product,
-    other, small, extended,
-    joint,
-):
-    for half in range(HALVES):
-        joint[half, 0:EDGE] = halo[:, lanes(half)].astype(WIDE)
-        joint[half, EDGE:] = gated[half, 0:8]
+    mine, other, small, extended,
+    padded,
+):
+    for half in range(HALVES):
+        padded[half, 0:EDGE] = halo[:, lanes(half)].astype(WIDE)
+        padded[half, EDGE:] = gated[:, lanes(half)].astype(WIDE)
     total = (sums[0] + sums[1]) + (sums[2] + sums[3])
     total = total * (1.0 / (TP * WIDTH))
     blocks = ROWS // LANES
@@ -251,11 +244,7 @@
                 if m < groups:
                     begin = EDGE + 8 * m
                     loaded[half, m] = extended[half, begin : begin + 8]
-                begin = 8 * m + offset
-                if begin < EDGE:
-                    moved = joint[half, begin : begin + 8]
-                else:
-                    moved = gated[half, begin - EDGE : begin - EDGE + 8]
+                moved = padded[half, 8 * m + offset : 8 * m + offset + 8]
                 for q in steps:
                     if 0 <= m - q < groups:
                         found[half, q] = found[half, q] + loaded[half, m - q] * moved
@@ -264,8 +253,12 @@
                 tap = 8 * q + offset - lead
                 small[tap : tap + 1, lanes(half)] = jnp.sum(found[half, q], 0, keepdims=True)
         near = offset
-        whole = product[near, :, BLOCK:] + head_product(first_cotangent, first_hidden, place, near, 1)
-        other[near * WIDTH : (near + 1) * WIDTH] = whole.astype(NARROW)
+        whole = product[near] + lax.dot_general(
+            first_hidden[...], both_blocks(first_cotangent, place, near),
+            (((0,), (0,)), ((), ())), preferred_element_type=WIDE,
+        )
+        mine[near] = whole[:, 0:BLOCK]
+        other[near * WIDTH : (near + 1) * WIDTH] = whole[:, BLOCK:].astype(NARROW)
     for half in range(HALVES):
         small[TAPS:SMALL, lanes(half)] = jnp.sum(gain_part[half], 0, keepdims=True)
     for half in range(HALVES):
@@ -291,49 +284,18 @@
             pieces[near, rows] = (mine[near, rows] + there).astype(NARROW)
 
 
-def gated_gradient(
-    place, extended, taps, value, gate, first_cotangent, first_hidden, product,
-    value_grad, gate_grad, margin, last, mine,
-    taps_wide, held_value_grad, held_gate_grad, departures,
-):
+def gated_gradient(extended, taps, d_gated, margin, taps_wide):
     taps_wide[0:TAPS] = taps[...].astype(WIDE)
-    parts = []
-    for start in range(0, EDGE + ROWS, EDGE):
-        rows = slice(start - EDGE, start)
-        for half in range(HALVES):
+    for half in range(HALVES):
+        for start in range(0, EDGE + ROWS, EDGE):
             found = jnp.zeros((EDGE, LANES), WIDE)
             for tap in range(TAPS):
                 begin = start + TAPS - 1 - tap
                 found = found + taps_wide[tap : tap + 1, lanes(half)] * extended[half, begin : begin + EDGE]
             if start == 0:
                 margin[half] = found
-                continue
-            sig = jax.nn.sigmoid(gate[rows, lanes(half)].astype(WIDE))
-            slope = value[rows, lanes(half)].astype(WIDE) * sig * (1.0 - sig)
-            if start == ROWS:
-                last[0, half], last[1, half], last[2, half] = found, sig, slope
             else:
-                held_value_grad[rows, lanes(half)] = (found * sig).astype(NARROW)
-                held_gate_grad[rows, lanes(half)] = (found * slope).astype(NARROW)
-        if start in PART_ENDS:
-            part = PART_ENDS.index(start)
-            begin = PART_ENDS[part - 1] if part else 0
-            sent = pl.ds(begin, start - begin)
-            for i, (source, target) in enumerate(
-                ((held_value_grad, value_grad), (held_gate_grad, gate_grad))
-            ):
-                parts.append(
-                    pltpu.make_async_copy(
-                        source.at[sent], target.at[sent], departures.at[2 * part + i]
-                    )
-                )
-                parts[-1].start()
-    for near in range(CLOSE):
-        mine[near] = product[near, :, 0:BLOCK] + head_product(
-            first_cotangent, first_hidden, place, near, 0
-        )
-    for part in parts:
-        part.wait()
+                d_gated[half, start - EDGE : start] = found
 
 
 def fold_near(arrived, payload):
@@ -363,27 +325,22 @@
 
 
 def finish(
-    value_part, gate_part, total, last, late,
+    total, d_gated, late, value, gate,
     value_grad, gate_grad, weight_grad, taps_grad, gain_grad,
-    held_value_grad, held_gate_grad, departures,
-):
-    del value_part, gate_part
-    for half in range(HALVES):
-        grad = last[0, half] + late[half]
-        held_value_grad[:, lanes(half)] = (grad * last[1, half]).astype(NARROW)
-        held_gate_grad[:, lanes(half)] = (grad * last[2, half]).astype(NARROW)
-    rows = pl.ds(ROWS - EDGE, EDGE)
-    copies = [
-        pltpu.make_async_copy(held_value_grad, value_grad.at[rows], departures.at[0]),
-        pltpu.make_async_copy(held_gate_grad, gate_grad.at[rows], departures.at[1]),
-    ]
-    for copy in copies:
-        copy.start()
+):
+    for half in range(HALVES):
+        for start in range(0, ROWS, EDGE):
+            rows = slice(start, start + EDGE)
+            grad = d_gated[half, rows]
+            if start == ROWS - EDGE:
+                grad = grad + late[half]
+            sig = jax.nn.sigmoid(gate[rows, lanes(half)].astype(WIDE))
+            wide = value[rows, lanes(half)].astype(WIDE)
+            value_grad[rows, lanes(half)] = (grad * sig).astype(NARROW)
+            gate_grad[rows, lanes(half)] = (grad * wide * sig * (1.0 - sig)).astype(NARROW)
     weight_grad[...] = total[0:OWN]
     taps_grad[...] = total[OWN : OWN + TAPS]
     gain_grad[...] = total[OWN + TAPS :]
-    for copy in copies:
-        copy.wait()
 
 
 def to_block(value):
@@ -413,7 +370,7 @@
         scalar_call(
             forward,
             [
-                (split, WIDE), (rest, WIDE), (rest, WIDE), ((8, LANES), WIDE),
+                narrow, (rest, WIDE), (rest, WIDE), ((8, LANES), WIDE),
                 ((HALVES, 8, LANES), WIDE), ((EDGE, WIDTH), WIDE), ((EDGE, MODEL), NARROW),
                 ((CLOSE, WIDTH, 2 * BLOCK), WIDE),
             ],
@@ -424,7 +381,7 @@
                 pltpu.VMEM((WIDTH, MODEL), NARROW), pltpu.VMEM((TAPS, WIDTH), NARROW),
                 pltpu.VMEM((1, WIDTH), WIDE), pltpu.VMEM((ROWS,), WIDE),
                 pltpu.VMEM((ROWS,), WIDE), pltpu.SemaphoreType.DMA((8,)),
-                taps_scratch, *([pltpu.VMEM((ROWS, LANES), WIDE)] * 4),
+                sides, taps_scratch, *([pltpu.VMEM((ROWS, LANES), WIDE)] * 4),
                 pltpu.VMEM((ROWS, WIDTH), WIDE), pltpu.VMEM(split, WIDE),
                 pltpu.VMEM((ROWS, WIDTH), WIDE),
             ],
@@ -448,30 +405,19 @@
     )
     sums = exchange(message, "tp", SUMS_ORDER)
     rows = CLOSE * WIDTH + 4 * SMALL
-    other, small, extended = scalar_call(
+    mine, other, small, extended = scalar_call(
         backward,
         [
-            ((rows, BLOCK), NARROW), ((SMALL, WIDTH), WIDE),
+            ((CLOSE, WIDTH, BLOCK), WIDE), ((rows, BLOCK), NARROW), ((SMALL, WIDTH), WIDE),
             ((HALVES, ROWS + 2 * EDGE, LANES), WIDE),
         ],
-        place, sums, scaled, spread, first_scaled, first_spread, halo, gated, row_scale,
-        gain_part, first_cotangent, first_hidden, product,
-        scratch=[pltpu.VMEM((HALVES, EDGE + 8, LANES), WIDE)], flops=100 * ROWS * WIDTH,
+        place, sums, scaled, spread, first_scaled, first_spread, halo, gated, row_scale, gain_part,
+        first_cotangent, first_hidden, product, scratch=[sides], flops=100 * ROWS * WIDTH,
     )
     other = lax.ppermute(other, "c", [(0, 1), (1, 0)])
-    value_grad, gate_grad, margin, last, mine = scalar_call(
-        gated_gradient,
-        [
-            narrow, narrow, (edge, WIDE), ((3, *edge), WIDE),
-            ((CLOSE, WIDTH, BLOCK), WIDE),
-        ],
-        place, extended, conv_taps, proj_value, proj_gate,
-        first_cotangent, first_hidden, product, outs_in_hbm=2,
-        scratch=[
-            taps_scratch, pltpu.VMEM(*narrow), pltpu.VMEM(*narrow),
-            pltpu.SemaphoreType.DMA((2 * len(PART_ENDS),)),
-        ],
-        flops=100 * ROWS * WIDTH,
+    d_gated, margin = call_with(
+        gated_gradient, [(split, WIDE), ((HALVES, EDGE, LANES), WIDE)], [taps_scratch],
+        extended, conv_taps, flops=100 * ROWS * WIDTH,
     )
     (pieces,) = call(
         pack, [((CLOSE, WIDTH + 2 * SMALL, BLOCK), NARROW)], mine, small, other, flops=1 << 20
@@ -485,9 +431,10 @@
     (message,) = call(hand_out, [((2 * CLOSE, OWN + SMALL, WIDTH), NARROW)], payload, flops=1 << 16)
     arrived = exchange(message, (*NEAR, "c"), GATHER_ORDER)
     (total,) = call(totals, [((OWN + SMALL, WIDTH), WIDE)], arrived, flops=1 << 20)
-    value_grad, gate_grad, weight_grad, taps_grad, gain_grad = last_call(
+    value_grad, gate_grad, weight_grad, taps_grad, gain_grad = call(
+        finish,
         [narrow, narrow, ((OWN, WIDTH), WIDE), ((TAPS, WIDTH), WIDE), ((1, WIDTH), WIDE)],
-        value_grad, gate_grad, total, last, late,
+        total, d_gated, late, proj_value, proj_gate, flops=10 * ROWS * WIDTH,
     )
     return (value_grad, gate_grad, weight_grad, taps_grad, gain_grad.reshape(WIDTH))
 
@@ -505,47 +452,25 @@
 
 
 def scalar_call(
-    body, outs, scalar, *args, scratch=(), flops=1 << 20, limit=6, in_hbm=0, outs_in_hbm=0
+    body, outs, scalar, *args, scratch=(), flops=1 << 20, limit=6, in_hbm=0
 ):
     shapes = [jax.ShapeDtypeStruct(shape, dtype) for shape, dtype in outs]
-    placed = [pltpu.HBM(*out) for out in outs[:outs_in_hbm]] + shapes[outs_in_hbm:]
     size = sum(a.size * a.dtype.itemsize for a in (*args, *shapes))
     whole = pl.BlockSpec(memory_space=pltpu.VMEM)
     far = [pltpu.with_memory_space_constraint(a, pltpu.HBM) for a in args[:in_hbm]]
     return pl.pallas_call(
         body,
-        out_shape=placed,
+        out_shape=shapes,
         in_specs=[
             pl.BlockSpec(memory_space=pltpu.SMEM),
             *([pl.BlockSpec(memory_space=pltpu.HBM)] * in_hbm),
             *([whole] * (len(args) - in_hbm)),
         ],
-        out_specs=[
-            *([pl.BlockSpec(memory_space=pltpu.HBM)] * outs_in_hbm),
-            *([whole] * (len(shapes) - outs_in_hbm)),
-        ],
+        out_specs=[whole] * len(shapes),
         scratch_shapes=scratch,
         compiler_params=pltpu.CompilerParams(vmem_limit_bytes=limit << 20),
         cost_estimate=pl.CostEstimate(flops=flops, bytes_accessed=size, transcendentals=0),
     )(scalar, *far, *args[in_hbm:])
-
-
-def last_call(outs, *args):
-    shapes = [jax.ShapeDtypeStruct(shape, dtype) for shape, dtype in outs]
-    far, whole = pl.BlockSpec(memory_space=pltpu.HBM), pl.BlockSpec(memory_space=pltpu.VMEM)
-    edge = pltpu.VMEM((EDGE, WIDTH), NARROW)
-    held = [pltpu.with_memory_space_constraint(a, pltpu.HBM) for a in args[:2]]
-    return pl.pallas_call(
-        finish,
-        out_shape=[*(pltpu.HBM(*out) for out in outs[:2]), *shapes[2:]],
-        in_specs=[far, far, whole, whole, whole],
-        out_specs=[far, far, whole, whole, whole],
-        scratch_shapes=[edge, edge, pltpu.SemaphoreType.DMA((2,))],
-        input_output_aliases={0: 0, 1: 1},
-        compiler_params=pltpu.CompilerParams(vmem_limit_bytes=6 << 20),
-        cost_estimate=pl.CostEstimate(flops=1 << 16, bytes_accessed=1 << 18, transcendentals=0),
-        name="finish",
-    )(*held, *args[2:])
 
 
 def solution(mesh):

time: 83.9 us -> 82.9 us (0.988)
  Pallas kernels: 9.59 us -> 7.99 us
  waiting for transfers between devices: 11.7 us -> 13 us
    pallas_call x4 -> x2, Pallas kernels: 8.32 us -> 4.99 us  [scalar_call(): pl.pallas_call(body, out_shape=shapes, in_specs=[pl.BlockSpec(memory_spac...]
    ppermute x1, waiting for transfers between devices: 0.01 us -> 1.92 us  [shards(): other = lax.ppermute(other, 'c', [(0, 1), (1, 0)])]
    pallas_call x4 -> x5, Pallas kernels: 1.06 us -> 1.94 us  [call(): pl.pallas_call(body, out_shape=shapes, compiler_params=pltpu.CompilerPara...]
    ppermute x2, waiting for transfers between devices: 0.54 us -> 1.4 us  [shifted(): lax.ppermute(value, axis, [(source, source + steps) for source in range(f...]
    all_to_all x1, waiting for transfers between devices: 4.45 us -> 3.58 us  [exchange(): lax.all_to_all(pieces, axes, 0, 0, tiled=True, axis_index_groups=groups)]
    ppermute x1, starting transfers between devices: 10.7 us -> 11.5 us  [to_block(): return lax.ppermute(value, SP, pairs)]
    pallas_call x1 -> x2, Pallas kernels: 0.21 us -> 1.07 us  [call_with(): pl.pallas_call(body, out_shape=shapes, scratch_shapes=scratch, compiler_p...]
  transfers between devices with their start and end apart: 5 -> 5, of which waited for: 3 -> 4; matrix products, arithmetic and copies ran while one was open for 0% -> 0% of each run, Pallas kernels for 7% -> 5%
where the time goes in v1:
time: 82.9 us; the launch traced here: 82.1 us
  starting transfers between devices  30.2 us (36%)
  blocking collectives  29.3 us (35%)
  waiting for transfers between devices  13 us (16%)
  Pallas kernels  7.99 us (10%)
    all_to_all x2, blocking collectives, exchange(): lax.all_to_all(pieces, axes, 0, 0, tiled=True, axis_index_groups=groups)  29.3 us
    ppermute x1, starting transfers between devices, to_block(): return lax.ppermute(value, SP, pairs)  11.5 us
    all_to_all x1, starting transfers between devices, exchange(): lax.all_to_all(pieces, axes, 0, 0, tiled=True, axis_index_groups=groups)  10.4 us
    ppermute x2, starting transfers between devices, shifted(): lax.ppermute(value, axis, [(source, source + steps) for source in range(f...  6.32 us
    ppermute x1, waiting for transfers between devices, to_block(): return lax.ppermute(value, SP, pairs)  6.09 us
    pallas_call x2, Pallas kernels, scalar_call(): pl.pallas_call(body, out_shape=shapes, in_specs=[pl.BlockSpec(memory_spac...  4.99 us
    all_to_all x1, waiting for transfers between devices, exchange(): lax.all_to_all(pieces, axes, 0, 0, tiled=True, axis_index_groups=groups)  3.58 us
    pallas_call x5, Pallas kernels, call(): pl.pallas_call(body, out_shape=shapes, compiler_params=pltpu.CompilerPara...  1.94 us
  transfers between devices with their start and end apart: 5, of which 4 were waited for; matrix products, arithmetic and copies ran while one was open for 0% of the time, Pallas kernels for 5%

profile of v1, /device:TPU:7, one launch (start us, length us, event | category | flops | bytes accessed | tf_op | source)
XLA Modules:
  0.0 82.1 jit_solution(1151215402403130475)
XLA Ops:
  0.6 0.0 copy-start.3
  0.6 0.0 copy-start.2
  0.7 0.0 copy-start.4
  0.7 0.0 copy-start.5
  0.7 0.8 multiply_convert_fusion
  1.5 4.0 %collective-permute-start = (bf16[32,256]{1,0:T(8,128)(2,1)S(1)}, bf16[32,256]{1,0:T(8,128)(2,1)S(1)}, u32[]{:S(2)}, u32[]{:S(2)}) collective-permute-start(bf16[32,256]{1,0:T(8,128)(2,1)S(1)} %multiply_convert_fusion), channel_id=1, source_target_pairs={{0,4},{4,8},{8,12},{12,16},{16,20},{20,24},{24,28},{28,32},{32,36}... | collective-permute-start | bytes 49160 | tf_op jit(solution)/shard_map/ppermute | solution.py:37
  5.5 3.4 %shard_map.119 = (bf16[384,256]{1,0:T(8,128)(2,1)S(1)}, f32[2,352,128]{2,1,0:T(8,128)S(1)}, f32[2,352,128]{2,1,0:T(8,128)S(1)}, f32[8,128]{1,0:T(8,128)S(1)}, f3...) custom-call(s32[1]{0:T(128)} %bitcast.place, ...), custom_call_target="tpu_custom_call" | custom-call | flops 805306368 | bytes 6225408 | tf_op jit(solution)/shard_map/pallas_call | solution.py:461
  8.9 0.0 collective-permute-done.halo
  8.9 0.0 copy-done.3
  8.9 0.0 copy-done.2
  8.9 0.0 copy-done.4
  8.9 0.0 copy-done.5
  8.9 0.2 shard_map.120
  9.2 7.5 %all_to_all.15.sums = f32[4,8,128]{2,1,0:T(8,128)S(1)} all-to-all(f32[4,8,128]{2,1,0:T(8,128)S(1)} %get-tuple-element.33), channel_id=1, replica_groups={{3,0,1,2},{7,4,5,6},{11,8,9,10},{15,12,13,14},{19,16,17,18},{23,20,21,2..., dimensions={0} | all-to-all | bytes 32768 | tf_op jit(solution)/shard_map/all_to_all | solution.py:42
  16.7 1.6 %shard_map.121 = (f32[8,256,128]{2,1,0:T(8,128)S(1)}, bf16[2176,128]{1,0:T(8,128)(2,1)S(1)}, f32[32,256]{1,0:T(8,128)S(1)}, f32[2,448,128]{2,1,0:T(8,128)S(1)}) custom-call(s32[1]{0:T(128)} %bitcast.place, f32[4,8,128]{2,1,0:T(8,128)S(1)} %all_to_all.15.sums, f32[2,352,128]{2,1,0:T(8,128)S(1)} %get-tuple-element.34.scaled, ...), custom_call_target="tpu_custom_call" | custom-call | flops 9830400 | bytes 5367296 | tf_op jit(solution)/shard_map/pallas_call | solution.py:461
  18.3 1.9 %collective-permute-start.1 = (bf16[2176,128]{1,0:T(8,128)(2,1)S(1)}, bf16[2176,128]{1,0:T(8,128)(2,1)S(1)}, u32[]{:S(2)}, u32[]{:S(2)}) collective-permute-start(bf16[2176,128]{1,0:T(8,128)(2,1)S(1)} %get-tuple-element.44), channel_id=1, source_target_pairs={{0,4},{4,0},{1,5},{5,1},{2,6},{6,2},{3,7},{7,3},{8,12},{12,8},{9,1... | collective-permute-start | bytes 1671176 | tf_op jit(solution)/shard_map/ppermute | solution.py:417
  20.2 1.9 %collective-permute-done.1.other = bf16[2176,128]{1,0:T(8,128)(2,1)S(1)} collective-permute-done((bf16[2176,128]{1,0:T(8,128)(2,1)S(1)}, bf16[2176,128]{1,0:T(8,128)(2,1)S(1)}, u32[]{:S(2)}, u32[]{:S(2)}) %collective-permute-start.1) | collective-permute-done | bytes 557088 | tf_op jit(solution)/shard_map/ppermute | solution.py:417
  22.1 0.1 shard_map.122
  22.2 0.0 copy-start
  22.2 0.0 copy-start.1
  22.2 21.8 %all_to_all.16.arrived = bf16[8,320,128]{2,1,0:T(8,128)(2,1)S(1)} all-to-all(bf16[8,320,128]{2,1,0:T(8,128)(2,1)S(1)} %shard_map.122), channel_id=1, replica_groups=mesh['zh'=16,'zl'=2,'x'=4,'c'=2,'tp'=4] {'zl','x'}, dimensions={0} | all-to-all | bytes 1310720 | tf_op jit(solution)/shard_map/all_to_all | solution.py:42
  44.1 0.1 shard_map.123
  44.2 11.5 %collective-permute-start.2 = (bf16[320,128]{1,0:T(8,128)(2,1)S(1)}, bf16[320,128]{1,0:T(8,128)(2,1)S(1)}, u32[]{:S(2)}, u32[]{:S(2)}) collective-permute-start(bf16[320,128]{1,0:T(8,128)(2,1)S(1)} %shard_map.123), channel_id=1, source_target_pairs={{0,0},{4,388},{8,968},{12,460},{16,912},{20,532},{24,856},{28,348}... | collective-permute-start | bytes 245768 | tf_op jit(solution)/shard_map/ppermute | solution.py:353
  55.7 6.1 %collective-permute-done.2.payload = bf16[320,128]{1,0:T(8,128)(2,1)S(1)} collective-permute-done((bf16[320,128]{1,0:T(8,128)(2,1)S(1)}, bf16[320,128]{1,0:T(8,128)(2,1)S(1)}, u32[]{:S(2)}, u32[]{:S(2)}) %collective-permute-start.2) | collective-permute-done | bytes 81952 | tf_op jit(solution)/shard_map/ppermute | solution.py:353
  61.8 0.8 %shard_map.124 = bf16[16,40,256]{2,1,0:T(8,128)(2,1)} custom-call(bf16[320,128]{1,0:T(8,128)(2,1)S(1)} %collective-permute-done.2.payload), custom_call_target="tpu_custom_call" | custom-call | flops 65536 | bytes 409600 | tf_op jit(solution)/shard_map/pallas_call | solution.py:56
  62.6 10.4 %all-to-all-start.2 = ((bf16[16,40,256]{2,1,0:T(8,128)(2,1)}), bf16[16,40,256]{2,1,0:T(8,128)(2,1)S(1)}, u32[]{:S(2)}, u32[]{:S(2)}) async-start(bf16[16,40,256]{2,1,0:T(8,128)(2,1)} %shard_map.124), calls=%async_computation.2 | async-start | bytes 655360 | tf_op jit(solution)/shard_map/all_to_all | solution.py:42
  73.0 0.9 %shard_map.126 = (f32[2,384,128]{2,1,0:T(8,128)S(1)}, f32[2,32,128]{2,1,0:T(8,128)S(1)}) custom-call(f32[2,448,128]{2,1,0:T(8,128)S(1)} %get-tuple-element.45.extended, bf16[31,256]{1,0:T(8,128)(2,1)S(1)} %copy-done.2), custom_call_target="tpu_custom_call" | custom-call | flops 9830400 | bytes 900608 | tf_op jit(solution)/shard_map/pallas_call | solution.py:445
  73.9 2.3 %collective-permute-start.3 = (f32[2,32,128]{2,1,0:T(8,128)S(1)}, f32[2,32,128]{2,1,0:T(8,128)S(1)}, u32[]{:S(2)}, u32[]{:S(2)}) collective-permute-start(f32[2,32,128]{2,1,0:T(8,128)S(1)} %get-tuple-element.47), channel_id=1, source_target_pairs={{4,0},{8,4},{12,8},{16,12},{20,16},{24,20},{28,24},{32,28},{36,32}... | collective-permute-start | bytes 98312 | tf_op jit(solution)/shard_map/ppermute | solution.py:37
  76.2 3.6 %all-to-all-done.2.arrived = bf16[16,40,256]{2,1,0:T(8,128)(2,1)S(1)} async-done(((bf16[16,40,256]{2,1,0:T(8,128)(2,1)}), bf16[16,40,256]{2,1,0:T(8,128)(2,1)S(1)}, u32[]{:S(2)}, u32[]{:S(2)}) %all-to-all-start.2) | async-done | bytes 327712 | tf_op jit(solution)/shard_map/all_to_all | solution.py:42
  79.8 1.4 %collective-permute-done.3.late = f32[2,32,128]{2,1,0:T(8,128)S(1)} collective-permute-done((f32[2,32,128]{2,1,0:T(8,128)S(1)}, f32[2,32,128]{2,1,0:T(8,128)S(1)}, u32[]{:S(2)}, u32[]{:S(2)}) %collective-permute-start.3) | collective-permute-done | bytes 32800 | tf_op jit(solution)/shard_map/ppermute | solution.py:37
  81.2 0.0 copy-done
  81.2 0.0 copy-done.1
  81.3 0.9 %shard_map.127 = (bf16[384,256]{1,0:T(8,128)(2,1)}, bf16[384,256]{1,0:T(8,128)(2,1)}, f32[8,256]{1,0:T(8,128)}, f32[31,256]{1,0:T(8,128)}, f32[1,256]{1,0:T(1,128)}) custom-call(f32[40,256]{1,0:T(8,128)S(1)} %shard_map.125.total, f32[2,384,128]{2,1,0:T(8,128)S(1)} %get-tuple-element.46.d_gated, f32[2,32,128]{2,1,0:T(8,128)S(1)} %collective-permute-done.3.late, ...), custom_call_target="tpu_custom_call" | custom-call | flops 983040 | bytes 1294336 | tf_op jit(solution)/shard_map/pallas_call | solution.py:56
  (1 shorter events, 0.0 us)
Async XLA Ops:
  0.6 8.3 %copy-start.3 = (f32[384]{0:T(512)S(1)}, f32[384]{0:T(512)}, u32[]{:S(2)}) copy-start(f32[384]{0:T(512)} %scale.3) | copy-start | bytes 4612
  0.6 8.3 %copy-start.2 = (bf16[31,256]{1,0:T(8,128)(2,1)S(1)}, bf16[31,256]{1,0:T(8,128)(2,1)}, u32[]{:S(2)}) copy-start(bf16[31,256]{1,0:T(8,128)(2,1)} %taps.3) | copy-start | bytes 47620
  0.7 8.3 %copy-start.4 = (f32[384]{0:T(512)S(1)}, f32[384]{0:T(512)}, u32[]{:S(2)}) copy-start(f32[384]{0:T(512)} %mean.1) | copy-start | bytes 4612
  0.7 8.3 %copy-start.5 = (f32[256]{0:T(256)S(1)}, f32[256]{0:T(256)}, u32[]{:S(2)}) copy-start(f32[256]{0:T(256)} %param.13) | copy-start | bytes 3076
  1.5 7.4 %collective-permute-start = (bf16[32,256]{1,0:T(8,128)(2,1)S(1)}, bf16[32,256]{1,0:T(8,128)(2,1)S(1)}, u32[]{:S(2)}, u32[]{:S(2)}) collective-permute-start(bf16[32,256]{1,0:T(8,128)(2,1)S(1)} %multiply_convert_fusion), channel_id=1, source_target_pairs={{0,4},{4,8},{8,12},{12,16},{16,20},{20,24},{24,28},{28,32},{32,36}... | collective-permute-start | bytes 49160 | tf_op jit(solution)/shard_map/ppermute | solution.py:37
  18.3 3.9 %collective-permute-start.1 = (bf16[2176,128]{1,0:T(8,128)(2,1)S(1)}, bf16[2176,128]{1,0:T(8,128)(2,1)S(1)}, u32[]{:S(2)}, u32[]{:S(2)}) collective-permute-start(bf16[2176,128]{1,0:T(8,128)(2,1)S(1)} %get-tuple-element.44), channel_id=1, source_target_pairs={{0,4},{4,0},{1,5},{5,1},{2,6},{6,2},{3,7},{7,3},{8,12},{12,8},{9,1... | collective-permute-start | bytes 1671176 | tf_op jit(solution)/shard_map/ppermute | solution.py:417
  22.2 59.0 %copy-start = (bf16[384,256]{1,0:T(8,128)(2,1)S(1)}, bf16[384,256]{1,0:T(8,128)(2,1)}, u32[]{:S(2)}) copy-start(bf16[384,256]{1,0:T(8,128)(2,1)} %gate.3) | copy-start | bytes 589828
  22.2 59.0 %copy-start.1 = (bf16[384,256]{1,0:T(8,128)(2,1)S(1)}, bf16[384,256]{1,0:T(8,128)(2,1)}, u32[]{:S(2)}) copy-start(bf16[384,256]{1,0:T(8,128)(2,1)} %value.3) | copy-start | bytes 589828
  44.2 17.6 %collective-permute-start.2 = (bf16[320,128]{1,0:T(8,128)(2,1)S(1)}, bf16[320,128]{1,0:T(8,128)(2,1)S(1)}, u32[]{:S(2)}, u32[]{:S(2)}) collective-permute-start(bf16[320,128]{1,0:T(8,128)(2,1)S(1)} %shard_map.123), channel_id=1, source_target_pairs={{0,0},{4,388},{8,968},{12,460},{16,912},{20,532},{24,856},{28,348}... | collective-permute-start | bytes 245768 | tf_op jit(solution)/shard_map/ppermute | solution.py:353
  62.6 17.2 %all-to-all-start.2 = ((bf16[16,40,256]{2,1,0:T(8,128)(2,1)}), bf16[16,40,256]{2,1,0:T(8,128)(2,1)S(1)}, u32[]{:S(2)}, u32[]{:S(2)}) async-start(bf16[16,40,256]{2,1,0:T(8,128)(2,1)} %shard_map.124), calls=%async_computation.2 | async-start | bytes 655360 | tf_op jit(solution)/shard_map/all_to_all | solution.py:42
  73.9 7.3 %collective-permute-start.3 = (f32[2,32,128]{2,1,0:T(8,128)S(1)}, f32[2,32,128]{2,1,0:T(8,128)S(1)}, u32[]{:S(2)}, u32[]{:S(2)}) collective-permute-start(f32[2,32,128]{2,1,0:T(8,128)S(1)} %get-tuple-element.47), channel_id=1, source_target_pairs={{4,0},{8,4},{12,8},{16,12},{20,16},{24,20},{28,24},{32,28},{36,32}... | collective-permute-start | bytes 98312 | tf_op jit(solution)/shard_map/ppermute | solution.py:37

commit v2 on v1

--- a/solution.py
+++ b/solution.py
@@ -16,7 +16,7 @@
 SUMS_ORDER = [3, 0, 1, 2]
 OFFSETS = ((0, -1, -2, -3, 3, 2, 1, -4), (6, 7, 8, 5, -7, -6, -5, 4))
 BLOCK = CLOSE * 2 * 8
-GATHER_ORDER = [(place + 1) % (2 * CLOSE) for place in range(2 * CLOSE)]
+GATHER_ORDER = [(place + 7) % (2 * CLOSE) for place in range(2 * CLOSE)]
 TAPS = 31
 SMALL = TAPS + 1
 ROWS = 384
@@ -205,10 +205,17 @@
         message[peer] = total
 
 
+def head_product(cotangent, hidden, place, near, side):
+    columns = both_blocks(cotangent, place, near)[:, side * BLOCK : (side + 1) * BLOCK]
+    return lax.dot_general(
+        hidden[...], columns, (((0,), (0,)), ((), ())), preferred_element_type=WIDE
+    )
+
+
 def backward(
     place, sums, scaled, spread, first_scaled, first_spread, halo, gated, scale, gain_part,
     first_cotangent, first_hidden, product,
-    mine, other, small, extended,
+    other, small, extended,
     padded,
 ):
     for half in range(HALVES):
@@ -253,12 +260,10 @@
                 tap = 8 * q + offset - lead
                 small[tap : tap + 1, lanes(half)] = jnp.sum(found[half, q], 0, keepdims=True)
         near = offset
-        whole = product[near] + lax.dot_general(
-            first_hidden[...], both_blocks(first_cotangent, place, near),
-            (((0,), (0,)), ((), ())), preferred_element_type=WIDE,
+        whole = product[near, :, BLOCK:] + head_product(
+            first_cotangent, first_hidden, place, near, 1
         )
-        mine[near] = whole[:, 0:BLOCK]
-        other[near * WIDTH : (near + 1) * WIDTH] = whole[:, BLOCK:].astype(NARROW)
+        other[near * WIDTH : (near + 1) * WIDTH] = whole.astype(NARROW)
     for half in range(HALVES):
         small[TAPS:SMALL, lanes(half)] = jnp.sum(gain_part[half], 0, keepdims=True)
     for half in range(HALVES):
@@ -284,7 +289,15 @@
             pieces[near, rows] = (mine[near, rows] + there).astype(NARROW)
 
 
-def gated_gradient(extended, taps, d_gated, margin, taps_wide):
+def gated_gradient(
+    place, extended, taps, first_cotangent, first_hidden, product,
+    d_gated, margin, mine,
+    taps_wide,
+):
+    for near in range(CLOSE):
+        mine[near] = product[near, :, 0:BLOCK] + head_product(
+            first_cotangent, first_hidden, place, near, 0
+        )
     taps_wide[0:TAPS] = taps[...].astype(WIDE)
     for half in range(HALVES):
         for start in range(0, EDGE + ROWS, EDGE):
@@ -405,19 +418,21 @@
     )
     sums = exchange(message, "tp", SUMS_ORDER)
     rows = CLOSE * WIDTH + 4 * SMALL
-    mine, other, small, extended = scalar_call(
+    other, small, extended = scalar_call(
         backward,
         [
-            ((CLOSE, WIDTH, BLOCK), WIDE), ((rows, BLOCK), NARROW), ((SMALL, WIDTH), WIDE),
+            ((rows, BLOCK), NARROW), ((SMALL, WIDTH), WIDE),
             ((HALVES, ROWS + 2 * EDGE, LANES), WIDE),
         ],
         place, sums, scaled, spread, first_scaled, first_spread, halo, gated, row_scale, gain_part,
         first_cotangent, first_hidden, product, scratch=[sides], flops=100 * ROWS * WIDTH,
     )
     other = lax.ppermute(other, "c", [(0, 1), (1, 0)])
-    d_gated, margin = call_with(
-        gated_gradient, [(split, WIDE), ((HALVES, EDGE, LANES), WIDE)], [taps_scratch],
-        extended, conv_taps, flops=100 * ROWS * WIDTH,
+    d_gated, margin, mine = scalar_call(
+        gated_gradient,
+        [(split, WIDE), ((HALVES, EDGE, LANES), WIDE), ((CLOSE, WIDTH, BLOCK), WIDE)],
+        place, extended, conv_taps, first_cotangent, first_hidden, product,
+        scratch=[taps_scratch], flops=100 * ROWS * WIDTH,
     )
     (pieces,) = call(
         pack, [((CLOSE, WIDTH + 2 * SMALL, BLOCK), NARROW)], mine, small, other, flops=1 << 20

time: 82.9 us -> 81.8 us (0.987)
  starting transfers between devices: 30.2 us -> 28.4 us
    all_to_all x1, waiting for transfers between devices: 3.58 us -> 6.33 us  [exchange(): lax.all_to_all(pieces, axes, 0, 0, tiled=True, axis_index_groups=groups)]
    all_to_all x1, starting transfers between devices: 10.4 us -> 8.61 us  [exchange(): lax.all_to_all(pieces, axes, 0, 0, tiled=True, axis_index_groups=groups)]
    ppermute x2, waiting for transfers between devices: 1.4 us -> 0.01 us  [shifted(): lax.ppermute(value, axis, [(source, source + steps) for source in range(f...]
    ppermute x1, waiting for transfers between devices: 1.92 us -> 0.71 us  [shards(): other = lax.ppermute(other, 'c', [(0, 1), (1, 0)])]
    pallas_call x2 -> x3, Pallas kernels: 4.99 us -> 6.09 us  [scalar_call(): pl.pallas_call(body, out_shape=shapes, in_specs=[pl.BlockSpec(memory_spac...]
    pallas_call x2 -> x1, Pallas kernels: 1.07 us -> 0.21 us  [call_with(): pl.pallas_call(body, out_shape=shapes, scratch_shapes=scratch, compiler_p...]
  transfers between devices with their start and end apart: 5 -> 5, of which waited for: 4 -> 3; matrix products, arithmetic and copies ran while one was open for 0% -> 0% of each run, Pallas kernels for 5% -> 6%
where the time goes in v2:
time: 81.8 us; the launch traced here: 80.8 us
  blocking collectives  29.3 us (36%)
  starting transfers between devices  28.4 us (35%)
  waiting for transfers between devices  13.1 us (16%)
  Pallas kernels  8.24 us (10%)
  between operations  0.82 us (1%)
    all_to_all x2, blocking collectives, exchange(): lax.all_to_all(pieces, axes, 0, 0, tiled=True, axis_index_groups=groups)  29.3 us
    ppermute x1, starting transfers between devices, to_block(): return lax.ppermute(value, SP, pairs)  11.6 us
    all_to_all x1, starting transfers between devices, exchange(): lax.all_to_all(pieces, axes, 0, 0, tiled=True, axis_index_groups=groups)  8.61 us
    ppermute x2, starting transfers between devices, shifted(): lax.ppermute(value, axis, [(source, source + steps) for source in range(f...  6.33 us
    all_to_all x1, waiting for transfers between devices, exchange(): lax.all_to_all(pieces, axes, 0, 0, tiled=True, axis_index_groups=groups)  6.33 us
    pallas_call x3, Pallas kernels, scalar_call(): pl.pallas_call(body, out_shape=shapes, in_specs=[pl.BlockSpec(memory_spac...  6.09 us
    ppermute x1, waiting for transfers between devices, to_block(): return lax.ppermute(value, SP, pairs)  6.09 us
    pallas_call x5, Pallas kernels, call(): pl.pallas_call(body, out_shape=shapes, compiler_params=pltpu.CompilerPara...  1.94 us
  transfers between devices with their start and end apart: 5, of which 3 were waited for; matrix products, arithmetic and copies ran while one was open for 0% of the time, Pallas kernels for 6%

profile of v2, /device:TPU:7, one launch (start us, length us, event | category | flops | bytes accessed | tf_op | source)
XLA Modules:
  0.0 80.8 jit_solution(4720335731609674390)
XLA Ops:
  0.6 0.0 copy-start.3
  0.6 0.0 copy-start.2
  0.7 0.0 copy-start.4
  0.7 0.0 copy-start.5
  0.7 0.8 multiply_convert_fusion
  1.5 4.0 %collective-permute-start = (bf16[32,256]{1,0:T(8,128)(2,1)S(1)}, bf16[32,256]{1,0:T(8,128)(2,1)S(1)}, u32[]{:S(2)}, u32[]{:S(2)}) collective-permute-start(bf16[32,256]{1,0:T(8,128)(2,1)S(1)} %multiply_convert_fusion), channel_id=1, source_target_pairs={{0,4},{4,8},{8,12},{12,16},{16,20},{20,24},{24,28},{28,32},{32,36}... | collective-permute-start | bytes 49160 | tf_op jit(solution)/shard_map/ppermute | solution.py:37
  5.5 3.4 %shard_map.119 = (bf16[384,256]{1,0:T(8,128)(2,1)S(1)}, f32[2,352,128]{2,1,0:T(8,128)S(1)}, f32[2,352,128]{2,1,0:T(8,128)S(1)}, f32[8,128]{1,0:T(8,128)S(1)}, f3...) custom-call(s32[1]{0:T(128)} %bitcast.place, ...), custom_call_target="tpu_custom_call" | custom-call | flops 805306368 | bytes 6225408 | tf_op jit(solution)/shard_map/pallas_call | solution.py:476
  8.9 0.0 collective-permute-done.halo
  8.9 0.0 copy-done.3
  8.9 0.0 copy-done.2
  8.9 0.0 copy-done.4
  8.9 0.0 copy-done.5
  8.9 0.2 shard_map.120
  9.2 7.5 %all_to_all.15.sums = f32[4,8,128]{2,1,0:T(8,128)S(1)} all-to-all(f32[4,8,128]{2,1,0:T(8,128)S(1)} %get-tuple-element.33), channel_id=1, replica_groups={{3,0,1,2},{7,4,5,6},{11,8,9,10},{15,12,13,14},{19,16,17,18},{23,20,21,2..., dimensions={0} | all-to-all | bytes 32768 | tf_op jit(solution)/shard_map/all_to_all | solution.py:42
  16.7 1.5 %shard_map.121 = (bf16[2176,128]{1,0:T(8,128)(2,1)S(1)}, f32[32,256]{1,0:T(8,128)S(1)}, f32[2,448,128]{2,1,0:T(8,128)S(1)}) custom-call(s32[1]{0:T(128)} %bitcast.place, f32[4,8,128]{2,1,0:T(8,128)S(1)} %all_to_all.15.sums, f32[2,352,128]{2,1,0:T(8,128)S(1)} %get-tuple-element.34.scaled, f32[2,352,128]{2,1,0:T(8,128)S(1)} %get-tuple-element.35.spread, ...), custom_call_target="tpu_custom_call" | custom-call | flops 9830400 | bytes 4318720 | tf_op jit(solution)/shard_map/pallas_call | solution.py:476
  18.2 1.9 %collective-permute-start.1 = (bf16[2176,128]{1,0:T(8,128)(2,1)S(1)}, bf16[2176,128]{1,0:T(8,128)(2,1)S(1)}, u32[]{:S(2)}, u32[]{:S(2)}) collective-permute-start(bf16[2176,128]{1,0:T(8,128)(2,1)S(1)} %get-tuple-element.45), channel_id=1, source_target_pairs={{0,4},{4,0},{1,5},{5,1},{2,6},{6,2},{3,7},{7,3},{8,12},{12,8},{9,1... | collective-permute-start | bytes 1671176 | tf_op jit(solution)/shard_map/ppermute | solution.py:430
  20.1 1.2 %shard_map.122 = (f32[2,384,128]{2,1,0:T(8,128)S(1)}, f32[2,32,128]{2,1,0:T(8,128)S(1)}, f32[8,256,128]{2,1,0:T(8,128)S(1)}) custom-call(s32[1]{0:T(128)} %bitcast.place, f32[2,448,128]{2,1,0:T(8,128)S(1)} %get-tuple-element.42.extended, bf16[31,256]{1,0:T(8,128)(2,1)S(1)} %copy-done.2, bf16[32,2048]{1,0:T(8,128)(2,1)S(1)} %get-tuple-element.39.first_cotangent, ...), custom_call_target="tpu_custom_call" | custom-call | flops 9830400 | bytes 4193792 | tf_op jit(solution)/shard_map/pallas_call | solution.py:476
  21.3 0.7 collective-permute-done.1.other
  22.0 0.1 shard_map.123
  22.1 0.0 copy-start
  22.1 0.0 copy-start.1
  22.1 21.8 %all_to_all.16.arrived = bf16[8,320,128]{2,1,0:T(8,128)(2,1)S(1)} all-to-all(bf16[8,320,128]{2,1,0:T(8,128)(2,1)S(1)} %shard_map.123), channel_id=1, replica_groups=mesh['zh'=16,'zl'=2,'x'=4,'c'=2,'tp'=4] {'zl','x'}, dimensions={0} | all-to-all | bytes 1310720 | tf_op jit(solution)/shard_map/all_to_all | solution.py:42
  44.0 0.1 shard_map.124
  44.1 11.6 %collective-permute-start.2 = (bf16[320,128]{1,0:T(8,128)(2,1)S(1)}, bf16[320,128]{1,0:T(8,128)(2,1)S(1)}, u32[]{:S(2)}, u32[]{:S(2)}) collective-permute-start(bf16[320,128]{1,0:T(8,128)(2,1)S(1)} %shard_map.124), channel_id=1, source_target_pairs={{0,0},{4,388},{8,968},{12,460},{16,912},{20,532},{24,856},{28,348}... | collective-permute-start | bytes 245768 | tf_op jit(solution)/shard_map/ppermute | solution.py:366
  55.6 6.1 %collective-permute-done.2.payload = bf16[320,128]{1,0:T(8,128)(2,1)S(1)} collective-permute-done((bf16[320,128]{1,0:T(8,128)(2,1)S(1)}, bf16[320,128]{1,0:T(8,128)(2,1)S(1)}, u32[]{:S(2)}, u32[]{:S(2)}) %collective-permute-start.2) | collective-permute-done | bytes 81952 | tf_op jit(solution)/shard_map/ppermute | solution.py:366
  61.7 0.8 %shard_map.125 = bf16[16,40,256]{2,1,0:T(8,128)(2,1)} custom-call(bf16[320,128]{1,0:T(8,128)(2,1)S(1)} %collective-permute-done.2.payload), custom_call_target="tpu_custom_call" | custom-call | flops 65536 | bytes 409600 | tf_op jit(solution)/shard_map/pallas_call | solution.py:56
  62.5 8.6 %all-to-all-start.2 = ((bf16[16,40,256]{2,1,0:T(8,128)(2,1)}), bf16[16,40,256]{2,1,0:T(8,128)(2,1)S(1)}, u32[]{:S(2)}, u32[]{:S(2)}) async-start(bf16[16,40,256]{2,1,0:T(8,128)(2,1)} %shard_map.125), calls=%async_computation.2 | async-start | bytes 655360 | tf_op jit(solution)/shard_map/all_to_all | solution.py:42
  71.2 2.3 %collective-permute-start.3 = (f32[2,32,128]{2,1,0:T(8,128)S(1)}, f32[2,32,128]{2,1,0:T(8,128)S(1)}, u32[]{:S(2)}, u32[]{:S(2)}) collective-permute-start(f32[2,32,128]{2,1,0:T(8,128)S(1)} %get-tuple-element.47), channel_id=1, source_target_pairs={{4,0},{8,4},{12,8},{16,12},{20,16},{24,20},{28,24},{32,28},{36,32}... | collective-permute-start | bytes 98312 | tf_op jit(solution)/shard_map/ppermute | solution.py:37
  73.5 6.3 %all-to-all-done.2.arrived = bf16[16,40,256]{2,1,0:T(8,128)(2,1)S(1)} async-done(((bf16[16,40,256]{2,1,0:T(8,128)(2,1)}), bf16[16,40,256]{2,1,0:T(8,128)(2,1)S(1)}, u32[]{:S(2)}, u32[]{:S(2)}) %all-to-all-start.2) | async-done | bytes 327712 | tf_op jit(solution)/shard_map/all_to_all | solution.py:42
  79.9 0.0 collective-permute-done.3.late
  79.9 0.0 copy-done
  79.9 0.0 copy-done.1
  79.9 0.9 %shard_map.127 = (bf16[384,256]{1,0:T(8,128)(2,1)}, bf16[384,256]{1,0:T(8,128)(2,1)}, f32[8,256]{1,0:T(8,128)}, f32[31,256]{1,0:T(8,128)}, f32[1,256]{1,0:T(1,128)}) custom-call(f32[40,256]{1,0:T(8,128)S(1)} %shard_map.126.total, f32[2,384,128]{2,1,0:T(8,128)S(1)} %get-tuple-element.46.d_gated, f32[2,32,128]{2,1,0:T(8,128)S(1)} %collective-permute-done.3.late, ...), custom_call_target="tpu_custom_call" | custom-call | flops 983040 | bytes 1294336 | tf_op jit(solution)/shard_map/pallas_call | solution.py:56
  (1 shorter events, 0.0 us)
Async XLA Ops:
  0.6 8.3 %copy-start.3 = (f32[384]{0:T(512)S(1)}, f32[384]{0:T(512)}, u32[]{:S(2)}) copy-start(f32[384]{0:T(512)} %scale.3) | copy-start | bytes 4612
  0.6 8.3 %copy-start.2 = (bf16[31,256]{1,0:T(8,128)(2,1)S(1)}, bf16[31,256]{1,0:T(8,128)(2,1)}, u32[]{:S(2)}) copy-start(bf16[31,256]{1,0:T(8,128)(2,1)} %taps.3) | copy-start | bytes 47620
  0.7 8.3 %copy-start.4 = (f32[384]{0:T(512)S(1)}, f32[384]{0:T(512)}, u32[]{:S(2)}) copy-start(f32[384]{0:T(512)} %mean.1) | copy-start | bytes 4612
  0.7 8.3 %copy-start.5 = (f32[256]{0:T(256)S(1)}, f32[256]{0:T(256)}, u32[]{:S(2)}) copy-start(f32[256]{0:T(256)} %param.13) | copy-start | bytes 3076
  1.5 7.4 %collective-permute-start = (bf16[32,256]{1,0:T(8,128)(2,1)S(1)}, bf16[32,256]{1,0:T(8,128)(2,1)S(1)}, u32[]{:S(2)}, u32[]{:S(2)}) collective-permute-start(bf16[32,256]{1,0:T(8,128)(2,1)S(1)} %multiply_convert_fusion), channel_id=1, source_target_pairs={{0,4},{4,8},{8,12},{12,16},{16,20},{20,24},{24,28},{28,32},{32,36}... | collective-permute-start | bytes 49160 | tf_op jit(solution)/shard_map/ppermute | solution.py:37
  18.2 3.9 %collective-permute-start.1 = (bf16[2176,128]{1,0:T(8,128)(2,1)S(1)}, bf16[2176,128]{1,0:T(8,128)(2,1)S(1)}, u32[]{:S(2)}, u32[]{:S(2)}) collective-permute-start(bf16[2176,128]{1,0:T(8,128)(2,1)S(1)} %get-tuple-element.45), channel_id=1, source_target_pairs={{0,4},{4,0},{1,5},{5,1},{2,6},{6,2},{3,7},{7,3},{8,12},{12,8},{9,1... | collective-permute-start | bytes 1671176 | tf_op jit(solution)/shard_map/ppermute | solution.py:430
  22.1 57.8 %copy-start = (bf16[384,256]{1,0:T(8,128)(2,1)S(1)}, bf16[384,256]{1,0:T(8,128)(2,1)}, u32[]{:S(2)}) copy-start(bf16[384,256]{1,0:T(8,128)(2,1)} %gate.3) | copy-start | bytes 589828
  22.1 57.8 %copy-start.1 = (bf16[384,256]{1,0:T(8,128)(2,1)S(1)}, bf16[384,256]{1,0:T(8,128)(2,1)}, u32[]{:S(2)}) copy-start(bf16[384,256]{1,0:T(8,128)(2,1)} %value.3) | copy-start | bytes 589828
  44.1 17.6 %collective-permute-start.2 = (bf16[320,128]{1,0:T(8,128)(2,1)S(1)}, bf16[320,128]{1,0:T(8,128)(2,1)S(1)}, u32[]{:S(2)}, u32[]{:S(2)}) collective-permute-start(bf16[320,128]{1,0:T(8,128)(2,1)S(1)} %shard_map.124), channel_id=1, source_target_pairs={{0,0},{4,388},{8,968},{12,460},{16,912},{20,532},{24,856},{28,348}... | collective-permute-start | bytes 245768 | tf_op jit(solution)/shard_map/ppermute | solution.py:366
  62.5 17.3 %all-to-all-start.2 = ((bf16[16,40,256]{2,1,0:T(8,128)(2,1)}), bf16[16,40,256]{2,1,0:T(8,128)(2,1)S(1)}, u32[]{:S(2)}, u32[]{:S(2)}) async-start(bf16[16,40,256]{2,1,0:T(8,128)(2,1)} %shard_map.125), calls=%async_computation.2 | async-start | bytes 655360 | tf_op jit(solution)/shard_map/all_to_all | solution.py:42
  71.2 8.7 %collective-permute-start.3 = (f32[2,32,128]{2,1,0:T(8,128)S(1)}, f32[2,32,128]{2,1,0:T(8,128)S(1)}, u32[]{:S(2)}, u32[]{:S(2)}) collective-permute-start(f32[2,32,128]{2,1,0:T(8,128)S(1)} %get-tuple-element.47), channel_id=1, source_target_pairs={{4,0},{8,4},{12,8},{16,12},{20,16},{24,20},{28,24},{32,28},{36,32}... | collective-permute-start | bytes 98312 | tf_op jit(solution)/shard_map/ppermute | solution.py:37

commit v3 on v2

--- a/solution.py
+++ b/solution.py
@@ -13,9 +13,10 @@
 CLOSE = 8
 AXES = (("zh", FAR), ("zl", 2), ("x", 4), ("c", 2))
 TP = 4
-SUMS_ORDER = [3, 0, 1, 2]
+SUMS_ORDER = [2, 3, 0, 1]
 OFFSETS = ((0, -1, -2, -3, 3, 2, 1, -4), (6, 7, 8, 5, -7, -6, -5, 4))
 BLOCK = CLOSE * 2 * 8
+NEAR_ORDER = [(place + 4) % CLOSE for place in range(CLOSE)]
 GATHER_ORDER = [(place + 7) % (2 * CLOSE) for place in range(2 * CLOSE)]
 TAPS = 31
 SMALL = TAPS + 1
@@ -92,20 +93,40 @@
     return jnp.concatenate([cotangent[:, columns[0]], cotangent[:, columns[1]]], 1)
 
 
-def forward(
-    place, value, gate, cotangent, weight, far_taps, far_gain, far_mean, far_scale,
-    gated, scaled, spread, sums, gain_part, first_upstream, first_cotangent, product,
-    held_value, held_gate, held, held_weight, taps, gain, mean, scale, arrivals,
-    padded, taps_wide, mean_columns, scale_columns, sum_first, sum_second,
-    hidden, normed, upstream,
+def load(
+    value, gate, taps, gain, mean, scale,
+    end, held_value, held_gate, held_taps, held_gain, held_mean, held_scale,
+    arrivals,
 ):
     copies = [
         pltpu.make_async_copy(source, target, arrivals.at[i])
         for i, (source, target) in enumerate(
             (
-                (value, held_value), (gate, held_gate), (far_taps, taps), (far_mean, mean),
-                (far_scale, scale), (far_gain, gain), (weight, held_weight), (cotangent, held),
+                (value, held_value), (gate, held_gate), (taps, held_taps), (gain, held_gain),
+                (mean, held_mean), (scale, held_scale),
             )
+        )
+    ]
+    for copy in copies:
+        copy.start()
+    for copy in copies:
+        copy.wait()
+    rows = slice(ROWS - EDGE, ROWS)
+    sig = jax.nn.sigmoid(held_gate[rows].astype(WIDE))
+    end[...] = (held_value[rows].astype(WIDE) * sig).astype(NARROW)
+
+
+def forward(
+    place, cotangent, weight, held_value, held_gate, taps, gain, mean, scale,
+    gated, scaled, spread, sums, gain_part, first_upstream, first_cotangent, product,
+    held, held_weight, arrivals,
+    padded, taps_wide, mean_columns, scale_columns, sum_first, sum_second,
+    hidden, normed, upstream,
+):
+    copies = [
+        pltpu.make_async_copy(source, target, arrivals.at[i])
+        for i, (source, target) in enumerate(
+            ((weight, held_weight), (cotangent, held))
         )
     ]
     for copy in copies:
@@ -113,8 +134,6 @@
     sum_first[0:EDGE] = jnp.zeros((EDGE, LANES), WIDE)
     sum_second[0:EDGE] = jnp.zeros((EDGE, LANES), WIDE)
     hidden[0:EDGE] = jnp.zeros((EDGE, WIDTH), WIDE)
-    for copy in copies[:6]:
-        copy.wait()
     taps_wide[0:TAPS] = taps[...].astype(WIDE)
     for block in range(ROWS // LANES):
         rows = slice(block * LANES, (block + 1) * LANES)
@@ -131,8 +150,8 @@
             rows = slice(start, start + EDGE)
             conv = convolve(padded, half, taps_wide, start, EDGE)
             normed[half, rows] = (conv - mean_columns[rows]) * scale_columns[rows]
-    copies[6].wait()
-    copies[7].wait()
+    for copy in copies:
+        copy.wait()
     upstream[...] = lax.dot_general(
         held[...], held_weight[...], (((1,), (1,)), ((), ())), preferred_element_type=WIDE
     )
@@ -286,12 +305,12 @@
         for start in range(0, WIDTH, 64):
             rows = slice(start, start + 64)
             there = other[near * WIDTH + start : near * WIDTH + start + 64].astype(WIDE)
-            pieces[near, rows] = (mine[near, rows] + there).astype(NARROW)
+            pieces[NEAR_ORDER.index(near), rows] = (mine[near, rows] + there).astype(NARROW)
 
 
 def gated_gradient(
-    place, extended, taps, first_cotangent, first_hidden, product,
-    d_gated, margin, mine,
+    place, extended, taps, value, gate, first_cotangent, first_hidden, product,
+    value_grad, gate_grad, margin, last, mine,
     taps_wide,
 ):
     for near in range(CLOSE):
@@ -307,8 +326,15 @@
                 found = found + taps_wide[tap : tap + 1, lanes(half)] * extended[half, begin : begin + EDGE]
             if start == 0:
                 margin[half] = found
+                continue
+            rows = slice(start - EDGE, start)
+            sig = jax.nn.sigmoid(gate[rows, lanes(half)].astype(WIDE))
+            slope = value[rows, lanes(half)].astype(WIDE) * sig * (1.0 - sig)
+            if start == ROWS:
+                last[0, half], last[1, half], last[2, half] = found, sig, slope
             else:
-                d_gated[half, start - EDGE : start] = found
+                value_grad[rows, lanes(half)] = (found * sig).astype(NARROW)
+                gate_grad[rows, lanes(half)] = (found * slope).astype(NARROW)
 
 
 def fold_near(arrived, payload):
@@ -338,22 +364,30 @@
 
 
 def finish(
-    total, d_gated, late, value, gate,
+    total, value_part, gate_part, last, late,
     value_grad, gate_grad, weight_grad, taps_grad, gain_grad,
-):
-    for half in range(HALVES):
-        for start in range(0, ROWS, EDGE):
-            rows = slice(start, start + EDGE)
-            grad = d_gated[half, rows]
-            if start == ROWS - EDGE:
-                grad = grad + late[half]
-            sig = jax.nn.sigmoid(gate[rows, lanes(half)].astype(WIDE))
-            wide = value[rows, lanes(half)].astype(WIDE)
-            value_grad[rows, lanes(half)] = (grad * sig).astype(NARROW)
-            gate_grad[rows, lanes(half)] = (grad * wide * sig * (1.0 - sig)).astype(NARROW)
-    weight_grad[...] = total[0:OWN]
-    taps_grad[...] = total[OWN : OWN + TAPS]
-    gain_grad[...] = total[OWN + TAPS :]
+    value_end, gate_end, taps_held, gain_held, departures,
+):
+    main, end = pl.ds(0, ROWS - EDGE), pl.ds(ROWS - EDGE, EDGE)
+    taps_held[...] = total[OWN : OWN + TAPS]
+    gain_held[...] = total[OWN + TAPS :]
+    for half in range(HALVES):
+        grad = last[0, half] + late[half]
+        value_end[:, lanes(half)] = (grad * last[1, half]).astype(NARROW)
+        gate_end[:, lanes(half)] = (grad * last[2, half]).astype(NARROW)
+    copies = [
+        pltpu.make_async_copy(value_part, value_grad.at[main], departures.at[0]),
+        pltpu.make_async_copy(gate_part, gate_grad.at[main], departures.at[1]),
+        pltpu.make_async_copy(total.at[pl.ds(0, OWN)], weight_grad, departures.at[2]),
+        pltpu.make_async_copy(taps_held, taps_grad, departures.at[3]),
+        pltpu.make_async_copy(gain_held, gain_grad, departures.at[4]),
+        pltpu.make_async_copy(value_end, value_grad.at[end], departures.at[5]),
+        pltpu.make_async_copy(gate_end, gate_grad.at[end], departures.at[6]),
+    ]
+    for copy in copies:
+        copy.start()
+    for copy in copies:
+        copy.wait()
 
 
 def to_block(value):
@@ -369,12 +403,13 @@
 def shards(
     proj_value, proj_gate, out_cotangent, out_weight, conv_taps, norm_gain, row_mean, row_scale
 ):
-    end_gate = jax.nn.sigmoid(proj_gate[ROWS - EDGE :].astype(WIDE))
-    end = (proj_value[ROWS - EDGE :].astype(WIDE) * end_gate).astype(NARROW)
+    row_gain = norm_gain.reshape(1, WIDTH)
+    end, proj_value, proj_gate, conv_taps, row_gain, row_mean, row_scale = load_call(
+        proj_value, proj_gate, conv_taps, row_gain, row_mean, row_scale
+    )
     halo = shifted(end, SP, 1)
     split = (HALVES, ROWS, LANES)
     rest = (HALVES, ROWS - EDGE, LANES)
-    row_gain = norm_gain.reshape(1, WIDTH)
     sides = pltpu.VMEM((HALVES, EDGE + ROWS, LANES), WIDE)
     taps_scratch = pltpu.VMEM((TAPS + 1, WIDTH), WIDE)
     place = lax.axis_index(SP).reshape(1)
@@ -387,13 +422,11 @@
                 ((HALVES, 8, LANES), WIDE), ((EDGE, WIDTH), WIDE), ((EDGE, MODEL), NARROW),
                 ((CLOSE, WIDTH, 2 * BLOCK), WIDE),
             ],
-            place, proj_value, proj_gate, out_cotangent, out_weight,
-            conv_taps, row_gain, row_mean, row_scale, in_hbm=8,
+            place, out_cotangent, out_weight, proj_value, proj_gate,
+            conv_taps, row_gain, row_mean, row_scale, in_hbm=2,
             scratch=[
-                pltpu.VMEM(*narrow), pltpu.VMEM(*narrow), pltpu.VMEM((ROWS, MODEL), NARROW),
-                pltpu.VMEM((WIDTH, MODEL), NARROW), pltpu.VMEM((TAPS, WIDTH), NARROW),
-                pltpu.VMEM((1, WIDTH), WIDE), pltpu.VMEM((ROWS,), WIDE),
-                pltpu.VMEM((ROWS,), WIDE), pltpu.SemaphoreType.DMA((8,)),
+                pltpu.VMEM((ROWS, MODEL), NARROW), pltpu.VMEM((WIDTH, MODEL), NARROW),
+                pltpu.SemaphoreType.DMA((2,)),
                 sides, taps_scratch, *([pltpu.VMEM((ROWS, LANES), WIDE)] * 4),
                 pltpu.VMEM((ROWS, WIDTH), WIDE), pltpu.VMEM(split, WIDE),
                 pltpu.VMEM((ROWS, WIDTH), WIDE),
@@ -428,16 +461,17 @@
         first_cotangent, first_hidden, product, scratch=[sides], flops=100 * ROWS * WIDTH,
     )
     other = lax.ppermute(other, "c", [(0, 1), (1, 0)])
-    d_gated, margin, mine = scalar_call(
+    main = ((ROWS - EDGE, WIDTH), NARROW)
+    value_part, gate_part, margin, last, mine = scalar_call(
         gated_gradient,
-        [(split, WIDE), ((HALVES, EDGE, LANES), WIDE), ((CLOSE, WIDTH, BLOCK), WIDE)],
-        place, extended, conv_taps, first_cotangent, first_hidden, product,
-        scratch=[taps_scratch], flops=100 * ROWS * WIDTH,
+        [main, main, (edge, WIDE), ((3, *edge), WIDE), ((CLOSE, WIDTH, BLOCK), WIDE)],
+        place, extended, conv_taps, proj_value, proj_gate, first_cotangent, first_hidden,
+        product, scratch=[taps_scratch], flops=100 * ROWS * WIDTH,
     )
     (pieces,) = call(
         pack, [((CLOSE, WIDTH + 2 * SMALL, BLOCK), NARROW)], mine, small, other, flops=1 << 20
     )
-    arrived = exchange(pieces, NEAR)
+    arrived = exchange(pieces, NEAR, NEAR_ORDER)
     (payload,) = call(
         fold_near, [((WIDTH + 2 * SMALL, BLOCK), NARROW)], arrived, flops=1 << 20
     )
@@ -446,10 +480,9 @@
     (message,) = call(hand_out, [((2 * CLOSE, OWN + SMALL, WIDTH), NARROW)], payload, flops=1 << 16)
     arrived = exchange(message, (*NEAR, "c"), GATHER_ORDER)
     (total,) = call(totals, [((OWN + SMALL, WIDTH), WIDE)], arrived, flops=1 << 20)
-    value_grad, gate_grad, weight_grad, taps_grad, gain_grad = call(
-        finish,
+    value_grad, gate_grad, weight_grad, taps_grad, gain_grad = last_call(
         [narrow, narrow, ((OWN, WIDTH), WIDE), ((TAPS, WIDTH), WIDE), ((1, WIDTH), WIDE)],
-        total, d_gated, late, proj_value, proj_gate, flops=10 * ROWS * WIDTH,
+        total, value_part, gate_part, last, late,
     )
     return (value_grad, gate_grad, weight_grad, taps_grad, gain_grad.reshape(WIDTH))
 
@@ -488,6 +521,38 @@
     )(scalar, *far, *args[in_hbm:])
 
 
+def load_call(*args):
+    held = [pltpu.with_memory_space_constraint(a, pltpu.HBM) for a in args]
+    shapes = [jax.ShapeDtypeStruct((EDGE, WIDTH), NARROW)]
+    shapes += [jax.ShapeDtypeStruct(a.shape, a.dtype) for a in args]
+    return pl.pallas_call(
+        load,
+        out_shape=shapes,
+        in_specs=[pl.BlockSpec(memory_space=pltpu.HBM)] * len(args),
+        out_specs=[pl.BlockSpec(memory_space=pltpu.VMEM)] * len(shapes),
+        scratch_shapes=[pltpu.SemaphoreType.DMA((len(args),))],
+        compiler_params=pltpu.CompilerParams(vmem_limit_bytes=6 << 20),
+        cost_estimate=pl.CostEstimate(flops=1 << 16, bytes_accessed=1 << 19, transcendentals=0),
+        name="load",
+    )(*held)
+
+
+def last_call(outs, *args):
+    edge = pltpu.VMEM((EDGE, WIDTH), NARROW)
+    return pl.pallas_call(
+        finish,
+        out_shape=[pltpu.HBM(*out) for out in outs],
+        in_specs=[pl.BlockSpec(memory_space=pltpu.VMEM)] * len(args),
+        out_specs=[pl.BlockSpec(memory_space=pltpu.HBM)] * len(outs),
+        scratch_shapes=[
+            edge, edge, pltpu.VMEM(*outs[3]), pltpu.VMEM(*outs[4]), pltpu.SemaphoreType.DMA((7,)),
+        ],
+        compiler_params=pltpu.CompilerParams(vmem_limit_bytes=6 << 20),
+        cost_estimate=pl.CostEstimate(flops=1 << 16, bytes_accessed=1 << 19, transcendentals=0),
+        name="finish",
+    )(*args)
+
+
 def solution(mesh):
     sizes = [size for _, size in AXES]
     split = Mesh(mesh.devices.reshape(*sizes, mesh.shape["tp"]), (*SP, "tp"))

time: 81.8 us -> 79.6 us (0.973)
  starting transfers between devices: 28.4 us -> 26.6 us
  Pallas kernels: 8.24 us -> 9.12 us
    all_to_all x1, starting transfers between devices: 8.61 us -> 6.3 us  [exchange(): lax.all_to_all(pieces, axes, 0, 0, tiled=True, axis_index_groups=groups)]
    pallas_call x0 -> x2, Pallas kernels: none -> 1.91 us  [the longest x1 1.1 us: load_call(): pl.pallas_call(load, out_shape=shapes, in_specs=[pl.BlockSpec(memory_spac...]
    pallas_call x5 -> x4, Pallas kernels: 1.94 us -> 1.06 us  [call(): pl.pallas_call(body, out_shape=shapes, compiler_params=pltpu.CompilerPara...]
    all_to_all x2, blocking collectives: 29.3 us -> 28.5 us  [exchange(): lax.all_to_all(pieces, axes, 0, 0, tiled=True, axis_index_groups=groups)]
where the time goes in v3:
time: 79.6 us; the launch traced here: 78.6 us
  blocking collectives  28.5 us (36%)
  starting transfers between devices  26.6 us (33%)
  waiting for transfers between devices  13.6 us (17%)
  Pallas kernels  9.12 us (11%)
    all_to_all x2, blocking collectives, exchange(): lax.all_to_all(pieces, axes, 0, 0, tiled=True, axis_index_groups=groups)  28.5 us
    ppermute x1, starting transfers between devices, to_block(): return lax.ppermute(value, SP, pairs)  12 us
    ppermute x1, waiting for transfers between devices, to_block(): return lax.ppermute(value, SP, pairs)  6.76 us
    ppermute x2, starting transfers between devices, shifted(): lax.ppermute(value, axis, [(source, source + steps) for source in range(f...  6.33 us
    all_to_all x1, waiting for transfers between devices, exchange(): lax.all_to_all(pieces, axes, 0, 0, tiled=True, axis_index_groups=groups)  6.33 us
    all_to_all x1, starting transfers between devices, exchange(): lax.all_to_all(pieces, axes, 0, 0, tiled=True, axis_index_groups=groups)  6.3 us
    pallas_call x3, Pallas kernels, scalar_call(): pl.pallas_call(body, out_shape=shapes, in_specs=[pl.BlockSpec(memory_spac...  5.94 us
    ppermute x1, starting transfers between devices, shards(): other = lax.ppermute(other, 'c', [(0, 1), (1, 0)])  1.92 us
  transfers between devices with their start and end apart: 5, of which 3 were waited for; matrix products, arithmetic and copies ran while one was open for 0% of the time, Pallas kernels for 6%

profile of v3, /device:TPU:7, one launch (start us, length us, event | category | flops | bytes accessed | tf_op | source)
XLA Modules:
  0.0 78.6 jit_solution(17192118257635428786)
XLA Ops:
  0.6 1.1 %load.1 = (bf16[32,256]{1,0:T(8,128)(2,1)S(1)}, bf16[384,256]{1,0:T(8,128)(2,1)S(1)}, bf16[384,256]{1,0:T(8,128)(2,1)S(1)}, bf16[31,256]{1,0:T(8,128)(2,1)S(1)},...) custom-call(bf16[384,256]{1,0:T(8,128)(2,1)} %value.1, bf16[384,256]{1,0:T(8,128)(2,1)} %gate.1, ...), custom_call_target="tpu_custom_call" | custom-call | flops 65536 | bytes 524288 | tf_op jit(solution)/shard_map/load/pallas_call | solution.py:528
  1.7 4.0 %collective-permute-start = (bf16[32,256]{1,0:T(8,128)(2,1)S(1)}, bf16[32,256]{1,0:T(8,128)(2,1)S(1)}, u32[]{:S(2)}, u32[]{:S(2)}) collective-permute-start(bf16[32,256]{1,0:T(8,128)(2,1)S(1)} %get-tuple-element.38), channel_id=1, source_target_pairs={{0,4},{4,8},{8,12},{12,16},{16,20},{20,24},{24,28},{28,32},{32,36}... | collective-permute-start | bytes 49160 | tf_op jit(solution)/shard_map/ppermute | solution.py:38
  5.8 3.1 %shard_map.119 = (bf16[384,256]{1,0:T(8,128)(2,1)S(1)}, f32[2,352,128]{2,1,0:T(8,128)S(1)}, f32[2,352,128]{2,1,0:T(8,128)S(1)}, f32[8,128]{1,0:T(8,128)S(1)}, f3...) custom-call(s32[1]{0:T(128)} %bitcast.place, ...), custom_call_target="tpu_custom_call" | custom-call | flops 805306368 | bytes 6225408 | tf_op jit(solution)/shard_map/pallas_call | solution.py:509
  8.8 0.0 collective-permute-done.halo
  8.8 0.2 shard_map.120
  9.1 6.7 %all_to_all.15.sums = f32[4,8,128]{2,1,0:T(8,128)S(1)} all-to-all(f32[4,8,128]{2,1,0:T(8,128)S(1)} %get-tuple-element.49), channel_id=1, replica_groups={{2,3,0,1},{6,7,4,5},{10,11,8,9},{14,15,12,13},{18,19,16,17},{22,23,20,2..., dimensions={0} | all-to-all | bytes 32768 | tf_op jit(solution)/shard_map/all_to_all | solution.py:43
  15.8 1.5 %shard_map.121 = (bf16[2176,128]{1,0:T(8,128)(2,1)S(1)}, f32[32,256]{1,0:T(8,128)S(1)}, f32[2,448,128]{2,1,0:T(8,128)S(1)}) custom-call(s32[1]{0:T(128)} %bitcast.place, f32[4,8,128]{2,1,0:T(8,128)S(1)} %all_to_all.15.sums, f32[2,352,128]{2,1,0:T(8,128)S(1)} %get-tuple-element.50.scaled, f32[2,352,128]{2,1,0:T(8,128)S(1)} %get-tuple-element.51.spread, ...), custom_call_target="tpu_custom_call" | custom-call | flops 9830400 | bytes 4318720 | tf_op jit(solution)/shard_map/pallas_call | solution.py:509
  17.3 1.9 %collective-permute-start.1 = (bf16[2176,128]{1,0:T(8,128)(2,1)S(1)}, bf16[2176,128]{1,0:T(8,128)(2,1)S(1)}, u32[]{:S(2)}, u32[]{:S(2)}) collective-permute-start(bf16[2176,128]{1,0:T(8,128)(2,1)S(1)} %get-tuple-element.61), channel_id=1, source_target_pairs={{0,4},{4,0},{1,5},{5,1},{2,6},{6,2},{3,7},{7,3},{8,12},{12,8},{9,1... | collective-permute-start | bytes 1671176 | tf_op jit(solution)/shard_map/ppermute | solution.py:463
  19.3 1.4 %shard_map.122 = (bf16[352,256]{1,0:T(8,128)(2,1)S(1)}, bf16[352,256]{1,0:T(8,128)(2,1)S(1)}, f32[2,32,128]{2,1,0:T(8,128)S(1)}, f32[3,2,32,128]{3,2,1,0:T(8,128)S(1)}, f32[8,256,128]{2,1,0:T(8,128)S(1)}) custom-call(s32[1]{0:T(128)} %bitcast.place, f32[2,448,128]{2,1,0:T(8,128)S(1)} %get-tuple-element.58.extended, ...), custom_call_target="tpu_custom_call" | custom-call | flops 9830400 | bytes 4652544 | tf_op jit(solution)/shard_map/pallas_call | solution.py:509
  20.6 0.6 collective-permute-done.1.other
  21.2 0.1 shard_map.123
  21.3 21.7 %all_to_all.16.arrived = bf16[8,320,128]{2,1,0:T(8,128)(2,1)S(1)} all-to-all(bf16[8,320,128]{2,1,0:T(8,128)(2,1)S(1)} %shard_map.123), channel_id=1, replica_groups={{32,40,48,56,0,8,16,24},{33,41,49,57,1,9,17,25},{34,42,50,58,2,10,18,26..., dimensions={0} | all-to-all | bytes 1310720 | tf_op jit(solution)/shard_map/all_to_all | solution.py:43
  43.0 0.1 shard_map.124
  43.1 12.0 %collective-permute-start.2 = (bf16[320,128]{1,0:T(8,128)(2,1)S(1)}, bf16[320,128]{1,0:T(8,128)(2,1)S(1)}, u32[]{:S(2)}, u32[]{:S(2)}) collective-permute-start(bf16[320,128]{1,0:T(8,128)(2,1)S(1)} %shard_map.124), channel_id=1, source_target_pairs={{0,0},{4,388},{8,968},{12,460},{16,912},{20,532},{24,856},{28,348}... | collective-permute-start | bytes 245768 | tf_op jit(solution)/shard_map/ppermute | solution.py:400
  55.1 6.8 %collective-permute-done.2.payload = bf16[320,128]{1,0:T(8,128)(2,1)S(1)} collective-permute-done((bf16[320,128]{1,0:T(8,128)(2,1)S(1)}, bf16[320,128]{1,0:T(8,128)(2,1)S(1)}, u32[]{:S(2)}, u32[]{:S(2)}) %collective-permute-start.2) | collective-permute-done | bytes 81952 | tf_op jit(solution)/shard_map/ppermute | solution.py:400
  61.9 0.8 %shard_map.125 = bf16[16,40,256]{2,1,0:T(8,128)(2,1)} custom-call(bf16[320,128]{1,0:T(8,128)(2,1)S(1)} %collective-permute-done.2.payload), custom_call_target="tpu_custom_call" | custom-call | flops 65536 | bytes 409600 | tf_op jit(solution)/shard_map/pallas_call | solution.py:57
  62.7 6.3 %all-to-all-start.2 = ((bf16[16,40,256]{2,1,0:T(8,128)(2,1)}), bf16[16,40,256]{2,1,0:T(8,128)(2,1)S(1)}, u32[]{:S(2)}, u32[]{:S(2)}) async-start(bf16[16,40,256]{2,1,0:T(8,128)(2,1)} %shard_map.125), calls=%async_computation.2 | async-start | bytes 655360 | tf_op jit(solution)/shard_map/all_to_all | solution.py:43
  69.0 2.3 %collective-permute-start.3 = (f32[2,32,128]{2,1,0:T(8,128)S(1)}, f32[2,32,128]{2,1,0:T(8,128)S(1)}, u32[]{:S(2)}, u32[]{:S(2)}) collective-permute-start(f32[2,32,128]{2,1,0:T(8,128)S(1)} %get-tuple-element.65), channel_id=1, source_target_pairs={{4,0},{8,4},{12,8},{16,12},{20,16},{24,20},{28,24},{32,28},{36,32}... | collective-permute-start | bytes 98312 | tf_op jit(solution)/shard_map/ppermute | solution.py:38
  71.4 6.3 %all-to-all-done.2.arrived = bf16[16,40,256]{2,1,0:T(8,128)(2,1)S(1)} async-done(((bf16[16,40,256]{2,1,0:T(8,128)(2,1)}), bf16[16,40,256]{2,1,0:T(8,128)(2,1)S(1)}, u32[]{:S(2)}, u32[]{:S(2)}) %all-to-all-start.2) | async-done | bytes 327712 | tf_op jit(solution)/shard_map/all_to_all | solution.py:43
  77.7 0.0 collective-permute-done.3.late
  77.7 0.8 %finish.1 = (bf16[384,256]{1,0:T(8,128)(2,1)}, bf16[384,256]{1,0:T(8,128)(2,1)}, f32[8,256]{1,0:T(8,128)}, f32[31,256]{1,0:T(8,128)}, f32[1,256]{1,0:T(1,128)}) custom-call(f32[40,256]{1,0:T(8,128)S(1)} %shard_map.126.total, bf16[352,256]{1,0:T(8,128)(2,1)S(1)} %get-tuple-element.62.value_part, bf16[352,256]{1,0:T(8,128)(2,1)S(1)} %get-tuple-element.63.gate_part, ...), custom_call_target="tpu_custom_call" | custom-call | flops 65536 | bytes 524288 | tf_op jit(solution)/shard_map/finish/pallas_call | solution.py:542
  (1 shorter events, 0.0 us)
Async XLA Ops:
  1.7 7.1 %collective-permute-start = (bf16[32,256]{1,0:T(8,128)(2,1)S(1)}, bf16[32,256]{1,0:T(8,128)(2,1)S(1)}, u32[]{:S(2)}, u32[]{:S(2)}) collective-permute-start(bf16[32,256]{1,0:T(8,128)(2,1)S(1)} %get-tuple-element.38), channel_id=1, source_target_pairs={{0,4},{4,8},{8,12},{12,16},{16,20},{20,24},{24,28},{28,32},{32,36}... | collective-permute-start | bytes 49160 | tf_op jit(solution)/shard_map/ppermute | solution.py:38
  17.3 3.9 %collective-permute-start.1 = (bf16[2176,128]{1,0:T(8,128)(2,1)S(1)}, bf16[2176,128]{1,0:T(8,128)(2,1)S(1)}, u32[]{:S(2)}, u32[]{:S(2)}) collective-permute-start(bf16[2176,128]{1,0:T(8,128)(2,1)S(1)} %get-tuple-element.61), channel_id=1, source_target_pairs={{0,4},{4,0},{1,5},{5,1},{2,6},{6,2},{3,7},{7,3},{8,12},{12,8},{9,1... | collective-permute-start | bytes 1671176 | tf_op jit(solution)/shard_map/ppermute | solution.py:463
  43.1 18.8 %collective-permute-start.2 = (bf16[320,128]{1,0:T(8,128)(2,1)S(1)}, bf16[320,128]{1,0:T(8,128)(2,1)S(1)}, u32[]{:S(2)}, u32[]{:S(2)}) collective-permute-start(bf16[320,128]{1,0:T(8,128)(2,1)S(1)} %shard_map.124), channel_id=1, source_target_pairs={{0,0},{4,388},{8,968},{12,460},{16,912},{20,532},{24,856},{28,348}... | collective-permute-start | bytes 245768 | tf_op jit(solution)/shard_map/ppermute | solution.py:400
  62.7 15.0 %all-to-all-start.2 = ((bf16[16,40,256]{2,1,0:T(8,128)(2,1)}), bf16[16,40,256]{2,1,0:T(8,128)(2,1)S(1)}, u32[]{:S(2)}, u32[]{:S(2)}) async-start(bf16[16,40,256]{2,1,0:T(8,128)(2,1)} %shard_map.125), calls=%async_computation.2 | async-start | bytes 655360 | tf_op jit(solution)/shard_map/all_to_all | solution.py:43
  69.0 8.7 %collective-permute-start.3 = (f32[2,32,128]{2,1,0:T(8,128)S(1)}, f32[2,32,128]{2,1,0:T(8,128)S(1)}, u32[]{:S(2)}, u32[]{:S(2)}) collective-permute-start(f32[2,32,128]{2,1,0:T(8,128)S(1)} %get-tuple-element.65), channel_id=1, source_target_pairs={{4,0},{8,4},{12,8},{16,12},{20,16},{24,20},{28,24},{32,28},{36,32}... | collective-permute-start | bytes 98312 | tf_op jit(solution)/shard_map/ppermute | solution.py:38

commit v4 on v3

--- a/solution.py
+++ b/solution.py
@@ -93,20 +93,30 @@
     return jnp.concatenate([cotangent[:, columns[0]], cotangent[:, columns[1]]], 1)
 
 
+def in_chunks(pairs, arrivals):
+    copies = []
+    for source, target, parts in pairs:
+        for part in range(parts):
+            if parts > 1:
+                size = source.shape[0] // parts
+                rows = pl.ds(part * size, size)
+                ends = source.at[rows], target.at[rows]
+            else:
+                ends = source, target
+            copies.append(pltpu.make_async_copy(*ends, arrivals.at[len(copies)]))
+    return copies
+
+
 def load(
     value, gate, taps, gain, mean, scale,
     end, held_value, held_gate, held_taps, held_gain, held_mean, held_scale,
     arrivals,
 ):
-    copies = [
-        pltpu.make_async_copy(source, target, arrivals.at[i])
-        for i, (source, target) in enumerate(
-            (
-                (value, held_value), (gate, held_gate), (taps, held_taps), (gain, held_gain),
-                (mean, held_mean), (scale, held_scale),
-            )
-        )
-    ]
+    pairs = (
+        (value, held_value, 3), (gate, held_gate, 3), (taps, held_taps, 1), (gain, held_gain, 1),
+        (mean, held_mean, 1), (scale, held_scale, 1),
+    )
+    copies = in_chunks(pairs, arrivals)
     for copy in copies:
         copy.start()
     for copy in copies:
@@ -123,12 +133,7 @@
     padded, taps_wide, mean_columns, scale_columns, sum_first, sum_second,
     hidden, normed, upstream,
 ):
-    copies = [
-        pltpu.make_async_copy(source, target, arrivals.at[i])
-        for i, (source, target) in enumerate(
-            ((weight, held_weight), (cotangent, held))
-        )
-    ]
+    copies = in_chunks(((weight, held_weight, 4), (cotangent, held, 6)), arrivals)
     for copy in copies:
         copy.start()
     sum_first[0:EDGE] = jnp.zeros((EDGE, LANES), WIDE)
@@ -426,7 +431,7 @@
             conv_taps, row_gain, row_mean, row_scale, in_hbm=2,
             scratch=[
                 pltpu.VMEM((ROWS, MODEL), NARROW), pltpu.VMEM((WIDTH, MODEL), NARROW),
-                pltpu.SemaphoreType.DMA((2,)),
+                pltpu.SemaphoreType.DMA((10,)),
                 sides, taps_scratch, *([pltpu.VMEM((ROWS, LANES), WIDE)] * 4),
                 pltpu.VMEM((ROWS, WIDTH), WIDE), pltpu.VMEM(split, WIDE),
                 pltpu.VMEM((ROWS, WIDTH), WIDE),
@@ -530,7 +535,7 @@
         out_shape=shapes,
         in_specs=[pl.BlockSpec(memory_space=pltpu.HBM)] * len(args),
         out_specs=[pl.BlockSpec(memory_space=pltpu.VMEM)] * len(shapes),
-        scratch_shapes=[pltpu.SemaphoreType.DMA((len(args),))],
+        scratch_shapes=[pltpu.SemaphoreType.DMA((10,))],
         compiler_params=pltpu.CompilerParams(vmem_limit_bytes=6 << 20),
         cost_estimate=pl.CostEstimate(flops=1 << 16, bytes_accessed=1 << 19, transcendentals=0),
         name="load",

time: 79.6 us -> 79.6 us (level)
  no operation moved by 1% of the time
where the time goes in v4:
time: 79.6 us; the launch traced here: 78.6 us
  blocking collectives  28.5 us (36%)
  starting transfers between devices  26.6 us (33%)
  waiting for transfers between devices  13.6 us (17%)
  Pallas kernels  9.14 us (11%)
    all_to_all x2, blocking collectives, exchange(): lax.all_to_all(pieces, axes, 0, 0, tiled=True, axis_index_groups=groups)  28.5 us
    ppermute x1, starting transfers between devices, to_block(): return lax.ppermute(value, SP, pairs)  12 us
    ppermute x1, waiting for transfers between devices, to_block(): return lax.ppermute(value, SP, pairs)  6.73 us
    ppermute x2, starting transfers between devices, shifted(): lax.ppermute(value, axis, [(source, source + steps) for source in range(f...  6.33 us
    all_to_all x1, waiting for transfers between devices, exchange(): lax.all_to_all(pieces, axes, 0, 0, tiled=True, axis_index_groups=groups)  6.33 us
    all_to_all x1, starting transfers between devices, exchange(): lax.all_to_all(pieces, axes, 0, 0, tiled=True, axis_index_groups=groups)  6.3 us
    pallas_call x3, Pallas kernels, scalar_call(): pl.pallas_call(body, out_shape=shapes, in_specs=[pl.BlockSpec(memory_spac...  5.95 us
    ppermute x1, starting transfers between devices, shards(): other = lax.ppermute(other, 'c', [(0, 1), (1, 0)])  1.92 us
  transfers between devices with their start and end apart: 5, of which 3 were waited for; matrix products, arithmetic and copies ran while one was open for 0% of the time, Pallas kernels for 6%

profile of v4, /device:TPU:7, one launch (start us, length us, event | category | flops | bytes accessed | tf_op | source)
XLA Modules:
  0.0 78.6 jit_solution(2469423057641026095)
XLA Ops:
  0.6 1.1 %load.1 = (bf16[32,256]{1,0:T(8,128)(2,1)S(1)}, bf16[384,256]{1,0:T(8,128)(2,1)S(1)}, bf16[384,256]{1,0:T(8,128)(2,1)S(1)}, bf16[31,256]{1,0:T(8,128)(2,1)S(1)},...) custom-call(bf16[384,256]{1,0:T(8,128)(2,1)} %value.1, bf16[384,256]{1,0:T(8,128)(2,1)} %gate.1, ...), custom_call_target="tpu_custom_call" | custom-call | flops 65536 | bytes 524288 | tf_op jit(solution)/shard_map/load/pallas_call | solution.py:533
  1.7 4.0 %collective-permute-start = (bf16[32,256]{1,0:T(8,128)(2,1)S(1)}, bf16[32,256]{1,0:T(8,128)(2,1)S(1)}, u32[]{:S(2)}, u32[]{:S(2)}) collective-permute-start(bf16[32,256]{1,0:T(8,128)(2,1)S(1)} %get-tuple-element.38), channel_id=1, source_target_pairs={{0,4},{4,8},{8,12},{12,16},{16,20},{20,24},{24,28},{28,32},{32,36}... | collective-permute-start | bytes 49160 | tf_op jit(solution)/shard_map/ppermute | solution.py:38
  5.8 3.1 %shard_map.119 = (bf16[384,256]{1,0:T(8,128)(2,1)S(1)}, f32[2,352,128]{2,1,0:T(8,128)S(1)}, f32[2,352,128]{2,1,0:T(8,128)S(1)}, f32[8,128]{1,0:T(8,128)S(1)}, f3...) custom-call(s32[1]{0:T(128)} %bitcast.place, ...), custom_call_target="tpu_custom_call" | custom-call | flops 805306368 | bytes 6225408 | tf_op jit(solution)/shard_map/pallas_call | solution.py:514
  8.9 0.0 collective-permute-done.halo
  8.9 0.2 shard_map.120
  9.1 6.7 %all_to_all.15.sums = f32[4,8,128]{2,1,0:T(8,128)S(1)} all-to-all(f32[4,8,128]{2,1,0:T(8,128)S(1)} %get-tuple-element.49), channel_id=1, replica_groups={{2,3,0,1},{6,7,4,5},{10,11,8,9},{14,15,12,13},{18,19,16,17},{22,23,20,2..., dimensions={0} | all-to-all | bytes 32768 | tf_op jit(solution)/shard_map/all_to_all | solution.py:43
  15.8 1.5 %shard_map.121 = (bf16[2176,128]{1,0:T(8,128)(2,1)S(1)}, f32[32,256]{1,0:T(8,128)S(1)}, f32[2,448,128]{2,1,0:T(8,128)S(1)}) custom-call(s32[1]{0:T(128)} %bitcast.place, f32[4,8,128]{2,1,0:T(8,128)S(1)} %all_to_all.15.sums, f32[2,352,128]{2,1,0:T(8,128)S(1)} %get-tuple-element.50.scaled, f32[2,352,128]{2,1,0:T(8,128)S(1)} %get-tuple-element.51.spread, ...), custom_call_target="tpu_custom_call" | custom-call | flops 9830400 | bytes 4318720 | tf_op jit(solution)/shard_map/pallas_call | solution.py:514
  17.4 1.9 %collective-permute-start.1 = (bf16[2176,128]{1,0:T(8,128)(2,1)S(1)}, bf16[2176,128]{1,0:T(8,128)(2,1)S(1)}, u32[]{:S(2)}, u32[]{:S(2)}) collective-permute-start(bf16[2176,128]{1,0:T(8,128)(2,1)S(1)} %get-tuple-element.61), channel_id=1, source_target_pairs={{0,4},{4,0},{1,5},{5,1},{2,6},{6,2},{3,7},{7,3},{8,12},{12,8},{9,1... | collective-permute-start | bytes 1671176 | tf_op jit(solution)/shard_map/ppermute | solution.py:468
  19.3 1.4 %shard_map.122 = (bf16[352,256]{1,0:T(8,128)(2,1)S(1)}, bf16[352,256]{1,0:T(8,128)(2,1)S(1)}, f32[2,32,128]{2,1,0:T(8,128)S(1)}, f32[3,2,32,128]{3,2,1,0:T(8,128)S(1)}, f32[8,256,128]{2,1,0:T(8,128)S(1)}) custom-call(s32[1]{0:T(128)} %bitcast.place, f32[2,448,128]{2,1,0:T(8,128)S(1)} %get-tuple-element.58.extended, ...), custom_call_target="tpu_custom_call" | custom-call | flops 9830400 | bytes 4652544 | tf_op jit(solution)/shard_map/pallas_call | solution.py:514
  20.7 0.6 collective-permute-done.1.other
  21.2 0.1 shard_map.123
  21.3 21.7 %all_to_all.16.arrived = bf16[8,320,128]{2,1,0:T(8,128)(2,1)S(1)} all-to-all(bf16[8,320,128]{2,1,0:T(8,128)(2,1)S(1)} %shard_map.123), channel_id=1, replica_groups={{32,40,48,56,0,8,16,24},{33,41,49,57,1,9,17,25},{34,42,50,58,2,10,18,26..., dimensions={0} | all-to-all | bytes 1310720 | tf_op jit(solution)/shard_map/all_to_all | solution.py:43
  43.0 0.1 shard_map.124
  43.1 12.0 %collective-permute-start.2 = (bf16[320,128]{1,0:T(8,128)(2,1)S(1)}, bf16[320,128]{1,0:T(8,128)(2,1)S(1)}, u32[]{:S(2)}, u32[]{:S(2)}) collective-permute-start(bf16[320,128]{1,0:T(8,128)(2,1)S(1)} %shard_map.124), channel_id=1, source_target_pairs={{0,0},{4,388},{8,968},{12,460},{16,912},{20,532},{24,856},{28,348}... | collective-permute-start | bytes 245768 | tf_op jit(solution)/shard_map/ppermute | solution.py:405
  55.2 6.7 %collective-permute-done.2.payload = bf16[320,128]{1,0:T(8,128)(2,1)S(1)} collective-permute-done((bf16[320,128]{1,0:T(8,128)(2,1)S(1)}, bf16[320,128]{1,0:T(8,128)(2,1)S(1)}, u32[]{:S(2)}, u32[]{:S(2)}) %collective-permute-start.2) | collective-permute-done | bytes 81952 | tf_op jit(solution)/shard_map/ppermute | solution.py:405
  61.9 0.8 %shard_map.125 = bf16[16,40,256]{2,1,0:T(8,128)(2,1)} custom-call(bf16[320,128]{1,0:T(8,128)(2,1)S(1)} %collective-permute-done.2.payload), custom_call_target="tpu_custom_call" | custom-call | flops 65536 | bytes 409600 | tf_op jit(solution)/shard_map/pallas_call | solution.py:57
  62.7 6.3 %all-to-all-start.2 = ((bf16[16,40,256]{2,1,0:T(8,128)(2,1)}), bf16[16,40,256]{2,1,0:T(8,128)(2,1)S(1)}, u32[]{:S(2)}, u32[]{:S(2)}) async-start(bf16[16,40,256]{2,1,0:T(8,128)(2,1)} %shard_map.125), calls=%async_computation.2 | async-start | bytes 655360 | tf_op jit(solution)/shard_map/all_to_all | solution.py:43
  69.0 2.3 %collective-permute-start.3 = (f32[2,32,128]{2,1,0:T(8,128)S(1)}, f32[2,32,128]{2,1,0:T(8,128)S(1)}, u32[]{:S(2)}, u32[]{:S(2)}) collective-permute-start(f32[2,32,128]{2,1,0:T(8,128)S(1)} %get-tuple-element.65), channel_id=1, source_target_pairs={{4,0},{8,4},{12,8},{16,12},{20,16},{24,20},{28,24},{32,28},{36,32}... | collective-permute-start | bytes 98312 | tf_op jit(solution)/shard_map/ppermute | solution.py:38
  71.4 6.3 %all-to-all-done.2.arrived = bf16[16,40,256]{2,1,0:T(8,128)(2,1)S(1)} async-done(((bf16[16,40,256]{2,1,0:T(8,128)(2,1)}), bf16[16,40,256]{2,1,0:T(8,128)(2,1)S(1)}, u32[]{:S(2)}, u32[]{:S(2)}) %all-to-all-start.2) | async-done | bytes 327712 | tf_op jit(solution)/shard_map/all_to_all | solution.py:43
  77.7 0.0 collective-permute-done.3.late
  77.8 0.8 %finish.1 = (bf16[384,256]{1,0:T(8,128)(2,1)}, bf16[384,256]{1,0:T(8,128)(2,1)}, f32[8,256]{1,0:T(8,128)}, f32[31,256]{1,0:T(8,128)}, f32[1,256]{1,0:T(1,128)}) custom-call(f32[40,256]{1,0:T(8,128)S(1)} %shard_map.126.total, bf16[352,256]{1,0:T(8,128)(2,1)S(1)} %get-tuple-element.62.value_part, bf16[352,256]{1,0:T(8,128)(2,1)S(1)} %get-tuple-element.63.gate_part, ...), custom_call_target="tpu_custom_call" | custom-call | flops 65536 | bytes 524288 | tf_op jit(solution)/shard_map/finish/pallas_call | solution.py:547
  (1 shorter events, 0.0 us)
Async XLA Ops:
  1.7 7.1 %collective-permute-start = (bf16[32,256]{1,0:T(8,128)(2,1)S(1)}, bf16[32,256]{1,0:T(8,128)(2,1)S(1)}, u32[]{:S(2)}, u32[]{:S(2)}) collective-permute-start(bf16[32,256]{1,0:T(8,128)(2,1)S(1)} %get-tuple-element.38), channel_id=1, source_target_pairs={{0,4},{4,8},{8,12},{12,16},{16,20},{20,24},{24,28},{28,32},{32,36}... | collective-permute-start | bytes 49160 | tf_op jit(solution)/shard_map/ppermute | solution.py:38
  17.4 3.9 %collective-permute-start.1 = (bf16[2176,128]{1,0:T(8,128)(2,1)S(1)}, bf16[2176,128]{1,0:T(8,128)(2,1)S(1)}, u32[]{:S(2)}, u32[]{:S(2)}) collective-permute-start(bf16[2176,128]{1,0:T(8,128)(2,1)S(1)} %get-tuple-element.61), channel_id=1, source_target_pairs={{0,4},{4,0},{1,5},{5,1},{2,6},{6,2},{3,7},{7,3},{8,12},{12,8},{9,1... | collective-permute-start | bytes 1671176 | tf_op jit(solution)/shard_map/ppermute | solution.py:468
  43.1 18.8 %collective-permute-start.2 = (bf16[320,128]{1,0:T(8,128)(2,1)S(1)}, bf16[320,128]{1,0:T(8,128)(2,1)S(1)}, u32[]{:S(2)}, u32[]{:S(2)}) collective-permute-start(bf16[320,128]{1,0:T(8,128)(2,1)S(1)} %shard_map.124), channel_id=1, source_target_pairs={{0,0},{4,388},{8,968},{12,460},{16,912},{20,532},{24,856},{28,348}... | collective-permute-start | bytes 245768 | tf_op jit(solution)/shard_map/ppermute | solution.py:405
  62.7 15.0 %all-to-all-start.2 = ((bf16[16,40,256]{2,1,0:T(8,128)(2,1)}), bf16[16,40,256]{2,1,0:T(8,128)(2,1)S(1)}, u32[]{:S(2)}, u32[]{:S(2)}) async-start(bf16[16,40,256]{2,1,0:T(8,128)(2,1)} %shard_map.125), calls=%async_computation.2 | async-start | bytes 655360 | tf_op jit(solution)/shard_map/all_to_all | solution.py:43
  69.0 8.7 %collective-permute-start.3 = (f32[2,32,128]{2,1,0:T(8,128)S(1)}, f32[2,32,128]{2,1,0:T(8,128)S(1)}, u32[]{:S(2)}, u32[]{:S(2)}) collective-permute-start(f32[2,32,128]{2,1,0:T(8,128)S(1)} %get-tuple-element.65), channel_id=1, source_target_pairs={{4,0},{8,4},{12,8},{16,12},{20,16},{24,20},{28,24},{32,28},{36,32}... | collective-permute-start | bytes 98312 | tf_op jit(solution)/shard_map/ppermute | solution.py:38

commit v5 on v3

--- a/solution.py
+++ b/solution.py
@@ -84,49 +84,36 @@
     return jnp.sum(jnp.transpose(source), 0, keepdims=True)
 
 
-def both_blocks(cotangent, place, near):
+def block_columns(place, near, side):
     far, core = place[0] // (2 * CLOSE), place[0] % 2
     low, high = OFFSETS[0][near], OFFSETS[1][near]
-    own = lax.rem(far + jnp.where(core == 0, low, high) + FAR, FAR)
-    theirs = lax.rem(far + jnp.where(core == 0, high, low) + FAR, FAR)
-    columns = [pl.ds(pl.multiple_of(block * BLOCK, BLOCK), BLOCK) for block in (own, theirs)]
-    return jnp.concatenate([cotangent[:, columns[0]], cotangent[:, columns[1]]], 1)
-
-
-def load(
-    value, gate, taps, gain, mean, scale,
-    end, held_value, held_gate, held_taps, held_gain, held_mean, held_scale,
-    arrivals,
+    step = jnp.where(core == side, low, high)
+    block = lax.rem(far + step + FAR, FAR)
+    return pl.ds(pl.multiple_of(block * BLOCK, BLOCK), BLOCK)
+
+
+def main_product(turned, cotangent, place, side, product):
+    for near in range(0, CLOSE, 2):
+        pair = [cotangent[:, block_columns(place, near + i, side)] for i in range(2)]
+        both = jnp.dot(turned, jnp.concatenate(pair, 1), preferred_element_type=WIDE)
+        for i in range(2):
+            product[near + i] = both[:, i * BLOCK : (i + 1) * BLOCK]
+
+
+def forward(
+    place, value, gate, cotangent, weight, far_taps, far_gain, far_mean, far_scale,
+    gated, scaled, spread, sums, gain_part, first_upstream, held, across, product,
+    held_value, held_gate, held_weight, taps, gain, mean, scale, arrivals,
+    padded, taps_wide, mean_columns, scale_columns, sum_first, sum_second,
+    hidden, normed, upstream,
 ):
     copies = [
         pltpu.make_async_copy(source, target, arrivals.at[i])
         for i, (source, target) in enumerate(
             (
-                (value, held_value), (gate, held_gate), (taps, held_taps), (gain, held_gain),
-                (mean, held_mean), (scale, held_scale),
+                (value, held_value), (gate, held_gate), (far_taps, taps), (far_mean, mean),
+                (far_scale, scale), (far_gain, gain), (weight, held_weight), (cotangent, held),
             )
-        )
-    ]
-    for copy in copies:
-        copy.start()
-    for copy in copies:
-        copy.wait()
-    rows = slice(ROWS - EDGE, ROWS)
-    sig = jax.nn.sigmoid(held_gate[rows].astype(WIDE))
-    end[...] = (held_value[rows].astype(WIDE) * sig).astype(NARROW)
-
-
-def forward(
-    place, cotangent, weight, held_value, held_gate, taps, gain, mean, scale,
-    gated, scaled, spread, sums, gain_part, first_upstream, first_cotangent, product,
-    held, held_weight, arrivals,
-    padded, taps_wide, mean_columns, scale_columns, sum_first, sum_second,
-    hidden, normed, upstream,
-):
-    copies = [
-        pltpu.make_async_copy(source, target, arrivals.at[i])
-        for i, (source, target) in enumerate(
-            ((weight, held_weight), (cotangent, held))
         )
     ]
     for copy in copies:
@@ -134,6 +121,8 @@
     sum_first[0:EDGE] = jnp.zeros((EDGE, LANES), WIDE)
     sum_second[0:EDGE] = jnp.zeros((EDGE, LANES), WIDE)
     hidden[0:EDGE] = jnp.zeros((EDGE, WIDTH), WIDE)
+    for copy in copies[:6]:
+        copy.wait()
     taps_wide[0:TAPS] = taps[...].astype(WIDE)
     for block in range(ROWS // LANES):
         rows = slice(block * LANES, (block + 1) * LANES)
@@ -150,13 +139,12 @@
             rows = slice(start, start + EDGE)
             conv = convolve(padded, half, taps_wide, start, EDGE)
             normed[half, rows] = (conv - mean_columns[rows]) * scale_columns[rows]
-    for copy in copies:
-        copy.wait()
+    copies[6].wait()
+    copies[7].wait()
     upstream[...] = lax.dot_general(
         held[...], held_weight[...], (((1,), (1,)), ((), ())), preferred_element_type=WIDE
     )
     first_upstream[...] = upstream[0:EDGE]
-    first_cotangent[...] = held[0:EDGE]
     for half in range(HALVES):
         gain_row = gain[0:1, lanes(half)]
         gain_sum = jnp.zeros((8, LANES), WIDE)
@@ -182,11 +170,8 @@
         for block in range(ROWS // LANES)
     ]
     sums[...] = jnp.concatenate([*found, jnp.zeros((2, LANES), WIDE)], 0)
-    turned = jnp.transpose(hidden[...]).astype(NARROW)
-    for near in range(CLOSE):
-        product[near] = jnp.dot(
-            turned, both_blocks(held, place, near), preferred_element_type=WIDE
-        )
+    across[...] = jnp.transpose(hidden[...]).astype(NARROW)
+    main_product(across[...], held, place, 1, product)
 
 
 def head(
@@ -225,7 +210,7 @@
 
 
 def head_product(cotangent, hidden, place, near, side):
-    columns = both_blocks(cotangent, place, near)[:, side * BLOCK : (side + 1) * BLOCK]
+    columns = cotangent[0:EDGE, block_columns(place, near, side)]
     return lax.dot_general(
         hidden[...], columns, (((0,), (0,)), ((), ())), preferred_element_type=WIDE
     )
@@ -233,7 +218,7 @@
 
 def backward(
     place, sums, scaled, spread, first_scaled, first_spread, halo, gated, scale, gain_part,
-    first_cotangent, first_hidden, product,
+    cotangent, first_hidden, product,
     other, small, extended,
     padded,
 ):
@@ -279,9 +264,7 @@
                 tap = 8 * q + offset - lead
                 small[tap : tap + 1, lanes(half)] = jnp.sum(found[half, q], 0, keepdims=True)
         near = offset
-        whole = product[near, :, BLOCK:] + head_product(
-            first_cotangent, first_hidden, place, near, 1
-        )
+        whole = product[near] + head_product(cotangent, first_hidden, place, near, 1)
         other[near * WIDTH : (near + 1) * WIDTH] = whole.astype(NARROW)
     for half in range(HALVES):
         small[TAPS:SMALL, lanes(half)] = jnp.sum(gain_part[half], 0, keepdims=True)
@@ -309,14 +292,13 @@
 
 
 def gated_gradient(
-    place, extended, taps, value, gate, first_cotangent, first_hidden, product,
+    place, extended, taps, value, gate, cotangent, first_hidden, across,
     value_grad, gate_grad, margin, last, mine,
     taps_wide,
 ):
+    main_product(across[...], cotangent, place, 0, mine)
     for near in range(CLOSE):
-        mine[near] = product[near, :, 0:BLOCK] + head_product(
-            first_cotangent, first_hidden, place, near, 0
-        )
+        mine[near] = mine[near] + head_product(cotangent, first_hidden, place, near, 0)
     taps_wide[0:TAPS] = taps[...].astype(WIDE)
     for half in range(HALVES):
         for start in range(0, EDGE + ROWS, EDGE):
@@ -403,30 +385,31 @@
 def shards(
     proj_value, proj_gate, out_cotangent, out_weight, conv_taps, norm_gain, row_mean, row_scale
 ):
-    row_gain = norm_gain.reshape(1, WIDTH)
-    end, proj_value, proj_gate, conv_taps, row_gain, row_mean, row_scale = load_call(
-        proj_value, proj_gate, conv_taps, row_gain, row_mean, row_scale
-    )
+    end_gate = jax.nn.sigmoid(proj_gate[ROWS - EDGE :].astype(WIDE))
+    end = (proj_value[ROWS - EDGE :].astype(WIDE) * end_gate).astype(NARROW)
     halo = shifted(end, SP, 1)
     split = (HALVES, ROWS, LANES)
     rest = (HALVES, ROWS - EDGE, LANES)
+    row_gain = norm_gain.reshape(1, WIDTH)
     sides = pltpu.VMEM((HALVES, EDGE + ROWS, LANES), WIDE)
     taps_scratch = pltpu.VMEM((TAPS + 1, WIDTH), WIDE)
     place = lax.axis_index(SP).reshape(1)
     narrow = ((ROWS, WIDTH), NARROW)
-    gated, scaled, spread, sums, gain_part, first_upstream, first_cotangent, product = (
+    gated, scaled, spread, sums, gain_part, first_upstream, cotangent, across, product = (
         scalar_call(
             forward,
             [
                 narrow, (rest, WIDE), (rest, WIDE), ((8, LANES), WIDE),
-                ((HALVES, 8, LANES), WIDE), ((EDGE, WIDTH), WIDE), ((EDGE, MODEL), NARROW),
-                ((CLOSE, WIDTH, 2 * BLOCK), WIDE),
+                ((HALVES, 8, LANES), WIDE), ((EDGE, WIDTH), WIDE), ((ROWS, MODEL), NARROW),
+                ((WIDTH, ROWS), NARROW), ((CLOSE, WIDTH, BLOCK), WIDE),
             ],
-            place, out_cotangent, out_weight, proj_value, proj_gate,
-            conv_taps, row_gain, row_mean, row_scale, in_hbm=2,
+            place, proj_value, proj_gate, out_cotangent, out_weight,
+            conv_taps, row_gain, row_mean, row_scale, in_hbm=8,
             scratch=[
-                pltpu.VMEM((ROWS, MODEL), NARROW), pltpu.VMEM((WIDTH, MODEL), NARROW),
-                pltpu.SemaphoreType.DMA((2,)),
+                pltpu.VMEM(*narrow), pltpu.VMEM(*narrow),
+                pltpu.VMEM((WIDTH, MODEL), NARROW), pltpu.VMEM((TAPS, WIDTH), NARROW),
+                pltpu.VMEM((1, WIDTH), WIDE), pltpu.VMEM((ROWS,), WIDE),
+                pltpu.VMEM((ROWS,), WIDE), pltpu.SemaphoreType.DMA((8,)),
                 sides, taps_scratch, *([pltpu.VMEM((ROWS, LANES), WIDE)] * 4),
                 pltpu.VMEM((ROWS, WIDTH), WIDE), pltpu.VMEM(split, WIDE),
                 pltpu.VMEM((ROWS, WIDTH), WIDE),
@@ -458,15 +441,15 @@
             ((HALVES, ROWS + 2 * EDGE, LANES), WIDE),
         ],
         place, sums, scaled, spread, first_scaled, first_spread, halo, gated, row_scale, gain_part,
-        first_cotangent, first_hidden, product, scratch=[sides], flops=100 * ROWS * WIDTH,
+        cotangent, first_hidden, product, scratch=[sides], flops=100 * ROWS * WIDTH,
     )
     other = lax.ppermute(other, "c", [(0, 1), (1, 0)])
     main = ((ROWS - EDGE, WIDTH), NARROW)
     value_part, gate_part, margin, last, mine = scalar_call(
         gated_gradient,
         [main, main, (edge, WIDE), ((3, *edge), WIDE), ((CLOSE, WIDTH, BLOCK), WIDE)],
-        place, extended, conv_taps, proj_value, proj_gate, first_cotangent, first_hidden,
-        product, scratch=[taps_scratch], flops=100 * ROWS * WIDTH,
+        place, extended, conv_taps, proj_value, proj_gate, cotangent, first_hidden,
+        across, scratch=[taps_scratch], flops=100 * ROWS * WIDTH,
     )
     (pieces,) = call(
         pack, [((CLOSE, WIDTH + 2 * SMALL, BLOCK), NARROW)], mine, small, other, flops=1 << 20
@@ -521,22 +504,6 @@
     )(scalar, *far, *args[in_hbm:])
 
 
-def load_call(*args):
-    held = [pltpu.with_memory_space_constraint(a, pltpu.HBM) for a in args]
-    shapes = [jax.ShapeDtypeStruct((EDGE, WIDTH), NARROW)]
-    shapes += [jax.ShapeDtypeStruct(a.shape, a.dtype) for a in args]
-    return pl.pallas_call(
-        load,
-        out_shape=shapes,
-        in_specs=[pl.BlockSpec(memory_space=pltpu.HBM)] * len(args),
-        out_specs=[pl.BlockSpec(memory_space=pltpu.VMEM)] * len(shapes),
-        scratch_shapes=[pltpu.SemaphoreType.DMA((len(args),))],
-        compiler_params=pltpu.CompilerParams(vmem_limit_bytes=6 << 20),
-        cost_estimate=pl.CostEstimate(flops=1 << 16, bytes_accessed=1 << 19, transcendentals=0),
-        name="load",
-    )(*held)
-
-
 def last_call(outs, *args):
     edge = pltpu.VMEM((EDGE, WIDTH), NARROW)
     return pl.pallas_call(

time: 79.6 us -> 79.8 us (level)
    pallas_call x1 -> x0, Pallas kernels: 1.1 us -> none  [load_call(): pl.pallas_call(load, out_shape=shapes, in_specs=[pl.BlockSpec(memory_spac...]
where the time goes in v5:
time: 79.8 us; the launch traced here: 78.8 us
  blocking collectives  28.8 us (36%)
  starting transfers between devices  26.2 us (33%)
  waiting for transfers between devices  13.8 us (17%)
  Pallas kernels  8.43 us (11%)
  between operations  0.81 us (1%)
    all_to_all x2, blocking collectives, exchange(): lax.all_to_all(pieces, axes, 0, 0, tiled=True, axis_index_groups=groups)  28.8 us
    ppermute x1, starting transfers between devices, to_block(): return lax.ppermute(value, SP, pairs)  11.4 us
    ppermute x1, waiting for transfers between devices, to_block(): return lax.ppermute(value, SP, pairs)  7.2 us
    all_to_all x1, starting transfers between devices, exchange(): lax.all_to_all(pieces, axes, 0, 0, tiled=True, axis_index_groups=groups)  6.47 us
    pallas_call x3, Pallas kernels, scalar_call(): pl.pallas_call(body, out_shape=shapes, in_specs=[pl.BlockSpec(memory_spac...  6.35 us
    ppermute x2, starting transfers between devices, shifted(): lax.ppermute(value, axis, [(source, source + steps) for source in range(f...  6.33 us
    all_to_all x1, waiting for transfers between devices, exchange(): lax.all_to_all(pieces, axes, 0, 0, tiled=True, axis_index_groups=groups)  6.33 us
    ppermute x1, starting transfers between devices, shards(): other = lax.ppermute(other, 'c', [(0, 1), (1, 0)])  1.92 us
  transfers between devices with their start and end apart: 5, of which 3 were waited for; matrix products, arithmetic and copies ran while one was open for 0% of the time, Pallas kernels for 6%

profile of v5, /device:TPU:7, one launch (start us, length us, event | category | flops | bytes accessed | tf_op | source)
XLA Modules:
  0.0 78.8 jit_solution(6973061320933123429)
XLA Ops:
  0.6 0.0 copy-start.3
  0.6 0.0 copy-start.2
  0.7 0.0 copy-start.4
  0.7 0.0 copy-start.5
  0.7 0.8 multiply_convert_fusion
  1.5 4.0 %collective-permute-start = (bf16[32,256]{1,0:T(8,128)(2,1)S(1)}, bf16[32,256]{1,0:T(8,128)(2,1)S(1)}, u32[]{:S(2)}, u32[]{:S(2)}) collective-permute-start(bf16[32,256]{1,0:T(8,128)(2,1)S(1)} %multiply_convert_fusion), channel_id=1, source_target_pairs={{0,4},{4,8},{8,12},{12,16},{16,20},{20,24},{24,28},{28,32},{32,36}... | collective-permute-start | bytes 49160 | tf_op jit(solution)/shard_map/ppermute | solution.py:38
  5.5 3.2 %shard_map.119 = (bf16[384,256]{1,0:T(8,128)(2,1)S(1)}, f32[2,352,128]{2,1,0:T(8,128)S(1)}, f32[2,352,128]{2,1,0:T(8,128)S(1)}, f32[8,128]{1,0:T(8,128)S(1)}, f3...) custom-call(s32[1]{0:T(128)} %bitcast.place, ...), custom_call_target="tpu_custom_call" | custom-call | flops 805306368 | bytes 6815232 | tf_op jit(solution)/shard_map/pallas_call | solution.py:492
  8.7 0.0 collective-permute-done.halo
  8.7 0.0 copy-done.3
  8.7 0.0 copy-done.2
  8.7 0.0 copy-done.4
  8.7 0.0 copy-done.5
  8.8 0.2 shard_map.120
  9.0 6.7 %all_to_all.15.sums = f32[4,8,128]{2,1,0:T(8,128)S(1)} all-to-all(f32[4,8,128]{2,1,0:T(8,128)S(1)} %get-tuple-element.36), channel_id=1, replica_groups={{2,3,0,1},{6,7,4,5},{10,11,8,9},{14,15,12,13},{18,19,16,17},{22,23,20,2..., dimensions={0} | all-to-all | bytes 32768 | tf_op jit(solution)/shard_map/all_to_all | solution.py:43
  15.7 0.0 copy-start
  15.7 0.0 copy-start.1
  15.7 1.5 %shard_map.121 = (bf16[2176,128]{1,0:T(8,128)(2,1)S(1)}, f32[32,256]{1,0:T(8,128)S(1)}, f32[2,448,128]{2,1,0:T(8,128)S(1)}) custom-call(s32[1]{0:T(128)} %bitcast.place, f32[4,8,128]{2,1,0:T(8,128)S(1)} %all_to_all.15.sums, f32[2,352,128]{2,1,0:T(8,128)S(1)} %get-tuple-element.37.scaled, f32[2,352,128]{2,1,0:T(8,128)S(1)} %get-tuple-element.38.spread, ...), custom_call_target="tpu_custom_call" | custom-call | flops 9830400 | bytes 4711936 | tf_op jit(solution)/shard_map/pallas_call | solution.py:492
  17.2 1.9 %collective-permute-start.1 = (bf16[2176,128]{1,0:T(8,128)(2,1)S(1)}, bf16[2176,128]{1,0:T(8,128)(2,1)S(1)}, u32[]{:S(2)}, u32[]{:S(2)}) collective-permute-start(bf16[2176,128]{1,0:T(8,128)(2,1)S(1)} %get-tuple-element.49), channel_id=1, source_target_pairs={{0,4},{4,0},{1,5},{5,1},{2,6},{6,2},{3,7},{7,3},{8,12},{12,8},{9,1... | collective-permute-start | bytes 1671176 | tf_op jit(solution)/shard_map/ppermute | solution.py:446
  19.1 0.0 copy-done
  19.1 0.0 copy-done.1
  19.2 1.7 %shard_map.122 = (bf16[352,256]{1,0:T(8,128)(2,1)S(1)}, bf16[352,256]{1,0:T(8,128)(2,1)S(1)}, f32[2,32,128]{2,1,0:T(8,128)S(1)}, f32[3,2,32,128]{3,2,1,0:T(8,128)S(1)}, f32[8,256,128]{2,1,0:T(8,128)S(1)}) custom-call(s32[1]{0:T(128)} %bitcast.place, f32[2,448,128]{2,1,0:T(8,128)S(1)} %get-tuple-element.45.extended, bf16[31,256]{1,0:T(8,128)(2,1)S(1)} %copy-done.2, ...), custom_call_target="tpu_custom_call" | custom-call | flops 9830400 | bytes 4193792 | tf_op jit(solution)/shard_map/pallas_call | solution.py:492
  20.8 0.2 collective-permute-done.1.other
  21.1 0.1 shard_map.123
  21.2 22.0 %all_to_all.16.arrived = bf16[8,320,128]{2,1,0:T(8,128)(2,1)S(1)} all-to-all(bf16[8,320,128]{2,1,0:T(8,128)(2,1)S(1)} %shard_map.123), channel_id=1, replica_groups={{32,40,48,56,0,8,16,24},{33,41,49,57,1,9,17,25},{34,42,50,58,2,10,18,26..., dimensions={0} | all-to-all | bytes 1310720 | tf_op jit(solution)/shard_map/all_to_all | solution.py:43
  43.2 0.1 shard_map.124
  43.3 11.4 %collective-permute-start.2 = (bf16[320,128]{1,0:T(8,128)(2,1)S(1)}, bf16[320,128]{1,0:T(8,128)(2,1)S(1)}, u32[]{:S(2)}, u32[]{:S(2)}) collective-permute-start(bf16[320,128]{1,0:T(8,128)(2,1)S(1)} %shard_map.124), channel_id=1, source_target_pairs={{0,0},{4,388},{8,968},{12,460},{16,912},{20,532},{24,856},{28,348}... | collective-permute-start | bytes 245768 | tf_op jit(solution)/shard_map/ppermute | solution.py:382
  54.7 7.2 %collective-permute-done.2.payload = bf16[320,128]{1,0:T(8,128)(2,1)S(1)} collective-permute-done((bf16[320,128]{1,0:T(8,128)(2,1)S(1)}, bf16[320,128]{1,0:T(8,128)(2,1)S(1)}, u32[]{:S(2)}, u32[]{:S(2)}) %collective-permute-start.2) | collective-permute-done | bytes 81952 | tf_op jit(solution)/shard_map/ppermute | solution.py:382
  61.9 0.8 %shard_map.125 = bf16[16,40,256]{2,1,0:T(8,128)(2,1)} custom-call(bf16[320,128]{1,0:T(8,128)(2,1)S(1)} %collective-permute-done.2.payload), custom_call_target="tpu_custom_call" | custom-call | flops 65536 | bytes 409600 | tf_op jit(solution)/shard_map/pallas_call | solution.py:57
  62.8 6.5 %all-to-all-start.2 = ((bf16[16,40,256]{2,1,0:T(8,128)(2,1)}), bf16[16,40,256]{2,1,0:T(8,128)(2,1)S(1)}, u32[]{:S(2)}, u32[]{:S(2)}) async-start(bf16[16,40,256]{2,1,0:T(8,128)(2,1)} %shard_map.125), calls=%async_computation.2 | async-start | bytes 655360 | tf_op jit(solution)/shard_map/all_to_all | solution.py:43
  69.2 2.3 %collective-permute-start.3 = (f32[2,32,128]{2,1,0:T(8,128)S(1)}, f32[2,32,128]{2,1,0:T(8,128)S(1)}, u32[]{:S(2)}, u32[]{:S(2)}) collective-permute-start(f32[2,32,128]{2,1,0:T(8,128)S(1)} %get-tuple-element.53), channel_id=1, source_target_pairs={{4,0},{8,4},{12,8},{16,12},{20,16},{24,20},{28,24},{32,28},{36,32}... | collective-permute-start | bytes 98312 | tf_op jit(solution)/shard_map/ppermute | solution.py:38
  71.6 6.3 %all-to-all-done.2.arrived = bf16[16,40,256]{2,1,0:T(8,128)(2,1)S(1)} async-done(((bf16[16,40,256]{2,1,0:T(8,128)(2,1)}), bf16[16,40,256]{2,1,0:T(8,128)(2,1)S(1)}, u32[]{:S(2)}, u32[]{:S(2)}) %all-to-all-start.2) | async-done | bytes 327712 | tf_op jit(solution)/shard_map/all_to_all | solution.py:43
  77.9 0.0 collective-permute-done.3.late
  78.0 0.8 %finish.1 = (bf16[384,256]{1,0:T(8,128)(2,1)}, bf16[384,256]{1,0:T(8,128)(2,1)}, f32[8,256]{1,0:T(8,128)}, f32[31,256]{1,0:T(8,128)}, f32[1,256]{1,0:T(1,128)}) custom-call(f32[40,256]{1,0:T(8,128)S(1)} %shard_map.126.total, bf16[352,256]{1,0:T(8,128)(2,1)S(1)} %get-tuple-element.50.value_part, bf16[352,256]{1,0:T(8,128)(2,1)S(1)} %get-tuple-element.51.gate_part, ...), custom_call_target="tpu_custom_call" | custom-call | flops 65536 | bytes 524288 | tf_op jit(solution)/shard_map/finish/pallas_call | solution.py:509
  (1 shorter events, 0.0 us)
Async XLA Ops:
  0.6 8.1 %copy-start.3 = (f32[384]{0:T(512)S(1)}, f32[384]{0:T(512)}, u32[]{:S(2)}) copy-start(f32[384]{0:T(512)} %scale.3) | copy-start | bytes 4612
  0.6 8.1 %copy-start.2 = (bf16[31,256]{1,0:T(8,128)(2,1)S(1)}, bf16[31,256]{1,0:T(8,128)(2,1)}, u32[]{:S(2)}) copy-start(bf16[31,256]{1,0:T(8,128)(2,1)} %taps.3) | copy-start | bytes 47620
  0.7 8.1 %copy-start.4 = (f32[384]{0:T(512)S(1)}, f32[384]{0:T(512)}, u32[]{:S(2)}) copy-start(f32[384]{0:T(512)} %mean.1) | copy-start | bytes 4612
  0.7 8.1 %copy-start.5 = (f32[256]{0:T(256)S(1)}, f32[256]{0:T(256)}, u32[]{:S(2)}) copy-start(f32[256]{0:T(256)} %param.13) | copy-start | bytes 3076
  1.5 7.3 %collective-permute-start = (bf16[32,256]{1,0:T(8,128)(2,1)S(1)}, bf16[32,256]{1,0:T(8,128)(2,1)S(1)}, u32[]{:S(2)}, u32[]{:S(2)}) collective-permute-start(bf16[32,256]{1,0:T(8,128)(2,1)S(1)} %multiply_convert_fusion), channel_id=1, source_target_pairs={{0,4},{4,8},{8,12},{12,16},{16,20},{20,24},{24,28},{28,32},{32,36}... | collective-permute-start | bytes 49160 | tf_op jit(solution)/shard_map/ppermute | solution.py:38
  15.7 3.4 %copy-start = (bf16[384,256]{1,0:T(8,128)(2,1)S(1)}, bf16[384,256]{1,0:T(8,128)(2,1)}, u32[]{:S(2)}) copy-start(bf16[384,256]{1,0:T(8,128)(2,1)} %gate.3) | copy-start | bytes 589828
  15.7 3.4 %copy-start.1 = (bf16[384,256]{1,0:T(8,128)(2,1)S(1)}, bf16[384,256]{1,0:T(8,128)(2,1)}, u32[]{:S(2)}) copy-start(bf16[384,256]{1,0:T(8,128)(2,1)} %value.3) | copy-start | bytes 589828
  17.2 3.9 %collective-permute-start.1 = (bf16[2176,128]{1,0:T(8,128)(2,1)S(1)}, bf16[2176,128]{1,0:T(8,128)(2,1)S(1)}, u32[]{:S(2)}, u32[]{:S(2)}) collective-permute-start(bf16[2176,128]{1,0:T(8,128)(2,1)S(1)} %get-tuple-element.49), channel_id=1, source_target_pairs={{0,4},{4,0},{1,5},{5,1},{2,6},{6,2},{3,7},{7,3},{8,12},{12,8},{9,1... | collective-permute-start | bytes 1671176 | tf_op jit(solution)/shard_map/ppermute | solution.py:446
  43.3 18.7 %collective-permute-start.2 = (bf16[320,128]{1,0:T(8,128)(2,1)S(1)}, bf16[320,128]{1,0:T(8,128)(2,1)S(1)}, u32[]{:S(2)}, u32[]{:S(2)}) collective-permute-start(bf16[320,128]{1,0:T(8,128)(2,1)S(1)} %shard_map.124), channel_id=1, source_target_pairs={{0,0},{4,388},{8,968},{12,460},{16,912},{20,532},{24,856},{28,348}... | collective-permute-start | bytes 245768 | tf_op jit(solution)/shard_map/ppermute | solution.py:382
  62.8 15.1 %all-to-all-start.2 = ((bf16[16,40,256]{2,1,0:T(8,128)(2,1)}), bf16[16,40,256]{2,1,0:T(8,128)(2,1)S(1)}, u32[]{:S(2)}, u32[]{:S(2)}) async-start(bf16[16,40,256]{2,1,0:T(8,128)(2,1)} %shard_map.125), calls=%async_computation.2 | async-start | bytes 655360 | tf_op jit(solution)/shard_map/all_to_all | solution.py:43
  69.2 8.7 %collective-permute-start.3 = (f32[2,32,128]{2,1,0:T(8,128)S(1)}, f32[2,32,128]{2,1,0:T(8,128)S(1)}, u32[]{:S(2)}, u32[]{:S(2)}) collective-permute-start(f32[2,32,128]{2,1,0:T(8,128)S(1)} %get-tuple-element.53), channel_id=1, source_target_pairs={{4,0},{8,4},{12,8},{16,12},{20,16},{24,20},{28,24},{32,28},{36,32}... | collective-permute-start | bytes 98312 | tf_op jit(solution)/shard_map/ppermute | solution.py:38

commit v6 on v3

--- a/solution.py
+++ b/solution.py
@@ -84,13 +84,20 @@
     return jnp.sum(jnp.transpose(source), 0, keepdims=True)
 
 
-def both_blocks(cotangent, place, near):
+def block_columns(place, near, side):
     far, core = place[0] // (2 * CLOSE), place[0] % 2
     low, high = OFFSETS[0][near], OFFSETS[1][near]
-    own = lax.rem(far + jnp.where(core == 0, low, high) + FAR, FAR)
-    theirs = lax.rem(far + jnp.where(core == 0, high, low) + FAR, FAR)
-    columns = [pl.ds(pl.multiple_of(block * BLOCK, BLOCK), BLOCK) for block in (own, theirs)]
-    return jnp.concatenate([cotangent[:, columns[0]], cotangent[:, columns[1]]], 1)
+    step = jnp.where(core == side, low, high)
+    block = lax.rem(far + step + FAR, FAR)
+    return pl.ds(pl.multiple_of(block * BLOCK, BLOCK), BLOCK)
+
+
+def main_product(turned, cotangent, place, side, product):
+    for near in range(0, CLOSE, 2):
+        pair = [cotangent[:, block_columns(place, near + i, side)] for i in range(2)]
+        both = jnp.dot(turned, jnp.concatenate(pair, 1), preferred_element_type=WIDE)
+        for i in range(2):
+            product[near + i] = both[:, i * BLOCK : (i + 1) * BLOCK]
 
 
 def load(
@@ -118,8 +125,8 @@
 
 def forward(
     place, cotangent, weight, held_value, held_gate, taps, gain, mean, scale,
-    gated, scaled, spread, sums, gain_part, first_upstream, first_cotangent, product,
-    held, held_weight, arrivals,
+    gated, scaled, spread, sums, gain_part, first_upstream, held, across, product,
+    held_weight, arrivals,
     padded, taps_wide, mean_columns, scale_columns, sum_first, sum_second,
     hidden, normed, upstream,
 ):
@@ -156,7 +163,6 @@
         held[...], held_weight[...], (((1,), (1,)), ((), ())), preferred_element_type=WIDE
     )
     first_upstream[...] = upstream[0:EDGE]
-    first_cotangent[...] = held[0:EDGE]
     for half in range(HALVES):
         gain_row = gain[0:1, lanes(half)]
         gain_sum = jnp.zeros((8, LANES), WIDE)
@@ -182,11 +188,8 @@
         for block in range(ROWS // LANES)
     ]
     sums[...] = jnp.concatenate([*found, jnp.zeros((2, LANES), WIDE)], 0)
-    turned = jnp.transpose(hidden[...]).astype(NARROW)
-    for near in range(CLOSE):
-        product[near] = jnp.dot(
-            turned, both_blocks(held, place, near), preferred_element_type=WIDE
-        )
+    across[...] = jnp.transpose(hidden[...]).astype(NARROW)
+    main_product(across[...], held, place, 1, product)
 
 
 def head(
@@ -225,7 +228,7 @@
 
 
 def head_product(cotangent, hidden, place, near, side):
-    columns = both_blocks(cotangent, place, near)[:, side * BLOCK : (side + 1) * BLOCK]
+    columns = cotangent[0:EDGE, block_columns(place, near, side)]
     return lax.dot_general(
         hidden[...], columns, (((0,), (0,)), ((), ())), preferred_element_type=WIDE
     )
@@ -233,7 +236,7 @@
 
 def backward(
     place, sums, scaled, spread, first_scaled, first_spread, halo, gated, scale, gain_part,
-    first_cotangent, first_hidden, product,
+    cotangent, first_hidden, product,
     other, small, extended,
     padded,
 ):
@@ -279,9 +282,7 @@
                 tap = 8 * q + offset - lead
                 small[tap : tap + 1, lanes(half)] = jnp.sum(found[half, q], 0, keepdims=True)
         near = offset
-        whole = product[near, :, BLOCK:] + head_product(
-            first_cotangent, first_hidden, place, near, 1
-        )
+        whole = product[near] + head_product(cotangent, first_hidden, place, near, 1)
         other[near * WIDTH : (near + 1) * WIDTH] = whole.astype(NARROW)
     for half in range(HALVES):
         small[TAPS:SMALL, lanes(half)] = jnp.sum(gain_part[half], 0, keepdims=True)
@@ -309,14 +310,13 @@
 
 
 def gated_gradient(
-    place, extended, taps, value, gate, first_cotangent, first_hidden, product,
+    place, extended, taps, value, gate, cotangent, first_hidden, across,
     value_grad, gate_grad, margin, last, mine,
     taps_wide,
 ):
+    main_product(across[...], cotangent, place, 0, mine)
     for near in range(CLOSE):
-        mine[near] = product[near, :, 0:BLOCK] + head_product(
-            first_cotangent, first_hidden, place, near, 0
-        )
+        mine[near] = mine[near] + head_product(cotangent, first_hidden, place, near, 0)
     taps_wide[0:TAPS] = taps[...].astype(WIDE)
     for half in range(HALVES):
         for start in range(0, EDGE + ROWS, EDGE):
@@ -414,19 +414,18 @@
     taps_scratch = pltpu.VMEM((TAPS + 1, WIDTH), WIDE)
     place = lax.axis_index(SP).reshape(1)
     narrow = ((ROWS, WIDTH), NARROW)
-    gated, scaled, spread, sums, gain_part, first_upstream, first_cotangent, product = (
+    gated, scaled, spread, sums, gain_part, first_upstream, cotangent, across, product = (
         scalar_call(
             forward,
             [
                 narrow, (rest, WIDE), (rest, WIDE), ((8, LANES), WIDE),
-                ((HALVES, 8, LANES), WIDE), ((EDGE, WIDTH), WIDE), ((EDGE, MODEL), NARROW),
-                ((CLOSE, WIDTH, 2 * BLOCK), WIDE),
+                ((HALVES, 8, LANES), WIDE), ((EDGE, WIDTH), WIDE), ((ROWS, MODEL), NARROW),
+                ((WIDTH, ROWS), NARROW), ((CLOSE, WIDTH, BLOCK), WIDE),
             ],
             place, out_cotangent, out_weight, proj_value, proj_gate,
             conv_taps, row_gain, row_mean, row_scale, in_hbm=2,
             scratch=[
-                pltpu.VMEM((ROWS, MODEL), NARROW), pltpu.VMEM((WIDTH, MODEL), NARROW),
-                pltpu.SemaphoreType.DMA((2,)),
+                pltpu.VMEM((WIDTH, MODEL), NARROW), pltpu.SemaphoreType.DMA((2,)),
                 sides, taps_scratch, *([pltpu.VMEM((ROWS, LANES), WIDE)] * 4),
                 pltpu.VMEM((ROWS, WIDTH), WIDE), pltpu.VMEM(split, WIDE),
                 pltpu.VMEM((ROWS, WIDTH), WIDE),
@@ -458,15 +457,15 @@
             ((HALVES, ROWS + 2 * EDGE, LANES), WIDE),
         ],
         place, sums, scaled, spread, first_scaled, first_spread, halo, gated, row_scale, gain_part,
-        first_cotangent, first_hidden, product, scratch=[sides], flops=100 * ROWS * WIDTH,
+        cotangent, first_hidden, product, scratch=[sides], flops=100 * ROWS * WIDTH,
     )
     other = lax.ppermute(other, "c", [(0, 1), (1, 0)])
     main = ((ROWS - EDGE, WIDTH), NARROW)
     value_part, gate_part, margin, last, mine = scalar_call(
         gated_gradient,
         [main, main, (edge, WIDE), ((3, *edge), WIDE), ((CLOSE, WIDTH, BLOCK), WIDE)],
-        place, extended, conv_taps, proj_value, proj_gate, first_cotangent, first_hidden,
-        product, scratch=[taps_scratch], flops=100 * ROWS * WIDTH,
+        place, extended, conv_taps, proj_value, proj_gate, cotangent, first_hidden,
+        across, scratch=[taps_scratch], flops=100 * ROWS * WIDTH,
     )
     (pieces,) = call(
         pack, [((CLOSE, WIDTH + 2 * SMALL, BLOCK), NARROW)], mine, small, other, flops=1 << 20

time: 79.6 us -> 80.1 us (level)
    ppermute x1, waiting for transfers between devices: 6.76 us -> 7.63 us  [to_block(): return lax.ppermute(value, SP, pairs)]
where the time goes in v6:
time: 80.1 us; the launch traced here: 79.1 us
  blocking collectives  28.7 us (36%)
  starting transfers between devices  26.2 us (33%)
  waiting for transfers between devices  14.2 us (18%)
  Pallas kernels  9.24 us (12%)
    all_to_all x2, blocking collectives, exchange(): lax.all_to_all(pieces, axes, 0, 0, tiled=True, axis_index_groups=groups)  28.7 us
    ppermute x1, starting transfers between devices, to_block(): return lax.ppermute(value, SP, pairs)  11.5 us
    ppermute x1, waiting for transfers between devices, to_block(): return lax.ppermute(value, SP, pairs)  7.63 us
    all_to_all x1, starting transfers between devices, exchange(): lax.all_to_all(pieces, axes, 0, 0, tiled=True, axis_index_groups=groups)  6.4 us
    ppermute x2, starting transfers between devices, shifted(): lax.ppermute(value, axis, [(source, source + steps) for source in range(f...  6.33 us
    all_to_all x1, waiting for transfers between devices, exchange(): lax.all_to_all(pieces, axes, 0, 0, tiled=True, axis_index_groups=groups)  6.33 us
    pallas_call x3, Pallas kernels, scalar_call(): pl.pallas_call(body, out_shape=shapes, in_specs=[pl.BlockSpec(memory_spac...  6.06 us
    ppermute x1, starting transfers between devices, shards(): other = lax.ppermute(other, 'c', [(0, 1), (1, 0)])  1.92 us
  transfers between devices with their start and end apart: 5, of which 3 were waited for; matrix products, arithmetic and copies ran while one was open for 0% of the time, Pallas kernels for 6%

profile of v6, /device:TPU:7, one launch (start us, length us, event | category | flops | bytes accessed | tf_op | source)
XLA Modules:
  0.0 79.1 jit_solution(2745748441712134765)
XLA Ops:
  0.6 1.1 %load.1 = (bf16[32,256]{1,0:T(8,128)(2,1)S(1)}, bf16[384,256]{1,0:T(8,128)(2,1)S(1)}, bf16[384,256]{1,0:T(8,128)(2,1)S(1)}, bf16[31,256]{1,0:T(8,128)(2,1)S(1)},...) custom-call(bf16[384,256]{1,0:T(8,128)(2,1)} %value.1, bf16[384,256]{1,0:T(8,128)(2,1)} %gate.1, ...), custom_call_target="tpu_custom_call" | custom-call | flops 65536 | bytes 524288 | tf_op jit(solution)/shard_map/load/pallas_call | solution.py:527
  1.7 4.0 %collective-permute-start = (bf16[32,256]{1,0:T(8,128)(2,1)S(1)}, bf16[32,256]{1,0:T(8,128)(2,1)S(1)}, u32[]{:S(2)}, u32[]{:S(2)}) collective-permute-start(bf16[32,256]{1,0:T(8,128)(2,1)S(1)} %get-tuple-element.39), channel_id=1, source_target_pairs={{0,4},{4,8},{8,12},{12,16},{16,20},{20,24},{24,28},{28,32},{32,36}... | collective-permute-start | bytes 49160 | tf_op jit(solution)/shard_map/ppermute | solution.py:38
  5.8 2.9 %shard_map.119 = (bf16[384,256]{1,0:T(8,128)(2,1)S(1)}, f32[2,352,128]{2,1,0:T(8,128)S(1)}, f32[2,352,128]{2,1,0:T(8,128)S(1)}, f32[8,128]{1,0:T(8,128)S(1)}, f3...) custom-call(s32[1]{0:T(128)} %bitcast.place, ...), custom_call_target="tpu_custom_call" | custom-call | flops 805306368 | bytes 6815232 | tf_op jit(solution)/shard_map/pallas_call | solution.py:508
  8.7 0.0 collective-permute-done.halo
  8.7 0.2 shard_map.120
  8.9 6.7 %all_to_all.15.sums = f32[4,8,128]{2,1,0:T(8,128)S(1)} all-to-all(f32[4,8,128]{2,1,0:T(8,128)S(1)} %get-tuple-element.50), channel_id=1, replica_groups={{2,3,0,1},{6,7,4,5},{10,11,8,9},{14,15,12,13},{18,19,16,17},{22,23,20,2..., dimensions={0} | all-to-all | bytes 32768 | tf_op jit(solution)/shard_map/all_to_all | solution.py:43
  15.6 1.5 %shard_map.121 = (bf16[2176,128]{1,0:T(8,128)(2,1)S(1)}, f32[32,256]{1,0:T(8,128)S(1)}, f32[2,448,128]{2,1,0:T(8,128)S(1)}) custom-call(s32[1]{0:T(128)} %bitcast.place, f32[4,8,128]{2,1,0:T(8,128)S(1)} %all_to_all.15.sums, f32[2,352,128]{2,1,0:T(8,128)S(1)} %get-tuple-element.51.scaled, f32[2,352,128]{2,1,0:T(8,128)S(1)} %get-tuple-element.52.spread, ...), custom_call_target="tpu_custom_call" | custom-call | flops 9830400 | bytes 4711936 | tf_op jit(solution)/shard_map/pallas_call | solution.py:508
  17.2 1.9 %collective-permute-start.1 = (bf16[2176,128]{1,0:T(8,128)(2,1)S(1)}, bf16[2176,128]{1,0:T(8,128)(2,1)S(1)}, u32[]{:S(2)}, u32[]{:S(2)}) collective-permute-start(bf16[2176,128]{1,0:T(8,128)(2,1)S(1)} %get-tuple-element.63), channel_id=1, source_target_pairs={{0,4},{4,0},{1,5},{5,1},{2,6},{6,2},{3,7},{7,3},{8,12},{12,8},{9,1... | collective-permute-start | bytes 1671176 | tf_op jit(solution)/shard_map/ppermute | solution.py:462
  19.1 1.7 %shard_map.122 = (bf16[352,256]{1,0:T(8,128)(2,1)S(1)}, bf16[352,256]{1,0:T(8,128)(2,1)S(1)}, f32[2,32,128]{2,1,0:T(8,128)S(1)}, f32[3,2,32,128]{3,2,1,0:T(8,128)S(1)}, f32[8,256,128]{2,1,0:T(8,128)S(1)}) custom-call(s32[1]{0:T(128)} %bitcast.place, f32[2,448,128]{2,1,0:T(8,128)S(1)} %get-tuple-element.59.extended, ...), custom_call_target="tpu_custom_call" | custom-call | flops 9830400 | bytes 4193792 | tf_op jit(solution)/shard_map/pallas_call | solution.py:508
  20.8 0.3 collective-permute-done.1.other
  21.0 0.1 shard_map.123
  21.1 22.0 %all_to_all.16.arrived = bf16[8,320,128]{2,1,0:T(8,128)(2,1)S(1)} all-to-all(bf16[8,320,128]{2,1,0:T(8,128)(2,1)S(1)} %shard_map.123), channel_id=1, replica_groups={{32,40,48,56,0,8,16,24},{33,41,49,57,1,9,17,25},{34,42,50,58,2,10,18,26..., dimensions={0} | all-to-all | bytes 1310720 | tf_op jit(solution)/shard_map/all_to_all | solution.py:43
  43.1 0.1 shard_map.124
  43.2 11.5 %collective-permute-start.2 = (bf16[320,128]{1,0:T(8,128)(2,1)S(1)}, bf16[320,128]{1,0:T(8,128)(2,1)S(1)}, u32[]{:S(2)}, u32[]{:S(2)}) collective-permute-start(bf16[320,128]{1,0:T(8,128)(2,1)S(1)} %shard_map.124), channel_id=1, source_target_pairs={{0,0},{4,388},{8,968},{12,460},{16,912},{20,532},{24,856},{28,348}... | collective-permute-start | bytes 245768 | tf_op jit(solution)/shard_map/ppermute | solution.py:400
  54.7 7.6 %collective-permute-done.2.payload = bf16[320,128]{1,0:T(8,128)(2,1)S(1)} collective-permute-done((bf16[320,128]{1,0:T(8,128)(2,1)S(1)}, bf16[320,128]{1,0:T(8,128)(2,1)S(1)}, u32[]{:S(2)}, u32[]{:S(2)}) %collective-permute-start.2) | collective-permute-done | bytes 81952 | tf_op jit(solution)/shard_map/ppermute | solution.py:400
  62.3 0.8 %shard_map.125 = bf16[16,40,256]{2,1,0:T(8,128)(2,1)} custom-call(bf16[320,128]{1,0:T(8,128)(2,1)S(1)} %collective-permute-done.2.payload), custom_call_target="tpu_custom_call" | custom-call | flops 65536 | bytes 409600 | tf_op jit(solution)/shard_map/pallas_call | solution.py:57
  63.2 6.4 %all-to-all-start.2 = ((bf16[16,40,256]{2,1,0:T(8,128)(2,1)}), bf16[16,40,256]{2,1,0:T(8,128)(2,1)S(1)}, u32[]{:S(2)}, u32[]{:S(2)}) async-start(bf16[16,40,256]{2,1,0:T(8,128)(2,1)} %shard_map.125), calls=%async_computation.2 | async-start | bytes 655360 | tf_op jit(solution)/shard_map/all_to_all | solution.py:43
  69.6 2.3 %collective-permute-start.3 = (f32[2,32,128]{2,1,0:T(8,128)S(1)}, f32[2,32,128]{2,1,0:T(8,128)S(1)}, u32[]{:S(2)}, u32[]{:S(2)}) collective-permute-start(f32[2,32,128]{2,1,0:T(8,128)S(1)} %get-tuple-element.67), channel_id=1, source_target_pairs={{4,0},{8,4},{12,8},{16,12},{20,16},{24,20},{28,24},{32,28},{36,32}... | collective-permute-start | bytes 98312 | tf_op jit(solution)/shard_map/ppermute | solution.py:38
  71.9 6.3 %all-to-all-done.2.arrived = bf16[16,40,256]{2,1,0:T(8,128)(2,1)S(1)} async-done(((bf16[16,40,256]{2,1,0:T(8,128)(2,1)}), bf16[16,40,256]{2,1,0:T(8,128)(2,1)S(1)}, u32[]{:S(2)}, u32[]{:S(2)}) %all-to-all-start.2) | async-done | bytes 327712 | tf_op jit(solution)/shard_map/all_to_all | solution.py:43
  78.3 0.0 collective-permute-done.3.late
  78.3 0.8 %finish.1 = (bf16[384,256]{1,0:T(8,128)(2,1)}, bf16[384,256]{1,0:T(8,128)(2,1)}, f32[8,256]{1,0:T(8,128)}, f32[31,256]{1,0:T(8,128)}, f32[1,256]{1,0:T(1,128)}) custom-call(f32[40,256]{1,0:T(8,128)S(1)} %shard_map.126.total, bf16[352,256]{1,0:T(8,128)(2,1)S(1)} %get-tuple-element.64.value_part, bf16[352,256]{1,0:T(8,128)(2,1)S(1)} %get-tuple-element.65.gate_part, ...), custom_call_target="tpu_custom_call" | custom-call | flops 65536 | bytes 524288 | tf_op jit(solution)/shard_map/finish/pallas_call | solution.py:541
  (1 shorter events, 0.0 us)
Async XLA Ops:
  1.7 6.9 %collective-permute-start = (bf16[32,256]{1,0:T(8,128)(2,1)S(1)}, bf16[32,256]{1,0:T(8,128)(2,1)S(1)}, u32[]{:S(2)}, u32[]{:S(2)}) collective-permute-start(bf16[32,256]{1,0:T(8,128)(2,1)S(1)} %get-tuple-element.39), channel_id=1, source_target_pairs={{0,4},{4,8},{8,12},{12,16},{16,20},{20,24},{24,28},{28,32},{32,36}... | collective-permute-start | bytes 49160 | tf_op jit(solution)/shard_map/ppermute | solution.py:38
  17.2 3.9 %collective-permute-start.1 = (bf16[2176,128]{1,0:T(8,128)(2,1)S(1)}, bf16[2176,128]{1,0:T(8,128)(2,1)S(1)}, u32[]{:S(2)}, u32[]{:S(2)}) collective-permute-start(bf16[2176,128]{1,0:T(8,128)(2,1)S(1)} %get-tuple-element.63), channel_id=1, source_target_pairs={{0,4},{4,0},{1,5},{5,1},{2,6},{6,2},{3,7},{7,3},{8,12},{12,8},{9,1... | collective-permute-start | bytes 1671176 | tf_op jit(solution)/shard_map/ppermute | solution.py:462
  43.2 19.2 %collective-permute-start.2 = (bf16[320,128]{1,0:T(8,128)(2,1)S(1)}, bf16[320,128]{1,0:T(8,128)(2,1)S(1)}, u32[]{:S(2)}, u32[]{:S(2)}) collective-permute-start(bf16[320,128]{1,0:T(8,128)(2,1)S(1)} %shard_map.124), channel_id=1, source_target_pairs={{0,0},{4,388},{8,968},{12,460},{16,912},{20,532},{24,856},{28,348}... | collective-permute-start | bytes 245768 | tf_op jit(solution)/shard_map/ppermute | solution.py:400
  63.2 15.1 %all-to-all-start.2 = ((bf16[16,40,256]{2,1,0:T(8,128)(2,1)}), bf16[16,40,256]{2,1,0:T(8,128)(2,1)S(1)}, u32[]{:S(2)}, u32[]{:S(2)}) async-start(bf16[16,40,256]{2,1,0:T(8,128)(2,1)} %shard_map.125), calls=%async_computation.2 | async-start | bytes 655360 | tf_op jit(solution)/shard_map/all_to_all | solution.py:43
  69.6 8.7 %collective-permute-start.3 = (f32[2,32,128]{2,1,0:T(8,128)S(1)}, f32[2,32,128]{2,1,0:T(8,128)S(1)}, u32[]{:S(2)}, u32[]{:S(2)}) collective-permute-start(f32[2,32,128]{2,1,0:T(8,128)S(1)} %get-tuple-element.67), channel_id=1, source_target_pairs={{4,0},{8,4},{12,8},{16,12},{20,16},{24,20},{28,24},{32,28},{36,32}... | collective-permute-start | bytes 98312 | tf_op jit(solution)/shard_map/ppermute | solution.py:38

commit v7 on v5

--- a/solution.py
+++ b/solution.py
@@ -17,7 +17,7 @@
 OFFSETS = ((0, -1, -2, -3, 3, 2, 1, -4), (6, 7, 8, 5, -7, -6, -5, 4))
 BLOCK = CLOSE * 2 * 8
 NEAR_ORDER = [(place + 4) % CLOSE for place in range(CLOSE)]
-GATHER_ORDER = [(place + 7) % (2 * CLOSE) for place in range(2 * CLOSE)]
+GATHER_ORDER = [(place + 5) % (2 * CLOSE) for place in range(2 * CLOSE)]
 TAPS = 31
 SMALL = TAPS + 1
 ROWS = 384
@@ -84,26 +84,19 @@
     return jnp.sum(jnp.transpose(source), 0, keepdims=True)
 
 
-def block_columns(place, near, side):
+def both_blocks(cotangent, place, near):
     far, core = place[0] // (2 * CLOSE), place[0] % 2
     low, high = OFFSETS[0][near], OFFSETS[1][near]
-    step = jnp.where(core == side, low, high)
-    block = lax.rem(far + step + FAR, FAR)
-    return pl.ds(pl.multiple_of(block * BLOCK, BLOCK), BLOCK)
-
-
-def main_product(turned, cotangent, place, side, product):
-    for near in range(0, CLOSE, 2):
-        pair = [cotangent[:, block_columns(place, near + i, side)] for i in range(2)]
-        both = jnp.dot(turned, jnp.concatenate(pair, 1), preferred_element_type=WIDE)
-        for i in range(2):
-            product[near + i] = both[:, i * BLOCK : (i + 1) * BLOCK]
+    own = lax.rem(far + jnp.where(core == 0, low, high) + FAR, FAR)
+    theirs = lax.rem(far + jnp.where(core == 0, high, low) + FAR, FAR)
+    columns = [pl.ds(pl.multiple_of(block * BLOCK, BLOCK), BLOCK) for block in (own, theirs)]
+    return jnp.concatenate([cotangent[:, columns[0]], cotangent[:, columns[1]]], 1)
 
 
 def forward(
     place, value, gate, cotangent, weight, far_taps, far_gain, far_mean, far_scale,
-    gated, scaled, spread, sums, gain_part, first_upstream, held, across, product,
-    held_value, held_gate, held_weight, taps, gain, mean, scale, arrivals,
+    gated, scaled, spread, sums, gain_part, first_upstream, first_cotangent, product,
+    held_value, held_gate, held, held_weight, taps, gain, mean, scale, arrivals,
     padded, taps_wide, mean_columns, scale_columns, sum_first, sum_second,
     hidden, normed, upstream,
 ):
@@ -145,6 +138,7 @@
         held[...], held_weight[...], (((1,), (1,)), ((), ())), preferred_element_type=WIDE
     )
     first_upstream[...] = upstream[0:EDGE]
+    first_cotangent[...] = held[0:EDGE]
     for half in range(HALVES):
         gain_row = gain[0:1, lanes(half)]
         gain_sum = jnp.zeros((8, LANES), WIDE)
@@ -170,8 +164,11 @@
         for block in range(ROWS // LANES)
     ]
     sums[...] = jnp.concatenate([*found, jnp.zeros((2, LANES), WIDE)], 0)
-    across[...] = jnp.transpose(hidden[...]).astype(NARROW)
-    main_product(across[...], held, place, 1, product)
+    turned = jnp.transpose(hidden[...]).astype(NARROW)
+    for near in range(CLOSE):
+        product[near] = jnp.dot(
+            turned, both_blocks(held, place, near), preferred_element_type=WIDE
+        )
 
 
 def head(
@@ -210,7 +207,7 @@
 
 
 def head_product(cotangent, hidden, place, near, side):
-    columns = cotangent[0:EDGE, block_columns(place, near, side)]
+    columns = both_blocks(cotangent, place, near)[:, side * BLOCK : (side + 1) * BLOCK]
     return lax.dot_general(
         hidden[...], columns, (((0,), (0,)), ((), ())), preferred_element_type=WIDE
     )
@@ -218,7 +215,7 @@
 
 def backward(
     place, sums, scaled, spread, first_scaled, first_spread, halo, gated, scale, gain_part,
-    cotangent, first_hidden, product,
+    first_cotangent, first_hidden, product,
     other, small, extended,
     padded,
 ):
@@ -264,7 +261,9 @@
                 tap = 8 * q + offset - lead
                 small[tap : tap + 1, lanes(half)] = jnp.sum(found[half, q], 0, keepdims=True)
         near = offset
-        whole = product[near] + head_product(cotangent, first_hidden, place, near, 1)
+        whole = product[near, :, BLOCK:] + head_product(
+            first_cotangent, first_hidden, place, near, 1
+        )
         other[near * WIDTH : (near + 1) * WIDTH] = whole.astype(NARROW)
     for half in range(HALVES):
         small[TAPS:SMALL, lanes(half)] = jnp.sum(gain_part[half], 0, keepdims=True)
@@ -292,13 +291,14 @@
 
 
 def gated_gradient(
-    place, extended, taps, value, gate, cotangent, first_hidden, across,
+    place, extended, taps, value, gate, first_cotangent, first_hidden, product,
     value_grad, gate_grad, margin, last, mine,
     taps_wide,
 ):
-    main_product(across[...], cotangent, place, 0, mine)
     for near in range(CLOSE):
-        mine[near] = mine[near] + head_product(cotangent, first_hidden, place, near, 0)
+        mine[near] = product[near, :, 0:BLOCK] + head_product(
+            first_cotangent, first_hidden, place, near, 0
+        )
     taps_wide[0:TAPS] = taps[...].astype(WIDE)
     for half in range(HALVES):
         for start in range(0, EDGE + ROWS, EDGE):
@@ -395,18 +395,18 @@
     taps_scratch = pltpu.VMEM((TAPS + 1, WIDTH), WIDE)
     place = lax.axis_index(SP).reshape(1)
     narrow = ((ROWS, WIDTH), NARROW)
-    gated, scaled, spread, sums, gain_part, first_upstream, cotangent, across, product = (
+    gated, scaled, spread, sums, gain_part, first_upstream, first_cotangent, product = (
         scalar_call(
             forward,
             [
                 narrow, (rest, WIDE), (rest, WIDE), ((8, LANES), WIDE),
-                ((HALVES, 8, LANES), WIDE), ((EDGE, WIDTH), WIDE), ((ROWS, MODEL), NARROW),
-                ((WIDTH, ROWS), NARROW), ((CLOSE, WIDTH, BLOCK), WIDE),
+                ((HALVES, 8, LANES), WIDE), ((EDGE, WIDTH), WIDE), ((EDGE, MODEL), NARROW),
+                ((CLOSE, WIDTH, 2 * BLOCK), WIDE),
             ],
             place, proj_value, proj_gate, out_cotangent, out_weight,
             conv_taps, row_gain, row_mean, row_scale, in_hbm=8,
             scratch=[
-                pltpu.VMEM(*narrow), pltpu.VMEM(*narrow),
+                pltpu.VMEM(*narrow), pltpu.VMEM(*narrow), pltpu.VMEM((ROWS, MODEL), NARROW),
                 pltpu.VMEM((WIDTH, MODEL), NARROW), pltpu.VMEM((TAPS, WIDTH), NARROW),
                 pltpu.VMEM((1, WIDTH), WIDE), pltpu.VMEM((ROWS,), WIDE),
                 pltpu.VMEM((ROWS,), WIDE), pltpu.SemaphoreType.DMA((8,)),
@@ -441,15 +441,15 @@
             ((HALVES, ROWS + 2 * EDGE, LANES), WIDE),
         ],
         place, sums, scaled, spread, first_scaled, first_spread, halo, gated, row_scale, gain_part,
-        cotangent, first_hidden, product, scratch=[sides], flops=100 * ROWS * WIDTH,
+        first_cotangent, first_hidden, product, scratch=[sides], flops=100 * ROWS * WIDTH,
     )
     other = lax.ppermute(other, "c", [(0, 1), (1, 0)])
     main = ((ROWS - EDGE, WIDTH), NARROW)
     value_part, gate_part, margin, last, mine = scalar_call(
         gated_gradient,
         [main, main, (edge, WIDE), ((3, *edge), WIDE), ((CLOSE, WIDTH, BLOCK), WIDE)],
-        place, extended, conv_taps, proj_value, proj_gate, cotangent, first_hidden,
-        across, scratch=[taps_scratch], flops=100 * ROWS * WIDTH,
+        place, extended, conv_taps, proj_value, proj_gate, first_cotangent, first_hidden,
+        product, scratch=[taps_scratch], flops=100 * ROWS * WIDTH,
     )
     (pieces,) = call(
         pack, [((CLOSE, WIDTH + 2 * SMALL, BLOCK), NARROW)], mine, small, other, flops=1 << 20

time: 79.8 us -> 81.1 us (1.016)
  starting transfers between devices: 26.2 us -> 29.1 us
  waiting for transfers between devices: 13.8 us -> 12.6 us
    all_to_all x1, starting transfers between devices: 6.47 us -> 8.87 us  [exchange(): lax.all_to_all(pieces, axes, 0, 0, tiled=True, axis_index_groups=groups)]
    ppermute x1, waiting for transfers between devices: 7.2 us -> 6.09 us  [to_block(): return lax.ppermute(value, SP, pairs)]
  transfers between devices with their start and end apart: 5 -> 5, of which waited for: 3 -> 4; matrix products, arithmetic and copies ran while one was open for 0% -> 0% of each run, Pallas kernels for 6% -> 6%
where the time goes in v7:
time: 81.1 us; the launch traced here: 80.2 us
  starting transfers between devices  29.1 us (36%)
  blocking collectives  28.5 us (35%)
  waiting for transfers between devices  12.6 us (16%)
  Pallas kernels  8.35 us (10%)
  between operations  0.82 us (1%)
    all_to_all x2, blocking collectives, exchange(): lax.all_to_all(pieces, axes, 0, 0, tiled=True, axis_index_groups=groups)  28.5 us
    ppermute x1, starting transfers between devices, to_block(): return lax.ppermute(value, SP, pairs)  12 us
    all_to_all x1, starting transfers between devices, exchange(): lax.all_to_all(pieces, axes, 0, 0, tiled=True, axis_index_groups=groups)  8.87 us
    ppermute x2, starting transfers between devices, shifted(): lax.ppermute(value, axis, [(source, source + steps) for source in range(f...  6.31 us
    pallas_call x3, Pallas kernels, scalar_call(): pl.pallas_call(body, out_shape=shapes, in_specs=[pl.BlockSpec(memory_spac...  6.27 us
    ppermute x1, waiting for transfers between devices, to_block(): return lax.ppermute(value, SP, pairs)  6.09 us
    all_to_all x1, waiting for transfers between devices, exchange(): lax.all_to_all(pieces, axes, 0, 0, tiled=True, axis_index_groups=groups)  5.68 us
    ppermute x1, starting transfers between devices, shards(): other = lax.ppermute(other, 'c', [(0, 1), (1, 0)])  1.92 us
  transfers between devices with their start and end apart: 5, of which 4 were waited for; matrix products, arithmetic and copies ran while one was open for 0% of the time, Pallas kernels for 6%

profile of v7, /device:TPU:7, one launch (start us, length us, event | category | flops | bytes accessed | tf_op | source)
XLA Modules:
  0.0 80.2 jit_solution(18378528625298992518)
XLA Ops:
  0.6 0.0 copy-start.3
  0.6 0.0 copy-start.2
  0.7 0.0 copy-start.4
  0.7 0.0 copy-start.5
  0.7 0.8 multiply_convert_fusion
  1.5 4.0 %collective-permute-start = (bf16[32,256]{1,0:T(8,128)(2,1)S(1)}, bf16[32,256]{1,0:T(8,128)(2,1)S(1)}, u32[]{:S(2)}, u32[]{:S(2)}) collective-permute-start(bf16[32,256]{1,0:T(8,128)(2,1)S(1)} %multiply_convert_fusion), channel_id=1, source_target_pairs={{0,4},{4,8},{8,12},{12,16},{16,20},{20,24},{24,28},{28,32},{32,36}... | collective-permute-start | bytes 49160 | tf_op jit(solution)/shard_map/ppermute | solution.py:38
  5.5 3.4 %shard_map.119 = (bf16[384,256]{1,0:T(8,128)(2,1)S(1)}, f32[2,352,128]{2,1,0:T(8,128)S(1)}, f32[2,352,128]{2,1,0:T(8,128)S(1)}, f32[8,128]{1,0:T(8,128)S(1)}, f3...) custom-call(s32[1]{0:T(128)} %bitcast.place, ...), custom_call_target="tpu_custom_call" | custom-call | flops 805306368 | bytes 6225408 | tf_op jit(solution)/shard_map/pallas_call | solution.py:492
  8.9 0.0 copy-start
  8.9 0.0 copy-start.1
  8.9 0.0 collective-permute-done.halo
  8.9 0.0 copy-done.3
  8.9 0.0 copy-done.2
  8.9 0.0 copy-done.4
  9.0 0.0 copy-done.5
  9.0 0.2 shard_map.120
  9.2 6.7 %all_to_all.15.sums = f32[4,8,128]{2,1,0:T(8,128)S(1)} all-to-all(f32[4,8,128]{2,1,0:T(8,128)S(1)} %get-tuple-element.35), channel_id=1, replica_groups={{2,3,0,1},{6,7,4,5},{10,11,8,9},{14,15,12,13},{18,19,16,17},{22,23,20,2..., dimensions={0} | all-to-all | bytes 32768 | tf_op jit(solution)/shard_map/all_to_all | solution.py:43
  15.9 1.5 %shard_map.121 = (bf16[2176,128]{1,0:T(8,128)(2,1)S(1)}, f32[32,256]{1,0:T(8,128)S(1)}, f32[2,448,128]{2,1,0:T(8,128)S(1)}) custom-call(s32[1]{0:T(128)} %bitcast.place, f32[4,8,128]{2,1,0:T(8,128)S(1)} %all_to_all.15.sums, f32[2,352,128]{2,1,0:T(8,128)S(1)} %get-tuple-element.36.scaled, f32[2,352,128]{2,1,0:T(8,128)S(1)} %get-tuple-element.37.spread, ...), custom_call_target="tpu_custom_call" | custom-call | flops 9830400 | bytes 4318720 | tf_op jit(solution)/shard_map/pallas_call | solution.py:492
  17.4 1.9 %collective-permute-start.1 = (bf16[2176,128]{1,0:T(8,128)(2,1)S(1)}, bf16[2176,128]{1,0:T(8,128)(2,1)S(1)}, u32[]{:S(2)}, u32[]{:S(2)}) collective-permute-start(bf16[2176,128]{1,0:T(8,128)(2,1)S(1)} %get-tuple-element.47), channel_id=1, source_target_pairs={{0,4},{4,0},{1,5},{5,1},{2,6},{6,2},{3,7},{7,3},{8,12},{12,8},{9,1... | collective-permute-start | bytes 1671176 | tf_op jit(solution)/shard_map/ppermute | solution.py:446
  19.4 0.0 copy-done
  19.4 0.0 copy-done.1
  19.4 1.4 %shard_map.122 = (bf16[352,256]{1,0:T(8,128)(2,1)S(1)}, bf16[352,256]{1,0:T(8,128)(2,1)S(1)}, f32[2,32,128]{2,1,0:T(8,128)S(1)}, f32[3,2,32,128]{3,2,1,0:T(8,128)S(1)}, f32[8,256,128]{2,1,0:T(8,128)S(1)}) custom-call(s32[1]{0:T(128)} %bitcast.place, f32[2,448,128]{2,1,0:T(8,128)S(1)} %get-tuple-element.44.extended, bf16[31,256]{1,0:T(8,128)(2,1)S(1)} %copy-done.2, ...), custom_call_target="tpu_custom_call" | custom-call | flops 9830400 | bytes 4652544 | tf_op jit(solution)/shard_map/pallas_call | solution.py:492
  20.8 0.5 collective-permute-done.1.other
  21.3 0.1 shard_map.123
  21.4 21.7 %all_to_all.16.arrived = bf16[8,320,128]{2,1,0:T(8,128)(2,1)S(1)} all-to-all(bf16[8,320,128]{2,1,0:T(8,128)(2,1)S(1)} %shard_map.123), channel_id=1, replica_groups={{32,40,48,56,0,8,16,24},{33,41,49,57,1,9,17,25},{34,42,50,58,2,10,18,26..., dimensions={0} | all-to-all | bytes 1310720 | tf_op jit(solution)/shard_map/all_to_all | solution.py:43
  43.1 0.1 shard_map.124
  43.2 12.0 %collective-permute-start.2 = (bf16[320,128]{1,0:T(8,128)(2,1)S(1)}, bf16[320,128]{1,0:T(8,128)(2,1)S(1)}, u32[]{:S(2)}, u32[]{:S(2)}) collective-permute-start(bf16[320,128]{1,0:T(8,128)(2,1)S(1)} %shard_map.124), channel_id=1, source_target_pairs={{0,0},{4,388},{8,968},{12,460},{16,912},{20,532},{24,856},{28,348}... | collective-permute-start | bytes 245768 | tf_op jit(solution)/shard_map/ppermute | solution.py:382
  55.3 6.1 %collective-permute-done.2.payload = bf16[320,128]{1,0:T(8,128)(2,1)S(1)} collective-permute-done((bf16[320,128]{1,0:T(8,128)(2,1)S(1)}, bf16[320,128]{1,0:T(8,128)(2,1)S(1)}, u32[]{:S(2)}, u32[]{:S(2)}) %collective-permute-start.2) | collective-permute-done | bytes 81952 | tf_op jit(solution)/shard_map/ppermute | solution.py:382
  61.3 0.8 %shard_map.125 = bf16[16,40,256]{2,1,0:T(8,128)(2,1)} custom-call(bf16[320,128]{1,0:T(8,128)(2,1)S(1)} %collective-permute-done.2.payload), custom_call_target="tpu_custom_call" | custom-call | flops 65536 | bytes 409600 | tf_op jit(solution)/shard_map/pallas_call | solution.py:57
  62.2 8.9 %all-to-all-start.2 = ((bf16[16,40,256]{2,1,0:T(8,128)(2,1)}), bf16[16,40,256]{2,1,0:T(8,128)(2,1)S(1)}, u32[]{:S(2)}, u32[]{:S(2)}) async-start(bf16[16,40,256]{2,1,0:T(8,128)(2,1)} %shard_map.125), calls=%async_computation.2 | async-start | bytes 655360 | tf_op jit(solution)/shard_map/all_to_all | solution.py:43
  71.0 2.3 %collective-permute-start.3 = (f32[2,32,128]{2,1,0:T(8,128)S(1)}, f32[2,32,128]{2,1,0:T(8,128)S(1)}, u32[]{:S(2)}, u32[]{:S(2)}) collective-permute-start(f32[2,32,128]{2,1,0:T(8,128)S(1)} %get-tuple-element.51), channel_id=1, source_target_pairs={{4,0},{8,4},{12,8},{16,12},{20,16},{24,20},{28,24},{32,28},{36,32}... | collective-permute-start | bytes 98312 | tf_op jit(solution)/shard_map/ppermute | solution.py:38
  73.3 5.7 %all-to-all-done.2.arrived = bf16[16,40,256]{2,1,0:T(8,128)(2,1)S(1)} async-done(((bf16[16,40,256]{2,1,0:T(8,128)(2,1)}), bf16[16,40,256]{2,1,0:T(8,128)(2,1)S(1)}, u32[]{:S(2)}, u32[]{:S(2)}) %all-to-all-start.2) | async-done | bytes 327712 | tf_op jit(solution)/shard_map/all_to_all | solution.py:43
  79.1 0.3 collective-permute-done.3.late
  79.4 0.8 %finish.1 = (bf16[384,256]{1,0:T(8,128)(2,1)}, bf16[384,256]{1,0:T(8,128)(2,1)}, f32[8,256]{1,0:T(8,128)}, f32[31,256]{1,0:T(8,128)}, f32[1,256]{1,0:T(1,128)}) custom-call(f32[40,256]{1,0:T(8,128)S(1)} %shard_map.126.total, bf16[352,256]{1,0:T(8,128)(2,1)S(1)} %get-tuple-element.48.value_part, bf16[352,256]{1,0:T(8,128)(2,1)S(1)} %get-tuple-element.49.gate_part, ...), custom_call_target="tpu_custom_call" | custom-call | flops 65536 | bytes 524288 | tf_op jit(solution)/shard_map/finish/pallas_call | solution.py:509
  (1 shorter events, 0.0 us)
Async XLA Ops:
  0.6 8.3 %copy-start.3 = (f32[384]{0:T(512)S(1)}, f32[384]{0:T(512)}, u32[]{:S(2)}) copy-start(f32[384]{0:T(512)} %scale.3) | copy-start | bytes 4612
  0.6 8.3 %copy-start.2 = (bf16[31,256]{1,0:T(8,128)(2,1)S(1)}, bf16[31,256]{1,0:T(8,128)(2,1)}, u32[]{:S(2)}) copy-start(bf16[31,256]{1,0:T(8,128)(2,1)} %taps.3) | copy-start | bytes 47620
  0.7 8.3 %copy-start.4 = (f32[384]{0:T(512)S(1)}, f32[384]{0:T(512)}, u32[]{:S(2)}) copy-start(f32[384]{0:T(512)} %mean.1) | copy-start | bytes 4612
  0.7 8.3 %copy-start.5 = (f32[256]{0:T(256)S(1)}, f32[256]{0:T(256)}, u32[]{:S(2)}) copy-start(f32[256]{0:T(256)} %param.13) | copy-start | bytes 3076
  1.5 7.5 %collective-permute-start = (bf16[32,256]{1,0:T(8,128)(2,1)S(1)}, bf16[32,256]{1,0:T(8,128)(2,1)S(1)}, u32[]{:S(2)}, u32[]{:S(2)}) collective-permute-start(bf16[32,256]{1,0:T(8,128)(2,1)S(1)} %multiply_convert_fusion), channel_id=1, source_target_pairs={{0,4},{4,8},{8,12},{12,16},{16,20},{20,24},{24,28},{28,32},{32,36}... | collective-permute-start | bytes 49160 | tf_op jit(solution)/shard_map/ppermute | solution.py:38
  8.9 10.5 %copy-start = (bf16[384,256]{1,0:T(8,128)(2,1)S(1)}, bf16[384,256]{1,0:T(8,128)(2,1)}, u32[]{:S(2)}) copy-start(bf16[384,256]{1,0:T(8,128)(2,1)} %gate.3) | copy-start | bytes 589828
  8.9 10.5 %copy-start.1 = (bf16[384,256]{1,0:T(8,128)(2,1)S(1)}, bf16[384,256]{1,0:T(8,128)(2,1)}, u32[]{:S(2)}) copy-start(bf16[384,256]{1,0:T(8,128)(2,1)} %value.3) | copy-start | bytes 589828
  17.4 3.9 %collective-permute-start.1 = (bf16[2176,128]{1,0:T(8,128)(2,1)S(1)}, bf16[2176,128]{1,0:T(8,128)(2,1)S(1)}, u32[]{:S(2)}, u32[]{:S(2)}) collective-permute-start(bf16[2176,128]{1,0:T(8,128)(2,1)S(1)} %get-tuple-element.47), channel_id=1, source_target_pairs={{0,4},{4,0},{1,5},{5,1},{2,6},{6,2},{3,7},{7,3},{8,12},{12,8},{9,1... | collective-permute-start | bytes 1671176 | tf_op jit(solution)/shard_map/ppermute | solution.py:446
  43.2 18.1 %collective-permute-start.2 = (bf16[320,128]{1,0:T(8,128)(2,1)S(1)}, bf16[320,128]{1,0:T(8,128)(2,1)S(1)}, u32[]{:S(2)}, u32[]{:S(2)}) collective-permute-start(bf16[320,128]{1,0:T(8,128)(2,1)S(1)} %shard_map.124), channel_id=1, source_target_pairs={{0,0},{4,388},{8,968},{12,460},{16,912},{20,532},{24,856},{28,348}... | collective-permute-start | bytes 245768 | tf_op jit(solution)/shard_map/ppermute | solution.py:382
  62.2 16.8 %all-to-all-start.2 = ((bf16[16,40,256]{2,1,0:T(8,128)(2,1)}), bf16[16,40,256]{2,1,0:T(8,128)(2,1)S(1)}, u32[]{:S(2)}, u32[]{:S(2)}) async-start(bf16[16,40,256]{2,1,0:T(8,128)(2,1)} %shard_map.125), calls=%async_computation.2 | async-start | bytes 655360 | tf_op jit(solution)/shard_map/all_to_all | solution.py:43
  71.0 8.3 %collective-permute-start.3 = (f32[2,32,128]{2,1,0:T(8,128)S(1)}, f32[2,32,128]{2,1,0:T(8,128)S(1)}, u32[]{:S(2)}, u32[]{:S(2)}) collective-permute-start(f32[2,32,128]{2,1,0:T(8,128)S(1)} %get-tuple-element.51), channel_id=1, source_target_pairs={{4,0},{8,4},{12,8},{16,12},{20,16},{24,20},{28,24},{32,28},{36,32}... | collective-permute-start | bytes 98312 | tf_op jit(solution)/shard_map/ppermute | solution.py:38
